TPU v7x, 512 devices: a whole 4x8x8 slice. The times are simulated.
512 devices in a mesh: fs: 64 (over z, y), tp: 8 (over x, core).
Axes of the slice: x: 4, y: 8, z: 8, core: 2. Of those that a mesh axis runs over, the one named last changes fastest.
Arguments:
- inputs: bfloat16 [24576, 2048], P('fs'), may hold values from -6 to 6
- gain: float32 [2048], replicated, may hold values from 0.1 to 1.9
- w_gate: bfloat16 [2048, 2816], P('fs', 'tp'), may hold values from -0.125 to 0.125
- w_up: bfloat16 [2048, 2816], P('fs', 'tp'), may hold values from -0.125 to 0.125
- w_down: bfloat16 [2816, 2048], P('tp', 'fs'), may hold values from -0.109375 to 0.109375
- cotangent: bfloat16 [24576, 2048], P('fs'), may hold values from -16 to 16
Outputs:
- input_gradient: bfloat16 [24576, 2048], P('fs')
- grad_down: float32 [2816, 2048], P('tp', 'fs')
All inputs are finite; a program needn't handle non-finite values.
Results may differ from a plain program's by a relative error of at most 0.014.
Values may be sent and summed in bfloat16 or wider, within the bound.
No kernel may reach another device: no remote copies, remote signals or barrier semaphores. Data moves between devices by JAX's collectives and lax.ppermute only.
A program may use at most 64 MiB of HBM per device.

v0:
```python
import jax
import jax.numpy as jnp
from jax import lax
from jax.experimental import pallas as pl
from jax.experimental.pallas import tpu as pltpu
from jax.sharding import Mesh
from jax.sharding import PartitionSpec as P


AXES = ("z", "y", "x", "c")
NZ, NY, NX, NC = 8, 8, 4, 2
FS = ("z", "y")
TP = ("x", "c")
EPSILON = 1e-06
HALF_STEP = 0.5
TOK = 384
D = 2048
HU = 352
HP = 384
DROWS = 32
HALF = TOK // NC
QUARTER = HALF // NX
VMEM_LIMIT = 32 * 2**20
SMALL_LIMIT = 10 * 2**20


def device_number(z, y, x, c):
    return ((z % NZ * NY + y % NY) * NX + x) * NC + c


def ring_pairs(step):
    return [
        (device_number(z, y, x, c), device_number(z + (1 - c) * step, y + c * step, x, c))
        for z in range(NZ)
        for y in range(NY)
        for x in range(NX)
        for c in range(NC)
    ]


def line_groups(along_ring):
    groups = []
    for x in range(NX):
        for c in range(NC):
            vary_z = (c == 0) == along_ring
            for fixed in range(8):
                groups.append(
                    [
                        device_number(k, fixed, x, c) if vary_z else device_number(fixed, k, x, c)
                        for k in range(8)
                    ]
                )
    return groups


def ring(array, step):
    return lax.ppermute(array, AXES, ring_pairs(step))


def exchange(array, along_ring):
    return lax.all_to_all(
        array, AXES, 0, 0, axis_index_groups=line_groups(along_ring), tiled=True
    )


def dot(left, right, dims):
    return lax.dot_general(left, right, (dims, ((), ())), preferred_element_type=jnp.float32)


def compute_kernel(
    x_ref, gain_ref, cot_ref, b0, p1, p2, p3, p4, m1, m2, m3, m4,
    own_ref, k1_ref, k2_ref, k3_ref, send_ref, x_own_ref, down_ref, w_ref, xn_ref, dt_ref,
):
    x = lax.axis_index("x")
    c = lax.axis_index("c")
    r = jnp.where(c == 0, lax.axis_index("z"), lax.axis_index("y"))

    def row_of(q, o):
        q = lax.rem(q + 16, 8)
        return pl.multiple_of(jnp.where(c == 0, q * 256 + o * 32, o * 256 + q * 32), 32)

    def put(q, block, first, last):
        for o in range(first, last):
            w_ref[pl.ds(row_of(q, o), DROWS), :] = block[pl.ds((o - first) * DROWS, DROWS), :]

    put(r, b0, 0, 8)
    for k, block in enumerate((p1, p2, p3)):
        put(r - k - 1, block, 0, 8)
    for k, block in enumerate((m1, m2, m3)):
        put(r + k + 1, block, 0, 8)
    put(r + 4, p4, 0, 4)
    put(r + 4, m4, 4, 8)

    gain = gain_ref[...]
    for k in range(6):
        rows = pl.ds(k * 64, 64)
        value = x_ref[rows, :].astype(jnp.float32)
        inverse = lax.rsqrt(jnp.mean(value * value, axis=-1, keepdims=True) + EPSILON)
        xn_ref[rows, :] = (value * inverse * gain).astype(jnp.bfloat16)

    gate_up = dot(xn_ref[...], w_ref[:, : 2 * HP], ((1,), (0,)))
    gate = gate_up[:, :HP]
    up = gate_up[:, HP:]
    d_hidden = HALF_STEP * dot(cot_ref[...], w_ref[:, 2 * HP :], ((1,), (0,)))
    sig = jax.nn.sigmoid(gate)
    hidden = (gate * sig * up).astype(jnp.bfloat16)
    d_gate = (d_hidden * up * sig * (1.0 + gate * (1.0 - sig))).astype(jnp.bfloat16)
    d_up = (d_hidden * gate * sig).astype(jnp.bfloat16)
    both = jnp.concatenate([d_gate, d_up], axis=1)
    xn_ref[...] = dot(both, w_ref[:, : 2 * HP], ((1,), (1,))).astype(jnp.bfloat16)

    def quarter(core, k):
        row = core * HALF + lax.rem(x + k, NX) * QUARTER
        return pl.ds(pl.multiple_of(row, 16), QUARTER)

    for k, ref in enumerate((own_ref, k1_ref, k2_ref, k3_ref)):
        ref[...] = xn_ref[quarter(c, k), :]
        send_ref[pl.ds(k * QUARTER, QUARTER), :] = xn_ref[quarter(1 - c, k), :]
    x_own_ref[...] = x_ref[quarter(c, 0), :]
    dt_ref[...] = (HALF_STEP * dot(cot_ref[...], hidden, ((0,), (0,)))).astype(jnp.bfloat16)
    for q in range(8):
        for o in range(8):
            down_ref[pl.ds(q * 256 + o * 32, DROWS), :] = dt_ref[pl.ds(row_of(q, o), DROWS), :]


def vmem_specs(count):
    return [pl.BlockSpec(memory_space=pltpu.VMEM)] * count


def small_call(kernel, out_shape, *operands):
    count = len(out_shape)
    return pl.pallas_call(
        kernel,
        out_shape=tuple(out_shape),
        in_specs=vmem_specs(len(operands)),
        out_specs=tuple(vmem_specs(count)),
        compiler_params=pltpu.CompilerParams(vmem_limit_bytes=SMALL_LIMIT),
    )(*operands)


def compute(inputs, gain, cotangent, blocks):
    quarter = jax.ShapeDtypeStruct((QUARTER, D), jnp.bfloat16)
    return pl.pallas_call(
        compute_kernel,
        out_shape=(
            quarter, quarter, quarter, quarter,
            jax.ShapeDtypeStruct((HALF, D), jnp.bfloat16),
            quarter,
            jax.ShapeDtypeStruct((D, HP), jnp.bfloat16),
        ),
        in_specs=vmem_specs(3 + len(blocks)),
        out_specs=tuple(vmem_specs(7)),
        scratch_shapes=[
            pltpu.VMEM((D, 3 * HP), jnp.bfloat16),
            pltpu.VMEM((TOK, D), jnp.bfloat16),
            pltpu.VMEM((D, HP), jnp.bfloat16),
        ],
        compiler_params=pltpu.CompilerParams(vmem_limit_bytes=VMEM_LIMIT),
    )(inputs, gain.reshape(1, D), cotangent, *blocks)


def pair_kernel(own_ref, k1_ref, k2_ref, k3_ref, other_ref, s0_ref, s1_ref, s2_ref, s3_ref):
    kept = (own_ref, k1_ref, k2_ref, k3_ref)
    for k, out in enumerate((s0_ref, s1_ref, s2_ref, s3_ref)):
        other = other_ref[pl.ds(k * QUARTER, QUARTER), :].astype(jnp.float32)
        out[...] = (kept[k][...].astype(jnp.float32) + other).astype(out.dtype)


def final_kernel(x_ref, gain_ref, own_ref, q1_ref, q2_ref, q3_ref, out_ref):
    value = x_ref[...].astype(jnp.float32)
    inverse = lax.rsqrt(jnp.mean(value * value, axis=-1, keepdims=True) + EPSILON)
    normalized = value * inverse
    d_normed = own_ref[...]
    for ref in (q1_ref, q2_ref, q3_ref):
        d_normed = d_normed + ref[...].astype(jnp.float32)
    scaled = d_normed * gain_ref[...]
    mean = jnp.mean(scaled * normalized, axis=-1, keepdims=True)
    out_ref[...] = (inverse * (scaled - normalized * mean)).astype(jnp.bfloat16)


def sum_kernel(parts_ref, out_ref):
    total = parts_ref[0].astype(jnp.float32)
    for k in range(1, 8):
        total = total + parts_ref[k].astype(jnp.float32)
    out_ref[...] = total.astype(out_ref.dtype)


def along_x(array, step):
    return lax.ppermute(array, "x", [(k, (k + step) % NX) for k in range(NX)])


def shards(inputs, gain, w_gate, w_up, w_down, cotangent):
    c = lax.axis_index("c")
    pad = ((0, 0), (0, HP - HU))
    packed = jnp.concatenate([jnp.pad(w, pad) for w in (w_gate, w_up, w_down.T)], axis=1)
    block = exchange(jnp.broadcast_to(packed[None], (8, DROWS, 3 * HP)), False)
    b0 = block.reshape(256, 3 * HP)
    p2 = ring(b0, 2)
    m2 = ring(b0, -2)
    p1 = ring(b0, 1)
    m1 = ring(b0, -1)
    p3 = ring(p2, 1)
    m3 = ring(m2, -1)
    p4 = ring(p2[:128], 2)
    m4 = ring(m2[128:], -2)

    own, k1, k2, k3, send, x_own, down = compute(
        inputs, gain, cotangent, (b0, p1, p2, p3, p4, m1, m2, m3, m4)
    )

    arrived = exchange(down.reshape(8, 256, HP), True)
    (line,) = small_call(sum_kernel, [jax.ShapeDtypeStruct((256, HP), jnp.bfloat16)], arrived)
    quarter = jax.ShapeDtypeStruct((QUARTER, D), jnp.bfloat16)
    other = lax.ppermute(send, "c", [(0, 1), (1, 0)])
    own, *sums = small_call(
        pair_kernel,
        [jax.ShapeDtypeStruct((QUARTER, D), jnp.float32)] + [quarter] * 3,
        own, k1, k2, k3, other,
    )
    quarters = [along_x(s, k + 1) for k, s in enumerate(sums)]
    (mine,) = small_call(final_kernel, [quarter], x_own, gain.reshape(1, D), own, *quarters)
    mine, line = lax.optimization_barrier((mine, line))
    arrived = exchange(line.reshape(8, DROWS, HP), False)
    (total,) = small_call(sum_kernel, [jax.ShapeDtypeStruct((DROWS, HP), jnp.float32)], arrived)
    grad_down = total[:, :HU].T
    half = lax.all_gather(mine, "x", axis=0, tiled=True)
    away = lax.ppermute(half, "c", [(0, 1), (1, 0)])
    whole = jnp.zeros((TOK, D), jnp.bfloat16)
    whole = lax.dynamic_update_slice_in_dim(whole, half, c * HALF, 0)
    whole = lax.dynamic_update_slice_in_dim(whole, away, (1 - c) * HALF, 0)
    return whole, grad_down


def solution(mesh):
    split = Mesh(mesh.devices.reshape(NZ, NY, NX, NC), AXES)
    in_specs = (P(FS, None), P(), P(FS, TP), P(FS, TP), P(TP, FS), P(FS, None))
    out_specs = (P(FS, None), P(TP, FS))
    return jax.shard_map(
        shards, mesh=split, in_specs=in_specs, out_specs=out_specs, check_vma=False
    )
```

profile of v0, /device:TPU:1, one launch (start us, length us, event | category | flops | bytes accessed | tf_op | source)
XLA Modules:
  0.0 141.7 jit_solution(18004432298905986871)
XLA Ops:
  0.7 0.9 fusion.5
  1.6 23.5 %all_to_all.15 = bf16[8,32,1152]{2,1,0:T(8,128)(2,1)S(1)} all-to-all(bf16[8,32,1152]{2,1,0:T(8,128)(2,1)S(1)} %broadcast_in_dim.10), channel_id=1, replica_groups={{0,8,16,24,32,40,48,56},{64,72,80,88,96,104,112,120},{128,136,144,152,1..., dimensions={0} | all-to-all | bytes 1179648 | tf_op jit(solution)/shard_map/all_to_all | solution.py:61
  25.1 4.2 %collective-permute-start.1 = (bf16[256,1152]{1,0:T(8,128)(2,1)S(1)}, bf16[256,1152]{1,0:T(8,128)(2,1)S(1)}, u32[]{:S(2)}, u32[]{:S(2)}) collective-permute-start(bf16[256,1152]{1,0:T(8,128)(2,1)S(1)} %bitcast.7), channel_id=1, source_target_pairs={{0,128},{1,17},{2,130},{3,19},{4,132},{5,21},{6,134},{7,23},{8,136... | collective-permute-start | bytes 1769480 | tf_op jit(solution)/shard_map/ppermute | solution.py:57
  29.4 3.6 %collective-permute-start.5 = (bf16[256,1152]{1,0:T(8,128)(2,1)S(1)}, bf16[256,1152]{1,0:T(8,128)(2,1)S(1)}, u32[]{:S(2)}, u32[]{:S(2)}) collective-permute-start(bf16[256,1152]{1,0:T(8,128)(2,1)S(1)} %bitcast.8), channel_id=1, source_target_pairs={{0,384},{1,49},{2,386},{3,51},{4,388},{5,53},{6,390},{7,55},{8,392... | collective-permute-start | bytes 1769480 | tf_op jit(solution)/shard_map/ppermute | solution.py:57
  33.0 2.8 %collective-permute-start = (bf16[256,1152]{1,0:T(8,128)(2,1)S(1)}, bf16[256,1152]{1,0:T(8,128)(2,1)S(1)}, u32[]{:S(2)}, u32[]{:S(2)}) collective-permute-start(bf16[256,1152]{1,0:T(8,128)(2,1)S(1)} %bitcast.9), channel_id=1, source_target_pairs={{0,64},{1,9},{2,66},{3,11},{4,68},{5,13},{6,70},{7,15},{8,72},{9,1... | collective-permute-start | bytes 1769480 | tf_op jit(solution)/shard_map/ppermute | solution.py:57
  35.8 3.7 %collective-permute-start.4 = (bf16[256,1152]{1,0:T(8,128)(2,1)S(1)}, bf16[256,1152]{1,0:T(8,128)(2,1)S(1)}, u32[]{:S(2)}, u32[]{:S(2)}) collective-permute-start(bf16[256,1152]{1,0:T(8,128)(2,1)S(1)} %bitcast.10), channel_id=1, source_target_pairs={{0,448},{1,57},{2,450},{3,59},{4,452},{5,61},{6,454},{7,63},{8,456... | collective-permute-start | bytes 1769480 | tf_op jit(solution)/shard_map/ppermute | solution.py:57
  39.5 2.1 %collective-permute-done.1.p2 = bf16[256,1152]{1,0:T(8,128)(2,1)S(1)} collective-permute-done((bf16[256,1152]{1,0:T(8,128)(2,1)S(1)}, bf16[256,1152]{1,0:T(8,128)(2,1)S(1)}, u32[]{:S(2)}, u32[]{:S(2)}) %collective-permute-start.1) | collective-permute-done | bytes 589856 | tf_op jit(solution)/shard_map/ppermute | solution.py:57
  41.5 5.9 %collective-permute-start.2 = (bf16[256,1152]{1,0:T(8,128)(2,1)S(1)}, bf16[256,1152]{1,0:T(8,128)(2,1)S(1)}, u32[]{:S(2)}, u32[]{:S(2)}) collective-permute-start(bf16[256,1152]{1,0:T(8,128)(2,1)S(1)} %collective-permute-done.1.p2), channel_id=1, source_target_pairs={{0,64},{1,9},{2,66},{3,11},{4,68},{5,13},{6,70},{7,15},{8,72},{9,1... | collective-permute-start | bytes 1769480 | tf_op jit(solution)/shard_map/ppermute | solution.py:57
  47.5 1.2 collective-permute-done.5.m2
  48.7 1.9 %collective-permute-start.6 = (bf16[256,1152]{1,0:T(8,128)(2,1)S(1)}, bf16[256,1152]{1,0:T(8,128)(2,1)S(1)}, u32[]{:S(2)}, u32[]{:S(2)}) collective-permute-start(bf16[256,1152]{1,0:T(8,128)(2,1)S(1)} %collective-permute-done.5.m2), channel_id=1, source_target_pairs={{0,448},{1,57},{2,450},{3,59},{4,452},{5,61},{6,454},{7,63},{8,456... | collective-permute-start | bytes 1769480 | tf_op jit(solution)/shard_map/ppermute | solution.py:57
  50.7 4.4 %collective-permute-start.3 = (bf16[128,1152]{1,0:T(8,128)(2,1)S(1)}, bf16[128,1152]{1,0:T(8,128)(2,1)S(1)}, u32[]{:S(2)}, u32[]{:S(2)}) collective-permute-start(bf16[128,1152]{1,0:T(8,128)(2,1)S(1)} %slice.12), channel_id=1, source_target_pairs={{0,128},{1,17},{2,130},{3,19},{4,132},{5,21},{6,134},{7,23},{8,136... | collective-permute-start | bytes 884744 | tf_op jit(solution)/shard_map/ppermute | solution.py:57
  55.1 3.0 %collective-permute-start.7 = (bf16[128,1152]{1,0:T(8,128)(2,1)S(1)}, bf16[128,1152]{1,0:T(8,128)(2,1)S(1)}, u32[]{:S(2)}, u32[]{:S(2)}) collective-permute-start(bf16[128,1152]{1,0:T(8,128)(2,1)S(1)} %slice.13), channel_id=1, source_target_pairs={{0,384},{1,49},{2,386},{3,51},{4,388},{5,53},{6,390},{7,55},{8,392... | collective-permute-start | bytes 884744 | tf_op jit(solution)/shard_map/ppermute | solution.py:57
  58.1 3.3 %collective-permute-done.3.p4 = bf16[128,1152]{1,0:T(8,128)(2,1)S(1)} collective-permute-done((bf16[128,1152]{1,0:T(8,128)(2,1)S(1)}, bf16[128,1152]{1,0:T(8,128)(2,1)S(1)}, u32[]{:S(2)}, u32[]{:S(2)}) %collective-permute-start.3) | collective-permute-done | bytes 294944 | tf_op jit(solution)/shard_map/ppermute | solution.py:57
  61.4 6.6 %collective-permute-done.7.m4 = bf16[128,1152]{1,0:T(8,128)(2,1)S(1)} collective-permute-done((bf16[128,1152]{1,0:T(8,128)(2,1)S(1)}, bf16[128,1152]{1,0:T(8,128)(2,1)S(1)}, u32[]{:S(2)}, u32[]{:S(2)}) %collective-permute-start.7) | collective-permute-done | bytes 294944 | tf_op jit(solution)/shard_map/ppermute | solution.py:57
  68.0 7.4 %shard_map.77 = (bf16[48,2048]{1,0:T(8,128)(2,1)S(1)}, bf16[48,2048]{1,0:T(8,128)(2,1)S(1)}, bf16[48,2048]{1,0:T(8,128)(2,1)S(1)}, bf16[48,2048]{1,0:T(8,128)(2,...) custom-call(bf16[384,2048]{1,0:T(8,128)(2,1)S(1)} %copy-done, ...), custom_call_target="tpu_custom_call" | custom-call | tf_op jit(solution)/shard_map/pallas_call | solution.py:143
  75.4 4.4 %all-to-all-start.1 = ((bf16[8,256,384]{2,1,0:T(8,128)(2,1)}), bf16[8,256,384]{2,1,0:T(8,128)(2,1)S(1)}, u32[]{:S(2)}, u32[]{:S(2)}) async-start(bf16[8,256,384]{2,1,0:T(8,128)(2,1)} %bitcast.3), calls=%async_computation.1 | async-start | bytes 3145728 | tf_op jit(solution)/shard_map/all_to_all | solution.py:61
  79.7 7.3 %collective-permute-start.8 = (bf16[192,2048]{1,0:T(8,128)(2,1)S(1)}, bf16[192,2048]{1,0:T(8,128)(2,1)S(1)}, u32[]{:S(2)}, u32[]{:S(2)}) collective-permute-start(bf16[192,2048]{1,0:T(8,128)(2,1)S(1)} %get-tuple-element.20), channel_id=1, source_target_pairs={{0,1},{1,0},{2,3},{3,2},{4,5},{5,4},{6,7},{7,6},{8,9},{9,8},{10,11... | collective-permute-start | bytes 2359304 | tf_op jit(solution)/shard_map/ppermute | solution.py:214
  87.1 1.9 %collective-permute-done.8.other_ref = bf16[192,2048]{1,0:T(8,128)(2,1)S(1)} collective-permute-done((bf16[192,2048]{1,0:T(8,128)(2,1)S(1)}, bf16[192,2048]{1,0:T(8,128)(2,1)S(1)}, u32[]{:S(2)}, u32[]{:S(2)}) %collective-permute-start.8) | collective-permute-done | bytes 786464 | tf_op jit(solution)/shard_map/ppermute | solution.py:214
  89.1 4.7 %collective-permute-start.10 = (bf16[48,2048]{1,0:T(8,128)(2,1)S(1)}, bf16[48,2048]{1,0:T(8,128)(2,1)S(1)}, u32[]{:S(2)}, u32[]{:S(2)}) collective-permute-start(bf16[48,2048]{1,0:T(8,128)(2,1)S(1)} %get-tuple-element.23), channel_id=1, source_target_pairs={{0,4},{2,6},{4,0},{6,2},{1,5},{3,7},{5,1},{7,3},{8,12},{10,14},{12... | collective-permute-start | bytes 589832 | tf_op jit(solution)/shard_map/ppermute | solution.py:189
  93.8 2.8 %collective-permute-start.11 = (bf16[48,2048]{1,0:T(8,128)(2,1)S(1)}, bf16[48,2048]{1,0:T(8,128)(2,1)S(1)}, u32[]{:S(2)}, u32[]{:S(2)}) collective-permute-start(bf16[48,2048]{1,0:T(8,128)(2,1)S(1)} %get-tuple-element.24), channel_id=1, source_target_pairs={{0,6},{2,0},{4,2},{6,4},{1,7},{3,1},{5,3},{7,5},{8,14},{10,8},{12,... | collective-permute-start | bytes 589832 | tf_op jit(solution)/shard_map/ppermute | solution.py:189
  96.6 2.5 %collective-permute-start.9 = (bf16[48,2048]{1,0:T(8,128)(2,1)S(1)}, bf16[48,2048]{1,0:T(8,128)(2,1)S(1)}, u32[]{:S(2)}, u32[]{:S(2)}) collective-permute-start(bf16[48,2048]{1,0:T(8,128)(2,1)S(1)} %get-tuple-element.22), channel_id=1, source_target_pairs={{0,2},{2,4},{4,6},{6,0},{1,3},{3,5},{5,7},{7,1},{8,10},{10,12},{12... | collective-permute-start | bytes 589832 | tf_op jit(solution)/shard_map/ppermute | solution.py:189
  99.1 3.8 %collective-permute-done.11.q3_ref = bf16[48,2048]{1,0:T(8,128)(2,1)S(1)} collective-permute-done((bf16[48,2048]{1,0:T(8,128)(2,1)S(1)}, bf16[48,2048]{1,0:T(8,128)(2,1)S(1)}, u32[]{:S(2)}, u32[]{:S(2)}) %collective-permute-start.11) | collective-permute-done | bytes 196640 | tf_op jit(solution)/shard_map/ppermute | solution.py:189
  102.9 2.3 %collective-permute-done.9.q1_ref = bf16[48,2048]{1,0:T(8,128)(2,1)S(1)} collective-permute-done((bf16[48,2048]{1,0:T(8,128)(2,1)S(1)}, bf16[48,2048]{1,0:T(8,128)(2,1)S(1)}, u32[]{:S(2)}, u32[]{:S(2)}) %collective-permute-start.9) | collective-permute-done | bytes 196640 | tf_op jit(solution)/shard_map/ppermute | solution.py:189
  105.2 0.3 shard_map.79
  105.5 0.9 shard_map.80
  106.4 11.6 %all_gather.3 = bf16[192,2048]{1,0:T(8,128)(2,1)S(1)} all-gather(bf16[48,2048]{1,0:T(8,128)(2,1)S(1)} %shard_map.79), channel_id=1, replica_groups=mesh['z'=8,'y'=8,'x'=4,'c'=2] {'x'}, dimensions={0}, use_global_device_ids=true | all-gather | bytes 983040 | tf_op jit(solution)/shard_map/all_gather | solution.py:226
  117.9 9.1 %collective-permute-start.12 = (bf16[192,2048]{1,0:T(8,128)(2,1)S(1)}, bf16[192,2048]{1,0:T(8,128)(2,1)S(1)}, u32[]{:S(2)}, u32[]{:S(2)}) collective-permute-start(bf16[192,2048]{1,0:T(8,128)(2,1)S(1)} %all_gather.3), channel_id=1, source_target_pairs={{0,1},{1,0},{2,3},{3,2},{4,5},{5,4},{6,7},{7,6},{8,9},{9,8},{10,11... | collective-permute-start | bytes 2359304 | tf_op jit(solution)/shard_map/ppermute | solution.py:227
  127.1 4.0 %all-to-all-start.2 = ((bf16[8,32,384]{2,1,0:T(8,128)(2,1)}), bf16[8,32,384]{2,1,0:T(8,128)(2,1)S(1)}, u32[]{:S(2)}, u32[]{:S(2)}) async-start(bf16[8,32,384]{2,1,0:T(8,128)(2,1)} %bitcast.4), calls=%async_computation.2 | async-start | bytes 393216 | tf_op jit(solution)/shard_map/all_to_all | solution.py:61
  131.0 0.2 broadcast_in_dim.4
  131.3 8.5 %all-to-all-done.2.parts_ref = bf16[8,32,384]{2,1,0:T(8,128)(2,1)S(1)} async-done(((bf16[8,32,384]{2,1,0:T(8,128)(2,1)}), bf16[8,32,384]{2,1,0:T(8,128)(2,1)S(1)}, u32[]{:S(2)}, u32[]{:S(2)}) %all-to-all-start.2) | async-done | bytes 196640 | tf_op jit(solution)/shard_map/all_to_all | solution.py:61
  139.8 0.6 slice_bitcast_fusion
  140.5 1.1 copy-done.3
  (21 shorter events, 0.5 us)
Async XLA Ops:
  0.6 67.4 %copy-start = (bf16[384,2048]{1,0:T(8,128)(2,1)S(1)}, bf16[384,2048]{1,0:T(8,128)(2,1)}, u32[]{:S(2)}) copy-start(bf16[384,2048]{1,0:T(8,128)(2,1)} %x_ref.1) | copy-start | bytes 4718596
  0.6 67.3 %copy-start.1 = (bf16[384,2048]{1,0:T(8,128)(2,1)S(1)}, bf16[384,2048]{1,0:T(8,128)(2,1)}, u32[]{:S(2)}) copy-start(bf16[384,2048]{1,0:T(8,128)(2,1)} %cot_ref.1) | copy-start | bytes 4718596
  0.7 67.3 %copy-start.2 = (f32[2048]{0:T(1024)S(1)}, f32[2048]{0:T(1024)}, u32[]{:S(2)}) copy-start(f32[2048]{0:T(1024)} %param.7) | copy-start | bytes 24580
  25.1 16.4 %collective-permute-start.1 = (bf16[256,1152]{1,0:T(8,128)(2,1)S(1)}, bf16[256,1152]{1,0:T(8,128)(2,1)S(1)}, u32[]{:S(2)}, u32[]{:S(2)}) collective-permute-start(bf16[256,1152]{1,0:T(8,128)(2,1)S(1)} %bitcast.7), channel_id=1, source_target_pairs={{0,128},{1,17},{2,130},{3,19},{4,132},{5,21},{6,134},{7,23},{8,136... | collective-permute-start | bytes 1769480 | tf_op jit(solution)/shard_map/ppermute | solution.py:57
  29.4 19.4 %collective-permute-start.5 = (bf16[256,1152]{1,0:T(8,128)(2,1)S(1)}, bf16[256,1152]{1,0:T(8,128)(2,1)S(1)}, u32[]{:S(2)}, u32[]{:S(2)}) collective-permute-start(bf16[256,1152]{1,0:T(8,128)(2,1)S(1)} %bitcast.8), channel_id=1, source_target_pairs={{0,384},{1,49},{2,386},{3,51},{4,388},{5,53},{6,390},{7,55},{8,392... | collective-permute-start | bytes 1769480 | tf_op jit(solution)/shard_map/ppermute | solution.py:57
  33.0 22.1 %collective-permute-start = (bf16[256,1152]{1,0:T(8,128)(2,1)S(1)}, bf16[256,1152]{1,0:T(8,128)(2,1)S(1)}, u32[]{:S(2)}, u32[]{:S(2)}) collective-permute-start(bf16[256,1152]{1,0:T(8,128)(2,1)S(1)} %bitcast.9), channel_id=1, source_target_pairs={{0,64},{1,9},{2,66},{3,11},{4,68},{5,13},{6,70},{7,15},{8,72},{9,1... | collective-permute-start | bytes 1769480 | tf_op jit(solution)/shard_map/ppermute | solution.py:57
  35.8 22.4 %collective-permute-start.4 = (bf16[256,1152]{1,0:T(8,128)(2,1)S(1)}, bf16[256,1152]{1,0:T(8,128)(2,1)S(1)}, u32[]{:S(2)}, u32[]{:S(2)}) collective-permute-start(bf16[256,1152]{1,0:T(8,128)(2,1)S(1)} %bitcast.10), channel_id=1, source_target_pairs={{0,448},{1,57},{2,450},{3,59},{4,452},{5,61},{6,454},{7,63},{8,456... | collective-permute-start | bytes 1769480 | tf_op jit(solution)/shard_map/ppermute | solution.py:57
  41.5 26.4 %collective-permute-start.2 = (bf16[256,1152]{1,0:T(8,128)(2,1)S(1)}, bf16[256,1152]{1,0:T(8,128)(2,1)S(1)}, u32[]{:S(2)}, u32[]{:S(2)}) collective-permute-start(bf16[256,1152]{1,0:T(8,128)(2,1)S(1)} %collective-permute-done.1.p2), channel_id=1, source_target_pairs={{0,64},{1,9},{2,66},{3,11},{4,68},{5,13},{6,70},{7,15},{8,72},{9,1... | collective-permute-start | bytes 1769480 | tf_op jit(solution)/shard_map/ppermute | solution.py:57
  48.7 19.3 %collective-permute-start.6 = (bf16[256,1152]{1,0:T(8,128)(2,1)S(1)}, bf16[256,1152]{1,0:T(8,128)(2,1)S(1)}, u32[]{:S(2)}, u32[]{:S(2)}) collective-permute-start(bf16[256,1152]{1,0:T(8,128)(2,1)S(1)} %collective-permute-done.5.m2), channel_id=1, source_target_pairs={{0,448},{1,57},{2,450},{3,59},{4,452},{5,61},{6,454},{7,63},{8,456... | collective-permute-start | bytes 1769480 | tf_op jit(solution)/shard_map/ppermute | solution.py:57
  50.7 10.7 %collective-permute-start.3 = (bf16[128,1152]{1,0:T(8,128)(2,1)S(1)}, bf16[128,1152]{1,0:T(8,128)(2,1)S(1)}, u32[]{:S(2)}, u32[]{:S(2)}) collective-permute-start(bf16[128,1152]{1,0:T(8,128)(2,1)S(1)} %slice.12), channel_id=1, source_target_pairs={{0,128},{1,17},{2,130},{3,19},{4,132},{5,21},{6,134},{7,23},{8,136... | collective-permute-start | bytes 884744 | tf_op jit(solution)/shard_map/ppermute | solution.py:57
  55.1 12.9 %collective-permute-start.7 = (bf16[128,1152]{1,0:T(8,128)(2,1)S(1)}, bf16[128,1152]{1,0:T(8,128)(2,1)S(1)}, u32[]{:S(2)}, u32[]{:S(2)}) collective-permute-start(bf16[128,1152]{1,0:T(8,128)(2,1)S(1)} %slice.13), channel_id=1, source_target_pairs={{0,384},{1,49},{2,386},{3,51},{4,388},{5,53},{6,390},{7,55},{8,392... | collective-permute-start | bytes 884744 | tf_op jit(solution)/shard_map/ppermute | solution.py:57
  75.4 30.1 %all-to-all-start.1 = ((bf16[8,256,384]{2,1,0:T(8,128)(2,1)}), bf16[8,256,384]{2,1,0:T(8,128)(2,1)S(1)}, u32[]{:S(2)}, u32[]{:S(2)}) async-start(bf16[8,256,384]{2,1,0:T(8,128)(2,1)} %bitcast.3), calls=%async_computation.1 | async-start | bytes 3145728 | tf_op jit(solution)/shard_map/all_to_all | solution.py:61
  79.7 9.2 %collective-permute-start.8 = (bf16[192,2048]{1,0:T(8,128)(2,1)S(1)}, bf16[192,2048]{1,0:T(8,128)(2,1)S(1)}, u32[]{:S(2)}, u32[]{:S(2)}) collective-permute-start(bf16[192,2048]{1,0:T(8,128)(2,1)S(1)} %get-tuple-element.20), channel_id=1, source_target_pairs={{0,1},{1,0},{2,3},{3,2},{4,5},{5,4},{6,7},{7,6},{8,9},{9,8},{10,11... | collective-permute-start | bytes 2359304 | tf_op jit(solution)/shard_map/ppermute | solution.py:214
  89.1 10.0 %collective-permute-start.10 = (bf16[48,2048]{1,0:T(8,128)(2,1)S(1)}, bf16[48,2048]{1,0:T(8,128)(2,1)S(1)}, u32[]{:S(2)}, u32[]{:S(2)}) collective-permute-start(bf16[48,2048]{1,0:T(8,128)(2,1)S(1)} %get-tuple-element.23), channel_id=1, source_target_pairs={{0,4},{2,6},{4,0},{6,2},{1,5},{3,7},{5,1},{7,3},{8,12},{10,14},{12... | collective-permute-start | bytes 589832 | tf_op jit(solution)/shard_map/ppermute | solution.py:189
  93.8 9.1 %collective-permute-start.11 = (bf16[48,2048]{1,0:T(8,128)(2,1)S(1)}, bf16[48,2048]{1,0:T(8,128)(2,1)S(1)}, u32[]{:S(2)}, u32[]{:S(2)}) collective-permute-start(bf16[48,2048]{1,0:T(8,128)(2,1)S(1)} %get-tuple-element.24), channel_id=1, source_target_pairs={{0,6},{2,0},{4,2},{6,4},{1,7},{3,1},{5,3},{7,5},{8,14},{10,8},{12,... | collective-permute-start | bytes 589832 | tf_op jit(solution)/shard_map/ppermute | solution.py:189
  96.6 8.6 %collective-permute-start.9 = (bf16[48,2048]{1,0:T(8,128)(2,1)S(1)}, bf16[48,2048]{1,0:T(8,128)(2,1)S(1)}, u32[]{:S(2)}, u32[]{:S(2)}) collective-permute-start(bf16[48,2048]{1,0:T(8,128)(2,1)S(1)} %get-tuple-element.22), channel_id=1, source_target_pairs={{0,2},{2,4},{4,6},{6,0},{1,3},{3,5},{5,7},{7,1},{8,10},{10,12},{12... | collective-permute-start | bytes 589832 | tf_op jit(solution)/shard_map/ppermute | solution.py:189
  117.9 22.5 %collective-permute-start.12 = (bf16[192,2048]{1,0:T(8,128)(2,1)S(1)}, bf16[192,2048]{1,0:T(8,128)(2,1)S(1)}, u32[]{:S(2)}, u32[]{:S(2)}) collective-permute-start(bf16[192,2048]{1,0:T(8,128)(2,1)S(1)} %all_gather.3), channel_id=1, source_target_pairs={{0,1},{1,0},{2,3},{3,2},{4,5},{5,4},{6,7},{7,6},{8,9},{9,8},{10,11... | collective-permute-start | bytes 2359304 | tf_op jit(solution)/shard_map/ppermute | solution.py:227
  127.1 12.7 %all-to-all-start.2 = ((bf16[8,32,384]{2,1,0:T(8,128)(2,1)}), bf16[8,32,384]{2,1,0:T(8,128)(2,1)S(1)}, u32[]{:S(2)}, u32[]{:S(2)}) async-start(bf16[8,32,384]{2,1,0:T(8,128)(2,1)} %bitcast.4), calls=%async_computation.2 | async-start | bytes 393216 | tf_op jit(solution)/shard_map/all_to_all | solution.py:61
  140.5 1.1 copy-start.3
where the time goes:
time: 142 us
  starting transfers between devices  64.2 us (45%)
  blocking collectives  35.1 us (25%)
  waiting for transfers between devices  29.6 us (21%)
  Pallas kernels  8.76 us (6%)
  local copies, waits for them, and re-layouts  2.18 us (2%)
    ppermute x8, starting transfers between devices, ring(): return lax.ppermute(array, AXES, ring_pairs(step))  29.5 us
    all_to_all x1, blocking collectives, exchange(): lax.all_to_all(array, AXES, 0, 0, axis_index_groups=line_groups(along_rin...  23.5 us
    ppermute x8, waiting for transfers between devices, ring(): return lax.ppermute(array, AXES, ring_pairs(step))  13.2 us
    all_gather x1, blocking collectives, shards(): half = lax.all_gather(mine, 'x', axis=0, tiled=True)  11.6 us
    ppermute x3, starting transfers between devices, along_x(): return lax.ppermute(array, 'x', [(k, (k + step) % NX) for k in range(NX)])  9.94 us
    ppermute x1, starting transfers between devices, shards(): away = lax.ppermute(half, 'c', [(0, 1), (1, 0)])  9.13 us
    all_to_all x2, waiting for transfers between devices, exchange(): lax.all_to_all(array, AXES, 0, 0, axis_index_groups=line_groups(along_rin...  8.5 us
    all_to_all x2, starting transfers between devices, exchange(): lax.all_to_all(array, AXES, 0, 0, axis_index_groups=line_groups(along_rin...  8.31 us
  transfers between devices with their start and end apart: 15, of which 8 were waited for; matrix products, arithmetic and copies ran while one was open for 1% of the time, Pallas kernels for 0%

commit v1 on v0

--- a/solution.py
+++ b/solution.py
@@ -22,6 +22,7 @@
 QUARTER = HALF // NX
 VMEM_LIMIT = 32 * 2**20
 SMALL_LIMIT = 10 * 2**20
+DOWN_LIMIT = 24 * 2**20
 
 
 def device_number(z, y, x, c):
@@ -67,9 +68,20 @@
     return lax.dot_general(left, right, (dims, ((), ())), preferred_element_type=jnp.float32)
 
 
+def partner(core, x, k):
+    near = jnp.where(core == 0, 3 - x, x + 1 - 2 * lax.rem(x, 2))
+    far = jnp.where(core == 0, x + 1 - 2 * lax.rem(x, 2), 3 - x)
+    return (x, near, far, lax.rem(x + 2, NX))[k]
+
+
+def quarter_rows(core, x, k):
+    row = core * HALF + partner(core, x, k) * QUARTER
+    return pl.ds(pl.multiple_of(row, 16), QUARTER)
+
+
 def compute_kernel(
     x_ref, gain_ref, cot_ref, b0, p1, p2, p3, p4, m1, m2, m3, m4,
-    own_ref, k1_ref, k2_ref, k3_ref, send_ref, x_own_ref, down_ref, w_ref, xn_ref, dt_ref,
+    keep_ref, send_ref, x_own_ref, hidden_ref, w_ref, xn_ref,
 ):
     x = lax.axis_index("x")
     c = lax.axis_index("c")
@@ -109,18 +121,23 @@
     both = jnp.concatenate([d_gate, d_up], axis=1)
     xn_ref[...] = dot(both, w_ref[:, : 2 * HP], ((1,), (1,))).astype(jnp.bfloat16)
 
-    def quarter(core, k):
-        row = core * HALF + lax.rem(x + k, NX) * QUARTER
-        return pl.ds(pl.multiple_of(row, 16), QUARTER)
-
-    for k, ref in enumerate((own_ref, k1_ref, k2_ref, k3_ref)):
-        ref[...] = xn_ref[quarter(c, k), :]
-        send_ref[pl.ds(k * QUARTER, QUARTER), :] = xn_ref[quarter(1 - c, k), :]
-    x_own_ref[...] = x_ref[quarter(c, 0), :]
-    dt_ref[...] = (HALF_STEP * dot(cot_ref[...], hidden, ((0,), (0,)))).astype(jnp.bfloat16)
+    hidden_ref[...] = hidden
+    for k in range(NX):
+        rows = pl.ds(k * QUARTER, QUARTER)
+        keep_ref[rows, :] = xn_ref[quarter_rows(c, x, k), :]
+        send_ref[rows, :] = xn_ref[quarter_rows(1 - c, x, k), :]
+    x_own_ref[...] = x_ref[quarter_rows(c, x, 0), :]
+
+
+def down_kernel(cot_ref, hidden_ref, down_ref, dt_ref):
+    c = lax.axis_index("c")
+    dt = dot(cot_ref[...], hidden_ref[...], ((0,), (0,)))
+    dt_ref[...] = (HALF_STEP * dt).astype(jnp.bfloat16)
     for q in range(8):
         for o in range(8):
-            down_ref[pl.ds(q * 256 + o * 32, DROWS), :] = dt_ref[pl.ds(row_of(q, o), DROWS), :]
+            row = jnp.where(c == 0, q * 256 + o * 32, o * 256 + q * 32)
+            rows = pl.ds(pl.multiple_of(row, 32), DROWS)
+            down_ref[pl.ds(q * 256 + o * 32, DROWS), :] = dt_ref[rows, :]
 
 
 def vmem_specs(count):
@@ -139,43 +156,91 @@
 
 
 def compute(inputs, gain, cotangent, blocks):
-    quarter = jax.ShapeDtypeStruct((QUARTER, D), jnp.bfloat16)
+    half = jax.ShapeDtypeStruct((HALF, D), jnp.bfloat16)
     return pl.pallas_call(
         compute_kernel,
         out_shape=(
-            quarter, quarter, quarter, quarter,
-            jax.ShapeDtypeStruct((HALF, D), jnp.bfloat16),
-            quarter,
-            jax.ShapeDtypeStruct((D, HP), jnp.bfloat16),
+            half,
+            half,
+            jax.ShapeDtypeStruct((QUARTER, D), jnp.bfloat16),
+            jax.ShapeDtypeStruct((TOK, HP), jnp.bfloat16),
         ),
         in_specs=vmem_specs(3 + len(blocks)),
-        out_specs=tuple(vmem_specs(7)),
+        out_specs=tuple(vmem_specs(4)),
         scratch_shapes=[
             pltpu.VMEM((D, 3 * HP), jnp.bfloat16),
             pltpu.VMEM((TOK, D), jnp.bfloat16),
-            pltpu.VMEM((D, HP), jnp.bfloat16),
         ],
         compiler_params=pltpu.CompilerParams(vmem_limit_bytes=VMEM_LIMIT),
-    )(inputs, gain.reshape(1, D), cotangent, *blocks)
-
-
-def pair_kernel(own_ref, k1_ref, k2_ref, k3_ref, other_ref, s0_ref, s1_ref, s2_ref, s3_ref):
-    kept = (own_ref, k1_ref, k2_ref, k3_ref)
-    for k, out in enumerate((s0_ref, s1_ref, s2_ref, s3_ref)):
-        other = other_ref[pl.ds(k * QUARTER, QUARTER), :].astype(jnp.float32)
-        out[...] = (kept[k][...].astype(jnp.float32) + other).astype(out.dtype)
-
-
-def final_kernel(x_ref, gain_ref, own_ref, q1_ref, q2_ref, q3_ref, out_ref):
+    )(inputs, gain, cotangent, *blocks)
+
+
+def down_product(cotangent, hidden):
+    return pl.pallas_call(
+        down_kernel,
+        out_shape=jax.ShapeDtypeStruct((D, HP), jnp.bfloat16),
+        in_specs=vmem_specs(2),
+        out_specs=vmem_specs(1)[0],
+        scratch_shapes=[pltpu.VMEM((D, HP), jnp.bfloat16)],
+        compiler_params=pltpu.CompilerParams(vmem_limit_bytes=DOWN_LIMIT),
+    )(cotangent, hidden)
+
+
+def pair_kernel(keep_ref, other_ref, sums_ref, out_ref):
+    total = keep_ref[...].astype(jnp.float32) + other_ref[...].astype(jnp.float32)
+    sums_ref[...] = total[: 2 * QUARTER]
+    out_ref[...] = total[2 * QUARTER :].astype(jnp.bfloat16)
+
+
+def second_kernel(sums_ref, got_ref, own_ref, out_ref):
+    total = sums_ref[...] + got_ref[...].astype(jnp.float32)
+    own_ref[...] = total[:QUARTER]
+    out_ref[...] = total[QUARTER:].astype(jnp.bfloat16)
+
+
+def final_kernel(x_ref, gain_ref, own_ref, got_ref, out_ref):
     value = x_ref[...].astype(jnp.float32)
     inverse = lax.rsqrt(jnp.mean(value * value, axis=-1, keepdims=True) + EPSILON)
     normalized = value * inverse
-    d_normed = own_ref[...]
-    for ref in (q1_ref, q2_ref, q3_ref):
-        d_normed = d_normed + ref[...].astype(jnp.float32)
-    scaled = d_normed * gain_ref[...]
+    scaled = (own_ref[...] + got_ref[...].astype(jnp.float32)) * gain_ref[...]
     mean = jnp.mean(scaled * normalized, axis=-1, keepdims=True)
     out_ref[...] = (inverse * (scaled - normalized * mean)).astype(jnp.bfloat16)
+
+
+def join_kernel(first_ref, second_ref, out_ref):
+    rows = first_ref.shape[0]
+    out_ref[pl.ds(0, rows), :] = first_ref[...]
+    out_ref[pl.ds(rows, rows), :] = second_ref[...]
+
+
+def place_kernel(mine_ref, away_ref, out_ref, sems):
+    x = lax.axis_index("x")
+    c = lax.axis_index("c")
+    copies = []
+    for half, (core, ref) in enumerate(((c, mine_ref), (1 - c, away_ref))):
+        for k in range(NX):
+            copies.append(
+                pltpu.make_async_copy(
+                    ref.at[pl.ds(k * QUARTER, QUARTER), :],
+                    out_ref.at[quarter_rows(core, x, k), :],
+                    sems.at[half * NX + k],
+                )
+            )
+    for copy in copies:
+        copy.start()
+    for copy in copies:
+        copy.wait()
+
+
+def place(mine, away):
+    return pl.pallas_call(
+        place_kernel,
+        out_shape=jax.ShapeDtypeStruct((TOK, D), jnp.bfloat16),
+        in_specs=vmem_specs(2),
+        out_specs=pl.BlockSpec(memory_space=pl.ANY),
+        scratch_shapes=[pltpu.SemaphoreType.DMA((2 * NX,))],
+        compiler_params=pltpu.CompilerParams(vmem_limit_bytes=SMALL_LIMIT),
+    )(mine, away)
 
 
 def sum_kernel(parts_ref, out_ref):
@@ -185,12 +250,22 @@
     out_ref[...] = total.astype(out_ref.dtype)
 
 
-def along_x(array, step):
-    return lax.ppermute(array, "x", [(k, (k + step) % NX) for k in range(NX)])
+def with_partner(array, first):
+    pairs = [
+        (device_number(z, y, x, c), device_number(z, y, x ^ (1 if (c == 0) == first else 3), c))
+        for z in range(NZ)
+        for y in range(NY)
+        for x in range(NX)
+        for c in range(NC)
+    ]
+    return lax.ppermute(array, AXES, pairs)
+
+
+def with_core(array):
+    return lax.ppermute(array, "c", [(0, 1), (1, 0)])
 
 
 def shards(inputs, gain, w_gate, w_up, w_down, cotangent):
-    c = lax.axis_index("c")
     pad = ((0, 0), (0, HP - HU))
     packed = jnp.concatenate([jnp.pad(w, pad) for w in (w_gate, w_up, w_down.T)], axis=1)
     block = exchange(jnp.broadcast_to(packed[None], (8, DROWS, 3 * HP)), False)
@@ -204,31 +279,34 @@
     p4 = ring(p2[:128], 2)
     m4 = ring(m2[128:], -2)
 
-    own, k1, k2, k3, send, x_own, down = compute(
-        inputs, gain, cotangent, (b0, p1, p2, p3, p4, m1, m2, m3, m4)
+    row = gain.reshape(1, D)
+    keep, send, x_own, hidden = compute(
+        inputs, row, cotangent, (b0, p1, p2, p3, p4, m1, m2, m3, m4)
     )
-
+    other = with_core(send)
+    down = down_product(cotangent, hidden)
     arrived = exchange(down.reshape(8, 256, HP), True)
     (line,) = small_call(sum_kernel, [jax.ShapeDtypeStruct((256, HP), jnp.bfloat16)], arrived)
-    quarter = jax.ShapeDtypeStruct((QUARTER, D), jnp.bfloat16)
-    other = lax.ppermute(send, "c", [(0, 1), (1, 0)])
-    own, *sums = small_call(
-        pair_kernel,
-        [jax.ShapeDtypeStruct((QUARTER, D), jnp.float32)] + [quarter] * 3,
-        own, k1, k2, k3, other,
-    )
-    quarters = [along_x(s, k + 1) for k, s in enumerate(sums)]
-    (mine,) = small_call(final_kernel, [quarter], x_own, gain.reshape(1, D), own, *quarters)
-    mine, line = lax.optimization_barrier((mine, line))
     arrived = exchange(line.reshape(8, DROWS, HP), False)
     (total,) = small_call(sum_kernel, [jax.ShapeDtypeStruct((DROWS, HP), jnp.float32)], arrived)
     grad_down = total[:, :HU].T
-    half = lax.all_gather(mine, "x", axis=0, tiled=True)
-    away = lax.ppermute(half, "c", [(0, 1), (1, 0)])
-    whole = jnp.zeros((TOK, D), jnp.bfloat16)
-    whole = lax.dynamic_update_slice_in_dim(whole, half, c * HALF, 0)
-    whole = lax.dynamic_update_slice_in_dim(whole, away, (1 - c) * HALF, 0)
-    return whole, grad_down
+
+    def shape(rows, kind=jnp.bfloat16):
+        return jax.ShapeDtypeStruct((rows, D), kind)
+
+    sums, out = small_call(
+        pair_kernel, [shape(2 * QUARTER, jnp.float32), shape(2 * QUARTER)], keep, other
+    )
+    got = with_partner(out, True)
+    own, out = small_call(second_kernel, [shape(QUARTER, jnp.float32), shape(QUARTER)], sums, got)
+    got = with_partner(out, False)
+    (mine,) = small_call(final_kernel, [shape(QUARTER)], x_own, row, own, got)
+    got = with_partner(mine, False)
+    (two,) = small_call(join_kernel, [shape(2 * QUARTER)], mine, got)
+    got = with_partner(two, True)
+    (four,) = small_call(join_kernel, [shape(HALF)], two, got)
+    away = with_core(four)
+    return place(four, away), grad_down
 
 
 def solution(mesh):

time: 142 us -> 148 us (1.042)
  waiting for transfers between devices: 29.6 us -> 42.3 us
  blocking collectives: 35.1 us -> 23.5 us
  starting transfers between devices: 64.2 us -> 68.5 us
    ppermute x5 -> x6, waiting for transfers between devices: 7.98 us -> 22.1 us  [the longest x4 20.2 us: with_partner(): return lax.ppermute(array, AXES, pairs)]
    all_gather x1 -> x0, blocking collectives: 11.6 us -> none  [shards(): half = lax.all_gather(mine, 'x', axis=0, tiled=True)]
    all_to_all x2, starting transfers between devices: 8.31 us -> 12.1 us  [exchange(): lax.all_to_all(array, AXES, 0, 0, axis_index_groups=line_groups(along_rin...]
    pallas_call x1 -> x3, Pallas kernels: 7.39 us -> 8.77 us  [the longest x1 4.76 us: compute(): pl.pallas_call(compute_kernel, out_shape=(half, half, jax.ShapeDtypeStruc...]
    ppermute x5 -> x6, starting transfers between devices: 26.4 us -> 27.3 us  [the longest x2 14.7 us: with_core(): return lax.ppermute(array, 'c', [(0, 1), (1, 0)])]
  transfers between devices with their start and end apart: 15 -> 16, of which waited for: 8 -> 9; matrix products, arithmetic and copies ran while one was open for 1% -> 0% of each run, Pallas kernels for 0% -> 2%
where the time goes in v1:
time: 148 us; the launch traced here: 147 us
  starting transfers between devices  68.5 us (46%)
  waiting for transfers between devices  42.3 us (29%)
  blocking collectives  23.5 us (16%)
  Pallas kernels  10.2 us (7%)
    ppermute x8, starting transfers between devices, ring(): return lax.ppermute(array, AXES, ring_pairs(step))  29.1 us
    all_to_all x1, blocking collectives, exchange(): lax.all_to_all(array, AXES, 0, 0, axis_index_groups=line_groups(along_rin...  23.5 us
    ppermute x4, waiting for transfers between devices, with_partner(): return lax.ppermute(array, AXES, pairs)  20.2 us
    ppermute x2, starting transfers between devices, with_core(): return lax.ppermute(array, 'c', [(0, 1), (1, 0)])  14.7 us
    ppermute x8, waiting for transfers between devices, ring(): return lax.ppermute(array, AXES, ring_pairs(step))  12.8 us
    ppermute x4, starting transfers between devices, with_partner(): return lax.ppermute(array, AXES, pairs)  12.6 us
    all_to_all x2, starting transfers between devices, exchange(): lax.all_to_all(array, AXES, 0, 0, axis_index_groups=line_groups(along_rin...  12.1 us
    all_to_all x2, waiting for transfers between devices, exchange(): lax.all_to_all(array, AXES, 0, 0, axis_index_groups=line_groups(along_rin...  7.41 us
  transfers between devices with their start and end apart: 16, of which 9 were waited for; matrix products, arithmetic and copies ran while one was open for 0% of the time, Pallas kernels for 2%

profile of v1, /device:TPU:1, one launch (start us, length us, event | category | flops | bytes accessed | tf_op | source)
XLA Modules:
  0.0 147.1 jit_solution(14031834482336365025)
XLA Ops:
  0.7 0.9 fusion.5
  1.6 23.5 %all_to_all.15 = bf16[8,32,1152]{2,1,0:T(8,128)(2,1)S(1)} all-to-all(bf16[8,32,1152]{2,1,0:T(8,128)(2,1)S(1)} %broadcast_in_dim.2), channel_id=1, replica_groups={{0,8,16,24,32,40,48,56},{64,72,80,88,96,104,112,120},{128,136,144,152,1..., dimensions={0} | all-to-all | bytes 1179648 | tf_op jit(solution)/shard_map/all_to_all | solution.py:62
  25.1 5.9 %collective-permute-start.5 = (bf16[256,1152]{1,0:T(8,128)(2,1)S(1)}, bf16[256,1152]{1,0:T(8,128)(2,1)S(1)}, u32[]{:S(2)}, u32[]{:S(2)}) collective-permute-start(bf16[256,1152]{1,0:T(8,128)(2,1)S(1)} %bitcast.7), channel_id=1, source_target_pairs={{0,384},{1,49},{2,386},{3,51},{4,388},{5,53},{6,390},{7,55},{8,392... | collective-permute-start | bytes 1769480 | tf_op jit(solution)/shard_map/ppermute | solution.py:58
  31.0 1.9 %collective-permute-start.1 = (bf16[256,1152]{1,0:T(8,128)(2,1)S(1)}, bf16[256,1152]{1,0:T(8,128)(2,1)S(1)}, u32[]{:S(2)}, u32[]{:S(2)}) collective-permute-start(bf16[256,1152]{1,0:T(8,128)(2,1)S(1)} %bitcast.8), channel_id=1, source_target_pairs={{0,128},{1,17},{2,130},{3,19},{4,132},{5,21},{6,134},{7,23},{8,136... | collective-permute-start | bytes 1769480 | tf_op jit(solution)/shard_map/ppermute | solution.py:58
  33.0 4.7 %collective-permute-start.4 = (bf16[256,1152]{1,0:T(8,128)(2,1)S(1)}, bf16[256,1152]{1,0:T(8,128)(2,1)S(1)}, u32[]{:S(2)}, u32[]{:S(2)}) collective-permute-start(bf16[256,1152]{1,0:T(8,128)(2,1)S(1)} %bitcast.9), channel_id=1, source_target_pairs={{0,448},{1,57},{2,450},{3,59},{4,452},{5,61},{6,454},{7,63},{8,456... | collective-permute-start | bytes 1769480 | tf_op jit(solution)/shard_map/ppermute | solution.py:58
  37.6 1.9 %collective-permute-start = (bf16[256,1152]{1,0:T(8,128)(2,1)S(1)}, bf16[256,1152]{1,0:T(8,128)(2,1)S(1)}, u32[]{:S(2)}, u32[]{:S(2)}) collective-permute-start(bf16[256,1152]{1,0:T(8,128)(2,1)S(1)} %bitcast.10), channel_id=1, source_target_pairs={{0,64},{1,9},{2,66},{3,11},{4,68},{5,13},{6,70},{7,15},{8,72},{9,1... | collective-permute-start | bytes 1769480 | tf_op jit(solution)/shard_map/ppermute | solution.py:58
  39.6 4.6 %collective-permute-done.5.m2 = bf16[256,1152]{1,0:T(8,128)(2,1)S(1)} collective-permute-done((bf16[256,1152]{1,0:T(8,128)(2,1)S(1)}, bf16[256,1152]{1,0:T(8,128)(2,1)S(1)}, u32[]{:S(2)}, u32[]{:S(2)}) %collective-permute-start.5) | collective-permute-done | bytes 589856 | tf_op jit(solution)/shard_map/ppermute | solution.py:58
  44.1 4.4 %collective-permute-start.6 = (bf16[256,1152]{1,0:T(8,128)(2,1)S(1)}, bf16[256,1152]{1,0:T(8,128)(2,1)S(1)}, u32[]{:S(2)}, u32[]{:S(2)}) collective-permute-start(bf16[256,1152]{1,0:T(8,128)(2,1)S(1)} %collective-permute-done.5.m2), channel_id=1, source_target_pairs={{0,448},{1,57},{2,450},{3,59},{4,452},{5,61},{6,454},{7,63},{8,456... | collective-permute-start | bytes 1769480 | tf_op jit(solution)/shard_map/ppermute | solution.py:58
  48.6 4.1 %collective-permute-start.2 = (bf16[256,1152]{1,0:T(8,128)(2,1)S(1)}, bf16[256,1152]{1,0:T(8,128)(2,1)S(1)}, u32[]{:S(2)}, u32[]{:S(2)}) collective-permute-start(bf16[256,1152]{1,0:T(8,128)(2,1)S(1)} %collective-permute-done.1.p2), channel_id=1, source_target_pairs={{0,64},{1,9},{2,66},{3,11},{4,68},{5,13},{6,70},{7,15},{8,72},{9,1... | collective-permute-start | bytes 1769480 | tf_op jit(solution)/shard_map/ppermute | solution.py:58
  52.7 3.0 %collective-permute-start.7 = (bf16[128,1152]{1,0:T(8,128)(2,1)S(1)}, bf16[128,1152]{1,0:T(8,128)(2,1)S(1)}, u32[]{:S(2)}, u32[]{:S(2)}) collective-permute-start(bf16[128,1152]{1,0:T(8,128)(2,1)S(1)} %slice.13), channel_id=1, source_target_pairs={{0,384},{1,49},{2,386},{3,51},{4,388},{5,53},{6,390},{7,55},{8,392... | collective-permute-start | bytes 884744 | tf_op jit(solution)/shard_map/ppermute | solution.py:58
  55.7 3.2 %collective-permute-start.3 = (bf16[128,1152]{1,0:T(8,128)(2,1)S(1)}, bf16[128,1152]{1,0:T(8,128)(2,1)S(1)}, u32[]{:S(2)}, u32[]{:S(2)}) collective-permute-start(bf16[128,1152]{1,0:T(8,128)(2,1)S(1)} %slice.12), channel_id=1, source_target_pairs={{0,128},{1,17},{2,130},{3,19},{4,132},{5,21},{6,134},{7,23},{8,136... | collective-permute-start | bytes 884744 | tf_op jit(solution)/shard_map/ppermute | solution.py:58
  59.0 5.3 %collective-permute-done.7.m4 = bf16[128,1152]{1,0:T(8,128)(2,1)S(1)} collective-permute-done((bf16[128,1152]{1,0:T(8,128)(2,1)S(1)}, bf16[128,1152]{1,0:T(8,128)(2,1)S(1)}, u32[]{:S(2)}, u32[]{:S(2)}) %collective-permute-start.7) | collective-permute-done | bytes 294944 | tf_op jit(solution)/shard_map/ppermute | solution.py:58
  64.3 2.9 %collective-permute-done.3.p4 = bf16[128,1152]{1,0:T(8,128)(2,1)S(1)} collective-permute-done((bf16[128,1152]{1,0:T(8,128)(2,1)S(1)}, bf16[128,1152]{1,0:T(8,128)(2,1)S(1)}, u32[]{:S(2)}, u32[]{:S(2)}) %collective-permute-start.3) | collective-permute-done | bytes 294944 | tf_op jit(solution)/shard_map/ppermute | solution.py:58
  67.2 4.8 %shard_map.77 = (bf16[192,2048]{1,0:T(8,128)(2,1)S(1)}, bf16[192,2048]{1,0:T(8,128)(2,1)S(1)}, bf16[48,2048]{1,0:T(8,128)(2,1)S(1)}, bf16[384,384]{1,0:T(8,128)(2,1)S(1)}) custom-call(bf16[384,2048]{1,0:T(8,128)(2,1)S(1)} %copy-done.1, f32[1,2048]{1,0:T(1,128)S(1)} %bitcast.12, bf16[384,2048]{1,0:T(8,128)(2,1)S(1)} %copy-done, ...), custom_call_target="tpu_custom_call" | custom-call | tf_op jit(solution)/shard_map/pallas_call | solution.py:160
  72.0 2.8 %shard_map.84 = bf16[2048,384]{1,0:T(8,128)(2,1)} custom-call(bf16[384,2048]{1,0:T(8,128)(2,1)S(1)} %copy-done, bf16[384,384]{1,0:T(8,128)(2,1)S(1)} %get-tuple-element.17.hidden_ref), custom_call_target="tpu_custom_call" | custom-call | tf_op jit(solution)/shard_map/pallas_call | solution.py:179
  74.8 5.2 %all-to-all-start.1 = ((bf16[8,256,384]{2,1,0:T(8,128)(2,1)}), bf16[8,256,384]{2,1,0:T(8,128)(2,1)S(1)}, u32[]{:S(2)}, u32[]{:S(2)}) async-start(bf16[8,256,384]{2,1,0:T(8,128)(2,1)} %bitcast.3), calls=%async_computation.1 | async-start | bytes 3145728 | tf_op jit(solution)/shard_map/all_to_all | solution.py:62
  79.9 8.4 %collective-permute-start.8 = (bf16[192,2048]{1,0:T(8,128)(2,1)S(1)}, bf16[192,2048]{1,0:T(8,128)(2,1)S(1)}, u32[]{:S(2)}, u32[]{:S(2)}) collective-permute-start(bf16[192,2048]{1,0:T(8,128)(2,1)S(1)} %get-tuple-element.12), channel_id=1, source_target_pairs={{0,1},{1,0},{2,3},{3,2},{4,5},{5,4},{6,7},{7,6},{8,9},{9,8},{10,11... | collective-permute-start | bytes 2359304 | tf_op jit(solution)/shard_map/ppermute | solution.py:265
  88.4 1.9 %collective-permute-done.8.other_ref = bf16[192,2048]{1,0:T(8,128)(2,1)S(1)} collective-permute-done((bf16[192,2048]{1,0:T(8,128)(2,1)S(1)}, bf16[192,2048]{1,0:T(8,128)(2,1)S(1)}, u32[]{:S(2)}, u32[]{:S(2)}) %collective-permute-start.8) | collective-permute-done | bytes 786464 | tf_op jit(solution)/shard_map/ppermute | solution.py:265
  90.4 4.4 %collective-permute-start.9 = (bf16[96,2048]{1,0:T(8,128)(2,1)S(1)}, bf16[96,2048]{1,0:T(8,128)(2,1)S(1)}, u32[]{:S(2)}, u32[]{:S(2)}) collective-permute-start(bf16[96,2048]{1,0:T(8,128)(2,1)S(1)} %get-tuple-element.14), channel_id=1, source_target_pairs={{0,2},{1,7},{2,0},{3,5},{4,6},{5,3},{6,4},{7,1},{8,10},{9,15},{10,... | collective-permute-start | bytes 1179656 | tf_op jit(solution)/shard_map/ppermute | solution.py:261
  94.8 5.6 %collective-permute-done.9.got_ref = bf16[96,2048]{1,0:T(8,128)(2,1)S(1)} collective-permute-done((bf16[96,2048]{1,0:T(8,128)(2,1)S(1)}, bf16[96,2048]{1,0:T(8,128)(2,1)S(1)}, u32[]{:S(2)}, u32[]{:S(2)}) %collective-permute-start.9) | collective-permute-done | bytes 393248 | tf_op jit(solution)/shard_map/ppermute | solution.py:261
  100.5 1.9 %collective-permute-start.10 = (bf16[48,2048]{1,0:T(8,128)(2,1)S(1)}, bf16[48,2048]{1,0:T(8,128)(2,1)S(1)}, u32[]{:S(2)}, u32[]{:S(2)}) collective-permute-start(bf16[48,2048]{1,0:T(8,128)(2,1)S(1)} %get-tuple-element.16), channel_id=1, source_target_pairs={{0,6},{1,3},{2,4},{3,1},{4,2},{5,7},{6,0},{7,5},{8,14},{9,11},{10,... | collective-permute-start | bytes 589832 | tf_op jit(solution)/shard_map/ppermute | solution.py:261
  102.5 4.8 %collective-permute-done.10.got_ref = bf16[48,2048]{1,0:T(8,128)(2,1)S(1)} collective-permute-done((bf16[48,2048]{1,0:T(8,128)(2,1)S(1)}, bf16[48,2048]{1,0:T(8,128)(2,1)S(1)}, u32[]{:S(2)}, u32[]{:S(2)}) %collective-permute-start.10) | collective-permute-done | bytes 196640 | tf_op jit(solution)/shard_map/ppermute | solution.py:261
  107.5 1.9 %collective-permute-start.11 = (bf16[48,2048]{1,0:T(8,128)(2,1)S(1)}, bf16[48,2048]{1,0:T(8,128)(2,1)S(1)}, u32[]{:S(2)}, u32[]{:S(2)}) collective-permute-start(bf16[48,2048]{1,0:T(8,128)(2,1)S(1)} %shard_map.80.first_ref), channel_id=1, source_target_pairs={{0,6},{1,3},{2,4},{3,1},{4,2},{5,7},{6,0},{7,5},{8,14},{9,11},{10,... | collective-permute-start | bytes 589832 | tf_op jit(solution)/shard_map/ppermute | solution.py:261
  109.4 4.5 %collective-permute-done.11.second_ref = bf16[48,2048]{1,0:T(8,128)(2,1)S(1)} collective-permute-done((bf16[48,2048]{1,0:T(8,128)(2,1)S(1)}, bf16[48,2048]{1,0:T(8,128)(2,1)S(1)}, u32[]{:S(2)}, u32[]{:S(2)}) %collective-permute-start.11) | collective-permute-done | bytes 196640 | tf_op jit(solution)/shard_map/ppermute | solution.py:261
  113.9 4.4 %collective-permute-start.12 = (bf16[96,2048]{1,0:T(8,128)(2,1)S(1)}, bf16[96,2048]{1,0:T(8,128)(2,1)S(1)}, u32[]{:S(2)}, u32[]{:S(2)}) collective-permute-start(bf16[96,2048]{1,0:T(8,128)(2,1)S(1)} %shard_map.81.first_ref), channel_id=1, source_target_pairs={{0,2},{1,7},{2,0},{3,5},{4,6},{5,3},{6,4},{7,1},{8,10},{9,15},{10,... | collective-permute-start | bytes 1179656 | tf_op jit(solution)/shard_map/ppermute | solution.py:261
  118.3 5.3 %collective-permute-done.12.second_ref = bf16[96,2048]{1,0:T(8,128)(2,1)S(1)} collective-permute-done((bf16[96,2048]{1,0:T(8,128)(2,1)S(1)}, bf16[96,2048]{1,0:T(8,128)(2,1)S(1)}, u32[]{:S(2)}, u32[]{:S(2)}) %collective-permute-start.12) | collective-permute-done | bytes 393248 | tf_op jit(solution)/shard_map/ppermute | solution.py:261
  123.7 6.3 %collective-permute-start.13 = (bf16[192,2048]{1,0:T(8,128)(2,1)S(1)}, bf16[192,2048]{1,0:T(8,128)(2,1)S(1)}, u32[]{:S(2)}, u32[]{:S(2)}) collective-permute-start(bf16[192,2048]{1,0:T(8,128)(2,1)S(1)} %shard_map.82.mine_ref), channel_id=1, source_target_pairs={{0,1},{1,0},{2,3},{3,2},{4,5},{5,4},{6,7},{7,6},{8,9},{9,8},{10,11... | collective-permute-start | bytes 2359304 | tf_op jit(solution)/shard_map/ppermute | solution.py:265
  130.0 0.9 shard_map.85
  130.9 6.9 %all-to-all-start.2 = ((bf16[8,32,384]{2,1,0:T(8,128)(2,1)}), bf16[8,32,384]{2,1,0:T(8,128)(2,1)S(1)}, u32[]{:S(2)}, u32[]{:S(2)}) async-start(bf16[8,32,384]{2,1,0:T(8,128)(2,1)} %bitcast.4), calls=%async_computation.2 | async-start | bytes 393216 | tf_op jit(solution)/shard_map/all_to_all | solution.py:62
  137.8 1.2 shard_map.83
  139.1 7.4 %all-to-all-done.2.parts_ref = bf16[8,32,384]{2,1,0:T(8,128)(2,1)S(1)} async-done(((bf16[8,32,384]{2,1,0:T(8,128)(2,1)}), bf16[8,32,384]{2,1,0:T(8,128)(2,1)S(1)}, u32[]{:S(2)}, u32[]{:S(2)}) %all-to-all-start.2) | async-done | bytes 196640 | tf_op jit(solution)/shard_map/all_to_all | solution.py:62
  146.5 0.6 slice_bitcast_fusion
  (22 shorter events, 0.7 us)
Async XLA Ops:
  0.6 66.6 %copy-start = (bf16[384,2048]{1,0:T(8,128)(2,1)S(1)}, bf16[384,2048]{1,0:T(8,128)(2,1)}, u32[]{:S(2)}) copy-start(bf16[384,2048]{1,0:T(8,128)(2,1)} %cot_ref.3) | copy-start | bytes 4718596
  0.6 66.6 %copy-start.1 = (bf16[384,2048]{1,0:T(8,128)(2,1)S(1)}, bf16[384,2048]{1,0:T(8,128)(2,1)}, u32[]{:S(2)}) copy-start(bf16[384,2048]{1,0:T(8,128)(2,1)} %x_ref.1) | copy-start | bytes 4718596
  0.7 66.6 %copy-start.2 = (f32[2048]{0:T(1024)S(1)}, f32[2048]{0:T(1024)}, u32[]{:S(2)}) copy-start(f32[2048]{0:T(1024)} %param.7) | copy-start | bytes 24580
  25.1 19.0 %collective-permute-start.5 = (bf16[256,1152]{1,0:T(8,128)(2,1)S(1)}, bf16[256,1152]{1,0:T(8,128)(2,1)S(1)}, u32[]{:S(2)}, u32[]{:S(2)}) collective-permute-start(bf16[256,1152]{1,0:T(8,128)(2,1)S(1)} %bitcast.7), channel_id=1, source_target_pairs={{0,384},{1,49},{2,386},{3,51},{4,388},{5,53},{6,390},{7,55},{8,392... | collective-permute-start | bytes 1769480 | tf_op jit(solution)/shard_map/ppermute | solution.py:58
  31.0 17.5 %collective-permute-start.1 = (bf16[256,1152]{1,0:T(8,128)(2,1)S(1)}, bf16[256,1152]{1,0:T(8,128)(2,1)S(1)}, u32[]{:S(2)}, u32[]{:S(2)}) collective-permute-start(bf16[256,1152]{1,0:T(8,128)(2,1)S(1)} %bitcast.8), channel_id=1, source_target_pairs={{0,128},{1,17},{2,130},{3,19},{4,132},{5,21},{6,134},{7,23},{8,136... | collective-permute-start | bytes 1769480 | tf_op jit(solution)/shard_map/ppermute | solution.py:58
  33.0 22.8 %collective-permute-start.4 = (bf16[256,1152]{1,0:T(8,128)(2,1)S(1)}, bf16[256,1152]{1,0:T(8,128)(2,1)S(1)}, u32[]{:S(2)}, u32[]{:S(2)}) collective-permute-start(bf16[256,1152]{1,0:T(8,128)(2,1)S(1)} %bitcast.9), channel_id=1, source_target_pairs={{0,448},{1,57},{2,450},{3,59},{4,452},{5,61},{6,454},{7,63},{8,456... | collective-permute-start | bytes 1769480 | tf_op jit(solution)/shard_map/ppermute | solution.py:58
  37.6 21.3 %collective-permute-start = (bf16[256,1152]{1,0:T(8,128)(2,1)S(1)}, bf16[256,1152]{1,0:T(8,128)(2,1)S(1)}, u32[]{:S(2)}, u32[]{:S(2)}) collective-permute-start(bf16[256,1152]{1,0:T(8,128)(2,1)S(1)} %bitcast.10), channel_id=1, source_target_pairs={{0,64},{1,9},{2,66},{3,11},{4,68},{5,13},{6,70},{7,15},{8,72},{9,1... | collective-permute-start | bytes 1769480 | tf_op jit(solution)/shard_map/ppermute | solution.py:58
  44.1 23.0 %collective-permute-start.6 = (bf16[256,1152]{1,0:T(8,128)(2,1)S(1)}, bf16[256,1152]{1,0:T(8,128)(2,1)S(1)}, u32[]{:S(2)}, u32[]{:S(2)}) collective-permute-start(bf16[256,1152]{1,0:T(8,128)(2,1)S(1)} %collective-permute-done.5.m2), channel_id=1, source_target_pairs={{0,448},{1,57},{2,450},{3,59},{4,452},{5,61},{6,454},{7,63},{8,456... | collective-permute-start | bytes 1769480 | tf_op jit(solution)/shard_map/ppermute | solution.py:58
  48.6 18.6 %collective-permute-start.2 = (bf16[256,1152]{1,0:T(8,128)(2,1)S(1)}, bf16[256,1152]{1,0:T(8,128)(2,1)S(1)}, u32[]{:S(2)}, u32[]{:S(2)}) collective-permute-start(bf16[256,1152]{1,0:T(8,128)(2,1)S(1)} %collective-permute-done.1.p2), channel_id=1, source_target_pairs={{0,64},{1,9},{2,66},{3,11},{4,68},{5,13},{6,70},{7,15},{8,72},{9,1... | collective-permute-start | bytes 1769480 | tf_op jit(solution)/shard_map/ppermute | solution.py:58
  52.7 11.5 %collective-permute-start.7 = (bf16[128,1152]{1,0:T(8,128)(2,1)S(1)}, bf16[128,1152]{1,0:T(8,128)(2,1)S(1)}, u32[]{:S(2)}, u32[]{:S(2)}) collective-permute-start(bf16[128,1152]{1,0:T(8,128)(2,1)S(1)} %slice.13), channel_id=1, source_target_pairs={{0,384},{1,49},{2,386},{3,51},{4,388},{5,53},{6,390},{7,55},{8,392... | collective-permute-start | bytes 884744 | tf_op jit(solution)/shard_map/ppermute | solution.py:58
  55.7 11.4 %collective-permute-start.3 = (bf16[128,1152]{1,0:T(8,128)(2,1)S(1)}, bf16[128,1152]{1,0:T(8,128)(2,1)S(1)}, u32[]{:S(2)}, u32[]{:S(2)}) collective-permute-start(bf16[128,1152]{1,0:T(8,128)(2,1)S(1)} %slice.12), channel_id=1, source_target_pairs={{0,128},{1,17},{2,130},{3,19},{4,132},{5,21},{6,134},{7,23},{8,136... | collective-permute-start | bytes 884744 | tf_op jit(solution)/shard_map/ppermute | solution.py:58
  74.8 55.2 %all-to-all-start.1 = ((bf16[8,256,384]{2,1,0:T(8,128)(2,1)}), bf16[8,256,384]{2,1,0:T(8,128)(2,1)S(1)}, u32[]{:S(2)}, u32[]{:S(2)}) async-start(bf16[8,256,384]{2,1,0:T(8,128)(2,1)} %bitcast.3), calls=%async_computation.1 | async-start | bytes 3145728 | tf_op jit(solution)/shard_map/all_to_all | solution.py:62
  79.9 10.3 %collective-permute-start.8 = (bf16[192,2048]{1,0:T(8,128)(2,1)S(1)}, bf16[192,2048]{1,0:T(8,128)(2,1)S(1)}, u32[]{:S(2)}, u32[]{:S(2)}) collective-permute-start(bf16[192,2048]{1,0:T(8,128)(2,1)S(1)} %get-tuple-element.12), channel_id=1, source_target_pairs={{0,1},{1,0},{2,3},{3,2},{4,5},{5,4},{6,7},{7,6},{8,9},{9,8},{10,11... | collective-permute-start | bytes 2359304 | tf_op jit(solution)/shard_map/ppermute | solution.py:265
  90.4 10.0 %collective-permute-start.9 = (bf16[96,2048]{1,0:T(8,128)(2,1)S(1)}, bf16[96,2048]{1,0:T(8,128)(2,1)S(1)}, u32[]{:S(2)}, u32[]{:S(2)}) collective-permute-start(bf16[96,2048]{1,0:T(8,128)(2,1)S(1)} %get-tuple-element.14), channel_id=1, source_target_pairs={{0,2},{1,7},{2,0},{3,5},{4,6},{5,3},{6,4},{7,1},{8,10},{9,15},{10,... | collective-permute-start | bytes 1179656 | tf_op jit(solution)/shard_map/ppermute | solution.py:261
  100.5 6.7 %collective-permute-start.10 = (bf16[48,2048]{1,0:T(8,128)(2,1)S(1)}, bf16[48,2048]{1,0:T(8,128)(2,1)S(1)}, u32[]{:S(2)}, u32[]{:S(2)}) collective-permute-start(bf16[48,2048]{1,0:T(8,128)(2,1)S(1)} %get-tuple-element.16), channel_id=1, source_target_pairs={{0,6},{1,3},{2,4},{3,1},{4,2},{5,7},{6,0},{7,5},{8,14},{9,11},{10,... | collective-permute-start | bytes 589832 | tf_op jit(solution)/shard_map/ppermute | solution.py:261
  107.5 6.4 %collective-permute-start.11 = (bf16[48,2048]{1,0:T(8,128)(2,1)S(1)}, bf16[48,2048]{1,0:T(8,128)(2,1)S(1)}, u32[]{:S(2)}, u32[]{:S(2)}) collective-permute-start(bf16[48,2048]{1,0:T(8,128)(2,1)S(1)} %shard_map.80.first_ref), channel_id=1, source_target_pairs={{0,6},{1,3},{2,4},{3,1},{4,2},{5,7},{6,0},{7,5},{8,14},{9,11},{10,... | collective-permute-start | bytes 589832 | tf_op jit(solution)/shard_map/ppermute | solution.py:261
  113.9 9.7 %collective-permute-start.12 = (bf16[96,2048]{1,0:T(8,128)(2,1)S(1)}, bf16[96,2048]{1,0:T(8,128)(2,1)S(1)}, u32[]{:S(2)}, u32[]{:S(2)}) collective-permute-start(bf16[96,2048]{1,0:T(8,128)(2,1)S(1)} %shard_map.81.first_ref), channel_id=1, source_target_pairs={{0,2},{1,7},{2,0},{3,5},{4,6},{5,3},{6,4},{7,1},{8,10},{9,15},{10,... | collective-permute-start | bytes 1179656 | tf_op jit(solution)/shard_map/ppermute | solution.py:261
  123.7 14.1 %collective-permute-start.13 = (bf16[192,2048]{1,0:T(8,128)(2,1)S(1)}, bf16[192,2048]{1,0:T(8,128)(2,1)S(1)}, u32[]{:S(2)}, u32[]{:S(2)}) collective-permute-start(bf16[192,2048]{1,0:T(8,128)(2,1)S(1)} %shard_map.82.mine_ref), channel_id=1, source_target_pairs={{0,1},{1,0},{2,3},{3,2},{4,5},{5,4},{6,7},{7,6},{8,9},{9,8},{10,11... | collective-permute-start | bytes 2359304 | tf_op jit(solution)/shard_map/ppermute | solution.py:265
  130.9 15.6 %all-to-all-start.2 = ((bf16[8,32,384]{2,1,0:T(8,128)(2,1)}), bf16[8,32,384]{2,1,0:T(8,128)(2,1)S(1)}, u32[]{:S(2)}, u32[]{:S(2)}) async-start(bf16[8,32,384]{2,1,0:T(8,128)(2,1)} %bitcast.4), calls=%async_computation.2 | async-start | bytes 393216 | tf_op jit(solution)/shard_map/all_to_all | solution.py:62

commit v2 on v1

v2 whole, which is shorter than its diff:
```python
import jax
import jax.numpy as jnp
from jax import lax
from jax.experimental import pallas as pl
from jax.experimental.pallas import tpu as pltpu
from jax.sharding import Mesh
from jax.sharding import PartitionSpec as P


AXES = ("z", "y", "x", "c")
NZ, NY, NX, NC = 8, 8, 4, 2
FS = ("z", "y")
TP = ("x", "c")
EPSILON = 1e-06
HALF_STEP = 0.5
TOK = 384
D = 2048
HU = 352
HP = 384
DROWS = 32
HALF = TOK // NC
QUARTER = HALF // NX
VMEM_LIMIT = 28 * 2**20
SMALL_LIMIT = 6 * 2**20
DOWN_LIMIT = 16 * 2**20


def device_number(z, y, x, c):
    return ((z % NZ * NY + y % NY) * NX + x) * NC + c


def ring_pairs(step):
    return [
        (device_number(z, y, x, c), device_number(z + (1 - c) * step, y + c * step, x, c))
        for z in range(NZ)
        for y in range(NY)
        for x in range(NX)
        for c in range(NC)
    ]


def line_groups(along_ring):
    groups = []
    for x in range(NX):
        for c in range(NC):
            vary_z = (c == 0) == along_ring
            for fixed in range(8):
                groups.append(
                    [
                        device_number(k, fixed, x, c) if vary_z else device_number(fixed, k, x, c)
                        for k in range(8)
                    ]
                )
    return groups


def ring(array, step):
    return lax.ppermute(array, AXES, ring_pairs(step))


def exchange(array, along_ring):
    return lax.all_to_all(
        array, AXES, 0, 0, axis_index_groups=line_groups(along_ring), tiled=True
    )


def dot(left, right, dims):
    return lax.dot_general(left, right, (dims, ((), ())), preferred_element_type=jnp.float32)


def half_rows(core):
    return pl.ds(pl.multiple_of(core * HALF, 64), HALF)


def normalize_kernel(x_ref, gain_ref, xn_ref, half_ref):
    half_ref[...] = x_ref[half_rows(lax.axis_index("c")), :]
    gain = gain_ref[...]
    for k in range(6):
        rows = pl.ds(k * 64, 64)
        value = x_ref[rows, :].astype(jnp.float32)
        inverse = lax.rsqrt(jnp.mean(value * value, axis=-1, keepdims=True) + EPSILON)
        xn_ref[rows, :] = (value * inverse * gain).astype(jnp.bfloat16)


def compute_kernel(
    norm_ref, cot_ref, b0, p1, p2, p3, p4, m1, m2, m3, m4,
    keep_ref, send_ref, hidden_ref, w_ref, part_ref,
):
    c = lax.axis_index("c")
    r = jnp.where(c == 0, lax.axis_index("z"), lax.axis_index("y"))

    def row_of(q, o):
        q = lax.rem(q + 16, 8)
        return pl.multiple_of(jnp.where(c == 0, q * 256 + o * 32, o * 256 + q * 32), 32)

    def put(q, block, first, last):
        for o in range(first, last):
            w_ref[pl.ds(row_of(q, o), DROWS), :] = block[pl.ds((o - first) * DROWS, DROWS), :]

    put(r, b0, 0, 8)
    for k, block in enumerate((p1, p2, p3)):
        put(r - k - 1, block, 0, 8)
    for k, block in enumerate((m1, m2, m3)):
        put(r + k + 1, block, 0, 8)
    put(r + 4, p4, 0, 4)
    put(r + 4, m4, 4, 8)

    gate_up = dot(norm_ref[...], w_ref[:, : 2 * HP], ((1,), (0,)))
    gate = gate_up[:, :HP]
    up = gate_up[:, HP:]
    d_hidden = HALF_STEP * dot(cot_ref[...], w_ref[:, 2 * HP :], ((1,), (0,)))
    sig = jax.nn.sigmoid(gate)
    hidden = (gate * sig * up).astype(jnp.bfloat16)
    d_gate = (d_hidden * up * sig * (1.0 + gate * (1.0 - sig))).astype(jnp.bfloat16)
    d_up = (d_hidden * gate * sig).astype(jnp.bfloat16)
    both = jnp.concatenate([d_gate, d_up], axis=1)
    part_ref[...] = dot(both, w_ref[:, : 2 * HP], ((1,), (1,))).astype(jnp.bfloat16)
    hidden_ref[...] = hidden
    keep_ref[...] = part_ref[half_rows(c), :]
    send_ref[...] = part_ref[half_rows(1 - c), :]


def down_kernel(cot_ref, hidden_ref, down_ref, dt_ref, ordered_ref, sems):
    c = lax.axis_index("c")
    dt = dot(cot_ref[...], hidden_ref[...], ((0,), (0,)))
    dt_ref[...] = (HALF_STEP * dt).astype(jnp.bfloat16)
    copies = []
    for q in range(8):
        for o in range(8):
            row = jnp.where(c == 0, q * 256 + o * 32, o * 256 + q * 32)
            rows = pl.ds(pl.multiple_of(row, 32), DROWS)
            ordered_ref[pl.ds(q * 256 + o * 32, DROWS), :] = dt_ref[rows, :]
        block = pl.ds(q * 256, 256)
        copies.append(
            pltpu.make_async_copy(ordered_ref.at[block, :], down_ref.at[block, :], sems.at[q])
        )
        copies[-1].start()
    for copy in copies:
        copy.wait()


def vmem_specs(count):
    return [pl.BlockSpec(memory_space=pltpu.VMEM)] * count


def small_call(kernel, out_shape, *operands):
    count = len(out_shape)
    return pl.pallas_call(
        kernel,
        out_shape=tuple(out_shape),
        in_specs=vmem_specs(len(operands)),
        out_specs=tuple(vmem_specs(count)),
        compiler_params=pltpu.CompilerParams(vmem_limit_bytes=SMALL_LIMIT),
    )(*operands)


def compute(normed, cotangent, blocks):
    half = jax.ShapeDtypeStruct((HALF, D), jnp.bfloat16)
    return pl.pallas_call(
        compute_kernel,
        out_shape=(
            half,
            half,
            jax.ShapeDtypeStruct((TOK, HP), jnp.bfloat16),
        ),
        in_specs=vmem_specs(2 + len(blocks)),
        out_specs=tuple(vmem_specs(3)),
        scratch_shapes=[
            pltpu.VMEM((D, 3 * HP), jnp.bfloat16),
            pltpu.VMEM((TOK, D), jnp.bfloat16),
        ],
        compiler_params=pltpu.CompilerParams(vmem_limit_bytes=VMEM_LIMIT),
    )(normed, cotangent, *blocks)


def down_product(cotangent, hidden):
    return pl.pallas_call(
        down_kernel,
        out_shape=jax.ShapeDtypeStruct((D, HP), jnp.bfloat16),
        in_specs=vmem_specs(2),
        out_specs=pl.BlockSpec(memory_space=pltpu.HBM),
        scratch_shapes=[
            pltpu.VMEM((D, HP), jnp.bfloat16),
            pltpu.VMEM((D, HP), jnp.bfloat16),
            pltpu.SemaphoreType.DMA((8,)),
        ],
        compiler_params=pltpu.CompilerParams(vmem_limit_bytes=DOWN_LIMIT),
    )(cotangent, hidden)


def pair_kernel(left_ref, right_ref, out_ref):
    total = left_ref[...].astype(jnp.float32) + right_ref[...].astype(jnp.float32)
    out_ref[...] = total.astype(jnp.bfloat16)


def final_kernel(x_ref, gain_ref, left_ref, right_ref, out_ref):
    gain = gain_ref[...]
    for k in range(4):
        rows = pl.ds(k * QUARTER, QUARTER)
        value = x_ref[rows, :].astype(jnp.float32)
        inverse = lax.rsqrt(jnp.mean(value * value, axis=-1, keepdims=True) + EPSILON)
        normalized = value * inverse
        total = left_ref[rows, :].astype(jnp.float32) + right_ref[rows, :].astype(jnp.float32)
        scaled = total * gain
        mean = jnp.mean(scaled * normalized, axis=-1, keepdims=True)
        out_ref[rows, :] = (inverse * (scaled - normalized * mean)).astype(jnp.bfloat16)


def place_kernel(mine_ref, away_ref, out_ref, sems):
    c = lax.axis_index("c")
    copies = [
        pltpu.make_async_copy(ref, out_ref.at[half_rows(core), :], sems.at[k])
        for k, (core, ref) in enumerate(((c, mine_ref), (1 - c, away_ref)))
    ]
    for copy in copies:
        copy.start()
    for copy in copies:
        copy.wait()


def place(mine, away):
    return pl.pallas_call(
        place_kernel,
        out_shape=jax.ShapeDtypeStruct((TOK, D), jnp.bfloat16),
        in_specs=vmem_specs(2),
        out_specs=pl.BlockSpec(memory_space=pltpu.HBM),
        scratch_shapes=[pltpu.SemaphoreType.DMA((2,))],
        compiler_params=pltpu.CompilerParams(vmem_limit_bytes=SMALL_LIMIT),
    )(mine, away)


def sum_kernel(parts_ref, out_ref):
    total = parts_ref[0].astype(jnp.float32)
    for k in range(1, 8):
        total = total + parts_ref[k].astype(jnp.float32)
    out_ref[...] = total.astype(out_ref.dtype)


def with_partner(array, first):
    pairs = [
        (device_number(z, y, x, c), device_number(z, y, x ^ (1 if (c == 0) == first else 3), c))
        for z in range(NZ)
        for y in range(NY)
        for x in range(NX)
        for c in range(NC)
    ]
    return lax.ppermute(array, AXES, pairs)


def with_core(array):
    return lax.ppermute(array, "c", [(0, 1), (1, 0)])


def shards(inputs, gain, w_gate, w_up, w_down, cotangent):
    pad = ((0, 0), (0, HP - HU))
    packed = jnp.concatenate([jnp.pad(w, pad) for w in (w_gate, w_up, w_down.T)], axis=1)
    block = exchange(jnp.broadcast_to(packed[None], (8, DROWS, 3 * HP)), False)
    b0 = block.reshape(256, 3 * HP)
    p2 = ring(b0, 2)
    m2 = ring(b0, -2)
    p1 = ring(b0, 1)
    m1 = ring(b0, -1)
    p3 = ring(p2, 1)
    m3 = ring(m2, -1)
    p4 = ring(p2[:128], 2)
    m4 = ring(m2[128:], -2)

    row = gain.reshape(1, D)
    half = jax.ShapeDtypeStruct((HALF, D), jnp.bfloat16)
    normed, x_half = small_call(
        normalize_kernel, [jax.ShapeDtypeStruct((TOK, D), jnp.bfloat16), half], inputs, row
    )
    keep, send, hidden = compute(normed, cotangent, (b0, p1, p2, p3, p4, m1, m2, m3, m4))
    other = with_core(send)
    down = down_product(cotangent, hidden)
    arrived = exchange(down.reshape(8, 256, HP), True)
    (line,) = small_call(sum_kernel, [jax.ShapeDtypeStruct((256, HP), jnp.bfloat16)], arrived)
    arrived = exchange(line.reshape(8, DROWS, HP), False)
    (total,) = small_call(sum_kernel, [jax.ShapeDtypeStruct((DROWS, HP), jnp.float32)], arrived)
    grad_down = total[:, :HU].T

    (chip,) = small_call(pair_kernel, [half], keep, other)
    got = with_partner(chip, True)
    (two,) = small_call(pair_kernel, [half], chip, got)
    got = with_partner(two, False)
    (mine,) = small_call(final_kernel, [half], x_half, row, two, got)
    away = with_core(mine)
    return place(mine, away), grad_down


def solution(mesh):
    split = Mesh(mesh.devices.reshape(NZ, NY, NX, NC), AXES)
    in_specs = (P(FS, None), P(), P(FS, TP), P(FS, TP), P(TP, FS), P(FS, None))
    out_specs = (P(FS, None), P(TP, FS))
    return jax.shard_map(
        shards, mesh=split, in_specs=in_specs, out_specs=out_specs, check_vma=False
    )
```

time: 148 us -> 139 us (0.939)
  starting transfers between devices: 68.5 us -> 51.7 us
  blocking collectives: 23.5 us -> 38.9 us
  waiting for transfers between devices: 42.3 us -> 35 us
    all_to_all x1 -> x2, blocking collectives: 23.5 us -> 38.9 us  [exchange(): lax.all_to_all(array, AXES, 0, 0, axis_index_groups=line_groups(along_rin...]
    all_to_all x2 -> x1, starting transfers between devices: 12.1 us -> 4.36 us  [exchange(): lax.all_to_all(array, AXES, 0, 0, axis_index_groups=line_groups(along_rin...]
    all_to_all x2 -> x1, waiting for transfers between devices: 7.41 us -> 0.01 us  [exchange(): lax.all_to_all(array, AXES, 0, 0, axis_index_groups=line_groups(along_rin...]
    ppermute x4 -> x2, starting transfers between devices: 12.6 us -> 6.59 us  [with_partner(): return lax.ppermute(array, AXES, pairs)]
    ppermute x2, starting transfers between devices: 14.7 us -> 11.1 us  [with_core(): return lax.ppermute(array, 'c', [(0, 1), (1, 0)])]
    ppermute x4 -> x2, waiting for transfers between devices: 20.2 us -> 20.4 us  [with_partner(): return lax.ppermute(array, AXES, pairs)]
  transfers between devices with their start and end apart: 16 -> 13, of which waited for: 9 -> 7; matrix products, arithmetic and copies ran while one was open for 0% -> 0% of each run, Pallas kernels for 2% -> 1%
where the time goes in v2:
time: 139 us; the launch traced here: 138 us
  starting transfers between devices  51.7 us (37%)
  blocking collectives  38.9 us (28%)
  waiting for transfers between devices  35 us (25%)
  Pallas kernels  10.4 us (7%)
    all_to_all x2, blocking collectives, exchange(): lax.all_to_all(array, AXES, 0, 0, axis_index_groups=line_groups(along_rin...  38.9 us
    ppermute x8, starting transfers between devices, ring(): return lax.ppermute(array, AXES, ring_pairs(step))  29.7 us
    ppermute x2, waiting for transfers between devices, with_partner(): return lax.ppermute(array, AXES, pairs)  20.4 us
    ppermute x8, waiting for transfers between devices, ring(): return lax.ppermute(array, AXES, ring_pairs(step))  12.5 us
    ppermute x2, starting transfers between devices, with_core(): return lax.ppermute(array, 'c', [(0, 1), (1, 0)])  11.1 us
    ppermute x2, starting transfers between devices, with_partner(): return lax.ppermute(array, AXES, pairs)  6.59 us
    pallas_call x1, Pallas kernels, compute(): pl.pallas_call(compute_kernel, out_shape=(half, half, jax.ShapeDtypeStruc...  4.76 us
    all_to_all x1, starting transfers between devices, exchange(): lax.all_to_all(array, AXES, 0, 0, axis_index_groups=line_groups(along_rin...  4.36 us
  transfers between devices with their start and end apart: 13, of which 7 were waited for; matrix products, arithmetic and copies ran while one was open for 0% of the time, Pallas kernels for 1%

profile of v2, /device:TPU:1, one launch (start us, length us, event | category | flops | bytes accessed | tf_op | source)
XLA Modules:
  0.0 138.4 jit_solution(18227064763148388398)
XLA Ops:
  0.7 0.9 fusion.5
  1.6 23.5 %all_to_all.15 = bf16[8,32,1152]{2,1,0:T(8,128)(2,1)S(1)} all-to-all(bf16[8,32,1152]{2,1,0:T(8,128)(2,1)S(1)} %broadcast_in_dim.2), channel_id=1, replica_groups={{0,8,16,24,32,40,48,56},{64,72,80,88,96,104,112,120},{128,136,144,152,1..., dimensions={0} | all-to-all | bytes 1179648 | tf_op jit(solution)/shard_map/all_to_all | solution.py:62
  25.1 4.3 %collective-permute-start.1 = (bf16[256,1152]{1,0:T(8,128)(2,1)S(1)}, bf16[256,1152]{1,0:T(8,128)(2,1)S(1)}, u32[]{:S(2)}, u32[]{:S(2)}) collective-permute-start(bf16[256,1152]{1,0:T(8,128)(2,1)S(1)} %bitcast.7), channel_id=1, source_target_pairs={{0,128},{1,17},{2,130},{3,19},{4,132},{5,21},{6,134},{7,23},{8,136... | collective-permute-start | bytes 1769480 | tf_op jit(solution)/shard_map/ppermute | solution.py:58
  29.4 3.6 %collective-permute-start.5 = (bf16[256,1152]{1,0:T(8,128)(2,1)S(1)}, bf16[256,1152]{1,0:T(8,128)(2,1)S(1)}, u32[]{:S(2)}, u32[]{:S(2)}) collective-permute-start(bf16[256,1152]{1,0:T(8,128)(2,1)S(1)} %bitcast.8), channel_id=1, source_target_pairs={{0,384},{1,49},{2,386},{3,51},{4,388},{5,53},{6,390},{7,55},{8,392... | collective-permute-start | bytes 1769480 | tf_op jit(solution)/shard_map/ppermute | solution.py:58
  33.0 2.8 %collective-permute-start = (bf16[256,1152]{1,0:T(8,128)(2,1)S(1)}, bf16[256,1152]{1,0:T(8,128)(2,1)S(1)}, u32[]{:S(2)}, u32[]{:S(2)}) collective-permute-start(bf16[256,1152]{1,0:T(8,128)(2,1)S(1)} %bitcast.9), channel_id=1, source_target_pairs={{0,64},{1,9},{2,66},{3,11},{4,68},{5,13},{6,70},{7,15},{8,72},{9,1... | collective-permute-start | bytes 1769480 | tf_op jit(solution)/shard_map/ppermute | solution.py:58
  35.8 3.7 %collective-permute-start.4 = (bf16[256,1152]{1,0:T(8,128)(2,1)S(1)}, bf16[256,1152]{1,0:T(8,128)(2,1)S(1)}, u32[]{:S(2)}, u32[]{:S(2)}) collective-permute-start(bf16[256,1152]{1,0:T(8,128)(2,1)S(1)} %bitcast.10), channel_id=1, source_target_pairs={{0,448},{1,57},{2,450},{3,59},{4,452},{5,61},{6,454},{7,63},{8,456... | collective-permute-start | bytes 1769480 | tf_op jit(solution)/shard_map/ppermute | solution.py:58
  39.5 2.1 %collective-permute-done.1.p2 = bf16[256,1152]{1,0:T(8,128)(2,1)S(1)} collective-permute-done((bf16[256,1152]{1,0:T(8,128)(2,1)S(1)}, bf16[256,1152]{1,0:T(8,128)(2,1)S(1)}, u32[]{:S(2)}, u32[]{:S(2)}) %collective-permute-start.1) | collective-permute-done | bytes 589856 | tf_op jit(solution)/shard_map/ppermute | solution.py:58
  41.6 5.9 %collective-permute-start.2 = (bf16[256,1152]{1,0:T(8,128)(2,1)S(1)}, bf16[256,1152]{1,0:T(8,128)(2,1)S(1)}, u32[]{:S(2)}, u32[]{:S(2)}) collective-permute-start(bf16[256,1152]{1,0:T(8,128)(2,1)S(1)} %collective-permute-done.1.p2), channel_id=1, source_target_pairs={{0,64},{1,9},{2,66},{3,11},{4,68},{5,13},{6,70},{7,15},{8,72},{9,1... | collective-permute-start | bytes 1769480 | tf_op jit(solution)/shard_map/ppermute | solution.py:58
  47.6 1.2 collective-permute-done.5.m2
  48.8 1.9 %collective-permute-start.6 = (bf16[256,1152]{1,0:T(8,128)(2,1)S(1)}, bf16[256,1152]{1,0:T(8,128)(2,1)S(1)}, u32[]{:S(2)}, u32[]{:S(2)}) collective-permute-start(bf16[256,1152]{1,0:T(8,128)(2,1)S(1)} %collective-permute-done.5.m2), channel_id=1, source_target_pairs={{0,448},{1,57},{2,450},{3,59},{4,452},{5,61},{6,454},{7,63},{8,456... | collective-permute-start | bytes 1769480 | tf_op jit(solution)/shard_map/ppermute | solution.py:58
  50.7 4.4 %collective-permute-start.3 = (bf16[128,1152]{1,0:T(8,128)(2,1)S(1)}, bf16[128,1152]{1,0:T(8,128)(2,1)S(1)}, u32[]{:S(2)}, u32[]{:S(2)}) collective-permute-start(bf16[128,1152]{1,0:T(8,128)(2,1)S(1)} %slice.12), channel_id=1, source_target_pairs={{0,128},{1,17},{2,130},{3,19},{4,132},{5,21},{6,134},{7,23},{8,136... | collective-permute-start | bytes 884744 | tf_op jit(solution)/shard_map/ppermute | solution.py:58
  55.2 3.0 %collective-permute-start.7 = (bf16[128,1152]{1,0:T(8,128)(2,1)S(1)}, bf16[128,1152]{1,0:T(8,128)(2,1)S(1)}, u32[]{:S(2)}, u32[]{:S(2)}) collective-permute-start(bf16[128,1152]{1,0:T(8,128)(2,1)S(1)} %slice.13), channel_id=1, source_target_pairs={{0,384},{1,49},{2,386},{3,51},{4,388},{5,53},{6,390},{7,55},{8,392... | collective-permute-start | bytes 884744 | tf_op jit(solution)/shard_map/ppermute | solution.py:58
  58.2 0.6 shard_map.77
  58.9 2.6 %collective-permute-done.3.p4 = bf16[128,1152]{1,0:T(8,128)(2,1)S(1)} collective-permute-done((bf16[128,1152]{1,0:T(8,128)(2,1)S(1)}, bf16[128,1152]{1,0:T(8,128)(2,1)S(1)}, u32[]{:S(2)}, u32[]{:S(2)}) %collective-permute-start.3) | collective-permute-done | bytes 294944 | tf_op jit(solution)/shard_map/ppermute | solution.py:58
  61.5 6.6 %collective-permute-done.7.m4 = bf16[128,1152]{1,0:T(8,128)(2,1)S(1)} collective-permute-done((bf16[128,1152]{1,0:T(8,128)(2,1)S(1)}, bf16[128,1152]{1,0:T(8,128)(2,1)S(1)}, u32[]{:S(2)}, u32[]{:S(2)}) %collective-permute-start.7) | collective-permute-done | bytes 294944 | tf_op jit(solution)/shard_map/ppermute | solution.py:58
  68.1 4.8 %shard_map.78 = (bf16[192,2048]{1,0:T(8,128)(2,1)S(1)}, bf16[192,2048]{1,0:T(8,128)(2,1)S(1)}, bf16[384,384]{1,0:T(8,128)(2,1)S(1)}) custom-call(bf16[384,2048]{1,0:T(8,128)(2,1)S(1)} %get-tuple-element.8.norm_ref, bf16[384,2048]{1,0:T(8,128)(2,1)S(1)} %copy-done, bf16[256,1152]{1,0:T(8,128)(2,1)S(1)} %bitcast.11, ...), custom_call_target="tpu_custom_call" | custom-call | tf_op jit(solution)/shard_map/pallas_call | solution.py:159
  72.8 2.4 %shard_map.83 = bf16[2048,384]{1,0:T(8,128)(2,1)} custom-call(bf16[384,2048]{1,0:T(8,128)(2,1)S(1)} %copy-done, bf16[384,384]{1,0:T(8,128)(2,1)S(1)} %get-tuple-element.11.hidden_ref), custom_call_target="tpu_custom_call" | custom-call | tf_op jit(solution)/shard_map/pallas_call | solution.py:177
  75.3 4.4 %all-to-all-start.1 = ((bf16[8,256,384]{2,1,0:T(8,128)(2,1)}), bf16[8,256,384]{2,1,0:T(8,128)(2,1)S(1)}, u32[]{:S(2)}, u32[]{:S(2)}) async-start(bf16[8,256,384]{2,1,0:T(8,128)(2,1)} %bitcast.3), calls=%async_computation.1 | async-start | bytes 3145728 | tf_op jit(solution)/shard_map/all_to_all | solution.py:62
  79.6 6.8 %collective-permute-start.8 = (bf16[192,2048]{1,0:T(8,128)(2,1)}, bf16[192,2048]{1,0:T(8,128)(2,1)S(1)}, u32[]{:S(2)}, u32[]{:S(2)}) collective-permute-start(bf16[192,2048]{1,0:T(8,128)(2,1)} %copy-done.3), channel_id=1, source_target_pairs={{0,1},{1,0},{2,3},{3,2},{4,5},{5,4},{6,7},{7,6},{8,9},{9,8},{10,11... | collective-permute-start | bytes 2359304 | tf_op jit(solution)/shard_map/ppermute | solution.py:251
  86.5 2.1 %collective-permute-done.8.right_ref = bf16[192,2048]{1,0:T(8,128)(2,1)S(1)} collective-permute-done((bf16[192,2048]{1,0:T(8,128)(2,1)}, bf16[192,2048]{1,0:T(8,128)(2,1)S(1)}, u32[]{:S(2)}, u32[]{:S(2)}) %collective-permute-start.8) | collective-permute-done | bytes 786464 | tf_op jit(solution)/shard_map/ppermute | solution.py:251
  88.6 0.2 shard_map.79.left_ref
  88.8 4.4 %collective-permute-start.9 = (bf16[192,2048]{1,0:T(8,128)(2,1)S(1)}, bf16[192,2048]{1,0:T(8,128)(2,1)S(1)}, u32[]{:S(2)}, u32[]{:S(2)}) collective-permute-start(bf16[192,2048]{1,0:T(8,128)(2,1)S(1)} %shard_map.79.left_ref), channel_id=1, source_target_pairs={{0,2},{1,7},{2,0},{3,5},{4,6},{5,3},{6,4},{7,1},{8,10},{9,15},{10,... | collective-permute-start | bytes 2359304 | tf_op jit(solution)/shard_map/ppermute | solution.py:247
  93.2 9.6 %collective-permute-done.9.right_ref = bf16[192,2048]{1,0:T(8,128)(2,1)S(1)} collective-permute-done((bf16[192,2048]{1,0:T(8,128)(2,1)S(1)}, bf16[192,2048]{1,0:T(8,128)(2,1)S(1)}, u32[]{:S(2)}, u32[]{:S(2)}) %collective-permute-start.9) | collective-permute-done | bytes 786464 | tf_op jit(solution)/shard_map/ppermute | solution.py:247
  102.7 0.2 shard_map.80.left_ref
  102.9 2.2 %collective-permute-start.10 = (bf16[192,2048]{1,0:T(8,128)(2,1)S(1)}, bf16[192,2048]{1,0:T(8,128)(2,1)S(1)}, u32[]{:S(2)}, u32[]{:S(2)}) collective-permute-start(bf16[192,2048]{1,0:T(8,128)(2,1)S(1)} %shard_map.80.left_ref), channel_id=1, source_target_pairs={{0,6},{1,3},{2,4},{3,1},{4,2},{5,7},{6,0},{7,5},{8,14},{9,11},{10,... | collective-permute-start | bytes 2359304 | tf_op jit(solution)/shard_map/ppermute | solution.py:247
  105.1 10.8 %collective-permute-done.10.right_ref = bf16[192,2048]{1,0:T(8,128)(2,1)S(1)} collective-permute-done((bf16[192,2048]{1,0:T(8,128)(2,1)S(1)}, bf16[192,2048]{1,0:T(8,128)(2,1)S(1)}, u32[]{:S(2)}, u32[]{:S(2)}) %collective-permute-start.10) | collective-permute-done | bytes 786464 | tf_op jit(solution)/shard_map/ppermute | solution.py:247
  115.9 0.8 shard_map.81.mine_ref
  116.7 4.3 %collective-permute-start.11 = (bf16[192,2048]{1,0:T(8,128)(2,1)S(1)}, bf16[192,2048]{1,0:T(8,128)(2,1)S(1)}, u32[]{:S(2)}, u32[]{:S(2)}) collective-permute-start(bf16[192,2048]{1,0:T(8,128)(2,1)S(1)} %shard_map.81.mine_ref), channel_id=1, source_target_pairs={{0,1},{1,0},{2,3},{3,2},{4,5},{5,4},{6,7},{7,6},{8,9},{9,8},{10,11... | collective-permute-start | bytes 2359304 | tf_op jit(solution)/shard_map/ppermute | solution.py:251
  121.0 0.2 shard_map.84
  121.2 15.4 %all_to_all.16.parts_ref = bf16[8,32,384]{2,1,0:T(8,128)(2,1)S(1)} all-to-all(bf16[8,32,384]{2,1,0:T(8,128)(2,1)S(1)} %bitcast.12), channel_id=1, replica_groups={{0,8,16,24,32,40,48,56},{64,72,80,88,96,104,112,120},{128,136,144,152,1..., dimensions={0} | all-to-all | bytes 393216 | tf_op jit(solution)/shard_map/all_to_all | solution.py:62
  136.6 0.6 slice_bitcast_fusion
  137.2 1.2 shard_map.82
  (18 shorter events, 0.2 us)
Async XLA Ops:
  0.6 57.6 %copy-start.1 = (bf16[384,2048]{1,0:T(8,128)(2,1)S(1)}, bf16[384,2048]{1,0:T(8,128)(2,1)}, u32[]{:S(2)}) copy-start(bf16[384,2048]{1,0:T(8,128)(2,1)} %x_ref.1) | copy-start | bytes 4718596
  0.6 57.6 %copy-start.2 = (f32[2048]{0:T(1024)S(1)}, f32[2048]{0:T(1024)}, u32[]{:S(2)}) copy-start(f32[2048]{0:T(1024)} %param.7) | copy-start | bytes 24580
  25.1 43.0 %copy-start = (bf16[384,2048]{1,0:T(8,128)(2,1)S(1)}, bf16[384,2048]{1,0:T(8,128)(2,1)}, u32[]{:S(2)}) copy-start(bf16[384,2048]{1,0:T(8,128)(2,1)} %cot_ref.3) | copy-start | bytes 4718596
  25.1 16.5 %collective-permute-start.1 = (bf16[256,1152]{1,0:T(8,128)(2,1)S(1)}, bf16[256,1152]{1,0:T(8,128)(2,1)S(1)}, u32[]{:S(2)}, u32[]{:S(2)}) collective-permute-start(bf16[256,1152]{1,0:T(8,128)(2,1)S(1)} %bitcast.7), channel_id=1, source_target_pairs={{0,128},{1,17},{2,130},{3,19},{4,132},{5,21},{6,134},{7,23},{8,136... | collective-permute-start | bytes 1769480 | tf_op jit(solution)/shard_map/ppermute | solution.py:58
  29.4 19.4 %collective-permute-start.5 = (bf16[256,1152]{1,0:T(8,128)(2,1)S(1)}, bf16[256,1152]{1,0:T(8,128)(2,1)S(1)}, u32[]{:S(2)}, u32[]{:S(2)}) collective-permute-start(bf16[256,1152]{1,0:T(8,128)(2,1)S(1)} %bitcast.8), channel_id=1, source_target_pairs={{0,384},{1,49},{2,386},{3,51},{4,388},{5,53},{6,390},{7,55},{8,392... | collective-permute-start | bytes 1769480 | tf_op jit(solution)/shard_map/ppermute | solution.py:58
  33.0 22.1 %collective-permute-start = (bf16[256,1152]{1,0:T(8,128)(2,1)S(1)}, bf16[256,1152]{1,0:T(8,128)(2,1)S(1)}, u32[]{:S(2)}, u32[]{:S(2)}) collective-permute-start(bf16[256,1152]{1,0:T(8,128)(2,1)S(1)} %bitcast.9), channel_id=1, source_target_pairs={{0,64},{1,9},{2,66},{3,11},{4,68},{5,13},{6,70},{7,15},{8,72},{9,1... | collective-permute-start | bytes 1769480 | tf_op jit(solution)/shard_map/ppermute | solution.py:58
  35.8 23.0 %collective-permute-start.4 = (bf16[256,1152]{1,0:T(8,128)(2,1)S(1)}, bf16[256,1152]{1,0:T(8,128)(2,1)S(1)}, u32[]{:S(2)}, u32[]{:S(2)}) collective-permute-start(bf16[256,1152]{1,0:T(8,128)(2,1)S(1)} %bitcast.10), channel_id=1, source_target_pairs={{0,448},{1,57},{2,450},{3,59},{4,452},{5,61},{6,454},{7,63},{8,456... | collective-permute-start | bytes 1769480 | tf_op jit(solution)/shard_map/ppermute | solution.py:58
  41.6 26.4 %collective-permute-start.2 = (bf16[256,1152]{1,0:T(8,128)(2,1)S(1)}, bf16[256,1152]{1,0:T(8,128)(2,1)S(1)}, u32[]{:S(2)}, u32[]{:S(2)}) collective-permute-start(bf16[256,1152]{1,0:T(8,128)(2,1)S(1)} %collective-permute-done.1.p2), channel_id=1, source_target_pairs={{0,64},{1,9},{2,66},{3,11},{4,68},{5,13},{6,70},{7,15},{8,72},{9,1... | collective-permute-start | bytes 1769480 | tf_op jit(solution)/shard_map/ppermute | solution.py:58
  48.8 19.3 %collective-permute-start.6 = (bf16[256,1152]{1,0:T(8,128)(2,1)S(1)}, bf16[256,1152]{1,0:T(8,128)(2,1)S(1)}, u32[]{:S(2)}, u32[]{:S(2)}) collective-permute-start(bf16[256,1152]{1,0:T(8,128)(2,1)S(1)} %collective-permute-done.5.m2), channel_id=1, source_target_pairs={{0,448},{1,57},{2,450},{3,59},{4,452},{5,61},{6,454},{7,63},{8,456... | collective-permute-start | bytes 1769480 | tf_op jit(solution)/shard_map/ppermute | solution.py:58
  50.7 10.7 %collective-permute-start.3 = (bf16[128,1152]{1,0:T(8,128)(2,1)S(1)}, bf16[128,1152]{1,0:T(8,128)(2,1)S(1)}, u32[]{:S(2)}, u32[]{:S(2)}) collective-permute-start(bf16[128,1152]{1,0:T(8,128)(2,1)S(1)} %slice.12), channel_id=1, source_target_pairs={{0,128},{1,17},{2,130},{3,19},{4,132},{5,21},{6,134},{7,23},{8,136... | collective-permute-start | bytes 884744 | tf_op jit(solution)/shard_map/ppermute | solution.py:58
  55.2 12.9 %collective-permute-start.7 = (bf16[128,1152]{1,0:T(8,128)(2,1)S(1)}, bf16[128,1152]{1,0:T(8,128)(2,1)S(1)}, u32[]{:S(2)}, u32[]{:S(2)}) collective-permute-start(bf16[128,1152]{1,0:T(8,128)(2,1)S(1)} %slice.13), channel_id=1, source_target_pairs={{0,384},{1,49},{2,386},{3,51},{4,388},{5,53},{6,390},{7,55},{8,392... | collective-permute-start | bytes 884744 | tf_op jit(solution)/shard_map/ppermute | solution.py:58
  72.8 2.4 %copy-start.3 = (bf16[192,2048]{1,0:T(8,128)(2,1)}, bf16[192,2048]{1,0:T(8,128)(2,1)S(1)}, u32[]{:S(2)}) copy-start(bf16[192,2048]{1,0:T(8,128)(2,1)S(1)} %get-tuple-element.10) | copy-start | bytes 2359300
  75.3 45.7 %all-to-all-start.1 = ((bf16[8,256,384]{2,1,0:T(8,128)(2,1)}), bf16[8,256,384]{2,1,0:T(8,128)(2,1)S(1)}, u32[]{:S(2)}, u32[]{:S(2)}) async-start(bf16[8,256,384]{2,1,0:T(8,128)(2,1)} %bitcast.3), calls=%async_computation.1 | async-start | bytes 3145728 | tf_op jit(solution)/shard_map/all_to_all | solution.py:62
  79.6 8.9 %collective-permute-start.8 = (bf16[192,2048]{1,0:T(8,128)(2,1)}, bf16[192,2048]{1,0:T(8,128)(2,1)S(1)}, u32[]{:S(2)}, u32[]{:S(2)}) collective-permute-start(bf16[192,2048]{1,0:T(8,128)(2,1)} %copy-done.3), channel_id=1, source_target_pairs={{0,1},{1,0},{2,3},{3,2},{4,5},{5,4},{6,7},{7,6},{8,9},{9,8},{10,11... | collective-permute-start | bytes 2359304 | tf_op jit(solution)/shard_map/ppermute | solution.py:251
  88.8 13.9 %collective-permute-start.9 = (bf16[192,2048]{1,0:T(8,128)(2,1)S(1)}, bf16[192,2048]{1,0:T(8,128)(2,1)S(1)}, u32[]{:S(2)}, u32[]{:S(2)}) collective-permute-start(bf16[192,2048]{1,0:T(8,128)(2,1)S(1)} %shard_map.79.left_ref), channel_id=1, source_target_pairs={{0,2},{1,7},{2,0},{3,5},{4,6},{5,3},{6,4},{7,1},{8,10},{9,15},{10,... | collective-permute-start | bytes 2359304 | tf_op jit(solution)/shard_map/ppermute | solution.py:247
  102.9 13.0 %collective-permute-start.10 = (bf16[192,2048]{1,0:T(8,128)(2,1)S(1)}, bf16[192,2048]{1,0:T(8,128)(2,1)S(1)}, u32[]{:S(2)}, u32[]{:S(2)}) collective-permute-start(bf16[192,2048]{1,0:T(8,128)(2,1)S(1)} %shard_map.80.left_ref), channel_id=1, source_target_pairs={{0,6},{1,3},{2,4},{3,1},{4,2},{5,7},{6,0},{7,5},{8,14},{9,11},{10,... | collective-permute-start | bytes 2359304 | tf_op jit(solution)/shard_map/ppermute | solution.py:247
  116.7 20.5 %collective-permute-start.11 = (bf16[192,2048]{1,0:T(8,128)(2,1)S(1)}, bf16[192,2048]{1,0:T(8,128)(2,1)S(1)}, u32[]{:S(2)}, u32[]{:S(2)}) collective-permute-start(bf16[192,2048]{1,0:T(8,128)(2,1)S(1)} %shard_map.81.mine_ref), channel_id=1, source_target_pairs={{0,1},{1,0},{2,3},{3,2},{4,5},{5,4},{6,7},{7,6},{8,9},{9,8},{10,11... | collective-permute-start | bytes 2359304 | tf_op jit(solution)/shard_map/ppermute | solution.py:251

commit v3 on v2

--- a/solution.py
+++ b/solution.py
@@ -188,19 +188,23 @@
     )(cotangent, hidden)
 
 
-def pair_kernel(left_ref, right_ref, out_ref):
+def pair_kernel(left_ref, right_ref, *out_refs):
     total = left_ref[...].astype(jnp.float32) + right_ref[...].astype(jnp.float32)
-    out_ref[...] = total.astype(jnp.bfloat16)
-
-
-def final_kernel(x_ref, gain_ref, left_ref, right_ref, out_ref):
+    rows = total.shape[0] // len(out_refs)
+    for k, out in enumerate(out_refs):
+        out[...] = total[k * rows : (k + 1) * rows].astype(jnp.bfloat16)
+
+
+def final_kernel(x_ref, gain_ref, left1, right1, left2, right2, out_ref):
     gain = gain_ref[...]
     for k in range(4):
         rows = pl.ds(k * QUARTER, QUARTER)
+        part = pl.ds(k % 2 * QUARTER, QUARTER)
+        left, right = ((left1, right1), (left2, right2))[k // 2]
         value = x_ref[rows, :].astype(jnp.float32)
         inverse = lax.rsqrt(jnp.mean(value * value, axis=-1, keepdims=True) + EPSILON)
         normalized = value * inverse
-        total = left_ref[rows, :].astype(jnp.float32) + right_ref[rows, :].astype(jnp.float32)
+        total = left[part, :].astype(jnp.float32) + right[part, :].astype(jnp.float32)
         scaled = total * gain
         mean = jnp.mean(scaled * normalized, axis=-1, keepdims=True)
         out_ref[rows, :] = (inverse * (scaled - normalized * mean)).astype(jnp.bfloat16)
@@ -279,11 +283,15 @@
     (total,) = small_call(sum_kernel, [jax.ShapeDtypeStruct((DROWS, HP), jnp.float32)], arrived)
     grad_down = total[:, :HU].T
 
-    (chip,) = small_call(pair_kernel, [half], keep, other)
-    got = with_partner(chip, True)
-    (two,) = small_call(pair_kernel, [half], chip, got)
-    got = with_partner(two, False)
-    (mine,) = small_call(final_kernel, [half], x_half, row, two, got)
+    piece = jax.ShapeDtypeStruct((HALF // 2, D), jnp.bfloat16)
+    chip1, chip2 = small_call(pair_kernel, [piece, piece], keep, other)
+    got1 = with_partner(chip1, True)
+    got2 = with_partner(chip2, True)
+    (two1,) = small_call(pair_kernel, [piece], chip1, got1)
+    far1 = with_partner(two1, False)
+    (two2,) = small_call(pair_kernel, [piece], chip2, got2)
+    far2 = with_partner(two2, False)
+    (mine,) = small_call(final_kernel, [half], x_half, row, two1, far1, two2, far2)
     away = with_core(mine)
     return place(mine, away), grad_down
 

time: 139 us -> 135 us (0.971)
  blocking collectives: 38.9 us -> 23.5 us
  starting transfers between devices: 51.7 us -> 62.8 us
    all_to_all x2 -> x1, blocking collectives: 38.9 us -> 23.5 us  [exchange(): lax.all_to_all(array, AXES, 0, 0, axis_index_groups=line_groups(along_rin...]
    ppermute x2 -> x4, waiting for transfers between devices: 20.4 us -> 12.5 us  [with_partner(): return lax.ppermute(array, AXES, pairs)]
    all_to_all x1 -> x2, waiting for transfers between devices: 0.01 us -> 7.46 us  [exchange(): lax.all_to_all(array, AXES, 0, 0, axis_index_groups=line_groups(along_rin...]
    all_to_all x1 -> x2, starting transfers between devices: 4.36 us -> 11.3 us  [exchange(): lax.all_to_all(array, AXES, 0, 0, axis_index_groups=line_groups(along_rin...]
    ppermute x2 -> x4, starting transfers between devices: 6.59 us -> 10.4 us  [with_partner(): return lax.ppermute(array, AXES, pairs)]
  transfers between devices with their start and end apart: 13 -> 16, of which waited for: 7 -> 10; matrix products, arithmetic and copies ran while one was open for 0% -> 0% of each run, Pallas kernels for 1% -> 3%
where the time goes in v3:
time: 135 us; the launch traced here: 134 us
  starting transfers between devices  62.8 us (47%)
  waiting for transfers between devices  34.5 us (26%)
  blocking collectives  23.5 us (17%)
  Pallas kernels  11 us (8%)
    ppermute x8, starting transfers between devices, ring(): return lax.ppermute(array, AXES, ring_pairs(step))  29.7 us
    all_to_all x1, blocking collectives, exchange(): lax.all_to_all(array, AXES, 0, 0, axis_index_groups=line_groups(along_rin...  23.5 us
    ppermute x8, waiting for transfers between devices, ring(): return lax.ppermute(array, AXES, ring_pairs(step))  12.5 us
    ppermute x4, waiting for transfers between devices, with_partner(): return lax.ppermute(array, AXES, pairs)  12.5 us
    ppermute x2, starting transfers between devices, with_core(): return lax.ppermute(array, 'c', [(0, 1), (1, 0)])  11.4 us
    all_to_all x2, starting transfers between devices, exchange(): lax.all_to_all(array, AXES, 0, 0, axis_index_groups=line_groups(along_rin...  11.3 us
    ppermute x4, starting transfers between devices, with_partner(): return lax.ppermute(array, AXES, pairs)  10.4 us
    all_to_all x2, waiting for transfers between devices, exchange(): lax.all_to_all(array, AXES, 0, 0, axis_index_groups=line_groups(along_rin...  7.46 us
  transfers between devices with their start and end apart: 16, of which 10 were waited for; matrix products, arithmetic and copies ran while one was open for 0% of the time, Pallas kernels for 3%

profile of v3, /device:TPU:1, one launch (start us, length us, event | category | flops | bytes accessed | tf_op | source)
XLA Modules:
  0.0 134.3 jit_solution(5070831010776025668)
XLA Ops:
  0.7 0.9 fusion.5
  1.6 23.5 %all_to_all.15 = bf16[8,32,1152]{2,1,0:T(8,128)(2,1)S(1)} all-to-all(bf16[8,32,1152]{2,1,0:T(8,128)(2,1)S(1)} %broadcast_in_dim.2), channel_id=1, replica_groups={{0,8,16,24,32,40,48,56},{64,72,80,88,96,104,112,120},{128,136,144,152,1..., dimensions={0} | all-to-all | bytes 1179648 | tf_op jit(solution)/shard_map/all_to_all | solution.py:62
  25.1 4.3 %collective-permute-start.1 = (bf16[256,1152]{1,0:T(8,128)(2,1)S(1)}, bf16[256,1152]{1,0:T(8,128)(2,1)S(1)}, u32[]{:S(2)}, u32[]{:S(2)}) collective-permute-start(bf16[256,1152]{1,0:T(8,128)(2,1)S(1)} %bitcast.7), channel_id=1, source_target_pairs={{0,128},{1,17},{2,130},{3,19},{4,132},{5,21},{6,134},{7,23},{8,136... | collective-permute-start | bytes 1769480 | tf_op jit(solution)/shard_map/ppermute | solution.py:58
  29.4 3.6 %collective-permute-start.5 = (bf16[256,1152]{1,0:T(8,128)(2,1)S(1)}, bf16[256,1152]{1,0:T(8,128)(2,1)S(1)}, u32[]{:S(2)}, u32[]{:S(2)}) collective-permute-start(bf16[256,1152]{1,0:T(8,128)(2,1)S(1)} %bitcast.8), channel_id=1, source_target_pairs={{0,384},{1,49},{2,386},{3,51},{4,388},{5,53},{6,390},{7,55},{8,392... | collective-permute-start | bytes 1769480 | tf_op jit(solution)/shard_map/ppermute | solution.py:58
  33.0 2.8 %collective-permute-start = (bf16[256,1152]{1,0:T(8,128)(2,1)S(1)}, bf16[256,1152]{1,0:T(8,128)(2,1)S(1)}, u32[]{:S(2)}, u32[]{:S(2)}) collective-permute-start(bf16[256,1152]{1,0:T(8,128)(2,1)S(1)} %bitcast.9), channel_id=1, source_target_pairs={{0,64},{1,9},{2,66},{3,11},{4,68},{5,13},{6,70},{7,15},{8,72},{9,1... | collective-permute-start | bytes 1769480 | tf_op jit(solution)/shard_map/ppermute | solution.py:58
  35.8 3.7 %collective-permute-start.4 = (bf16[256,1152]{1,0:T(8,128)(2,1)S(1)}, bf16[256,1152]{1,0:T(8,128)(2,1)S(1)}, u32[]{:S(2)}, u32[]{:S(2)}) collective-permute-start(bf16[256,1152]{1,0:T(8,128)(2,1)S(1)} %bitcast.10), channel_id=1, source_target_pairs={{0,448},{1,57},{2,450},{3,59},{4,452},{5,61},{6,454},{7,63},{8,456... | collective-permute-start | bytes 1769480 | tf_op jit(solution)/shard_map/ppermute | solution.py:58
  39.5 2.1 %collective-permute-done.1.p2 = bf16[256,1152]{1,0:T(8,128)(2,1)S(1)} collective-permute-done((bf16[256,1152]{1,0:T(8,128)(2,1)S(1)}, bf16[256,1152]{1,0:T(8,128)(2,1)S(1)}, u32[]{:S(2)}, u32[]{:S(2)}) %collective-permute-start.1) | collective-permute-done | bytes 589856 | tf_op jit(solution)/shard_map/ppermute | solution.py:58
  41.6 5.9 %collective-permute-start.2 = (bf16[256,1152]{1,0:T(8,128)(2,1)S(1)}, bf16[256,1152]{1,0:T(8,128)(2,1)S(1)}, u32[]{:S(2)}, u32[]{:S(2)}) collective-permute-start(bf16[256,1152]{1,0:T(8,128)(2,1)S(1)} %collective-permute-done.1.p2), channel_id=1, source_target_pairs={{0,64},{1,9},{2,66},{3,11},{4,68},{5,13},{6,70},{7,15},{8,72},{9,1... | collective-permute-start | bytes 1769480 | tf_op jit(solution)/shard_map/ppermute | solution.py:58
  47.6 1.2 collective-permute-done.5.m2
  48.8 1.9 %collective-permute-start.6 = (bf16[256,1152]{1,0:T(8,128)(2,1)S(1)}, bf16[256,1152]{1,0:T(8,128)(2,1)S(1)}, u32[]{:S(2)}, u32[]{:S(2)}) collective-permute-start(bf16[256,1152]{1,0:T(8,128)(2,1)S(1)} %collective-permute-done.5.m2), channel_id=1, source_target_pairs={{0,448},{1,57},{2,450},{3,59},{4,452},{5,61},{6,454},{7,63},{8,456... | collective-permute-start | bytes 1769480 | tf_op jit(solution)/shard_map/ppermute | solution.py:58
  50.7 4.4 %collective-permute-start.3 = (bf16[128,1152]{1,0:T(8,128)(2,1)S(1)}, bf16[128,1152]{1,0:T(8,128)(2,1)S(1)}, u32[]{:S(2)}, u32[]{:S(2)}) collective-permute-start(bf16[128,1152]{1,0:T(8,128)(2,1)S(1)} %slice.12), channel_id=1, source_target_pairs={{0,128},{1,17},{2,130},{3,19},{4,132},{5,21},{6,134},{7,23},{8,136... | collective-permute-start | bytes 884744 | tf_op jit(solution)/shard_map/ppermute | solution.py:58
  55.2 3.0 %collective-permute-start.7 = (bf16[128,1152]{1,0:T(8,128)(2,1)S(1)}, bf16[128,1152]{1,0:T(8,128)(2,1)S(1)}, u32[]{:S(2)}, u32[]{:S(2)}) collective-permute-start(bf16[128,1152]{1,0:T(8,128)(2,1)S(1)} %slice.13), channel_id=1, source_target_pairs={{0,384},{1,49},{2,386},{3,51},{4,388},{5,53},{6,390},{7,55},{8,392... | collective-permute-start | bytes 884744 | tf_op jit(solution)/shard_map/ppermute | solution.py:58
  58.9 2.6 %collective-permute-done.3.p4 = bf16[128,1152]{1,0:T(8,128)(2,1)S(1)} collective-permute-done((bf16[128,1152]{1,0:T(8,128)(2,1)S(1)}, bf16[128,1152]{1,0:T(8,128)(2,1)S(1)}, u32[]{:S(2)}, u32[]{:S(2)}) %collective-permute-start.3) | collective-permute-done | bytes 294944 | tf_op jit(solution)/shard_map/ppermute | solution.py:58
  61.5 6.6 %collective-permute-done.7.m4 = bf16[128,1152]{1,0:T(8,128)(2,1)S(1)} collective-permute-done((bf16[128,1152]{1,0:T(8,128)(2,1)S(1)}, bf16[128,1152]{1,0:T(8,128)(2,1)S(1)}, u32[]{:S(2)}, u32[]{:S(2)}) %collective-permute-start.7) | collective-permute-done | bytes 294944 | tf_op jit(solution)/shard_map/ppermute | solution.py:58
  68.1 4.7 %shard_map.78 = (bf16[192,2048]{1,0:T(8,128)(2,1)S(1)}, bf16[192,2048]{1,0:T(8,128)(2,1)S(1)}, bf16[384,384]{1,0:T(8,128)(2,1)S(1)}) custom-call(bf16[384,2048]{1,0:T(8,128)(2,1)S(1)} %get-tuple-element.10.norm_ref, bf16[384,2048]{1,0:T(8,128)(2,1)S(1)} %copy-done, bf16[256,1152]{1,0:T(8,128)(2,1)S(1)} %bitcast.11, ...), custom_call_target="tpu_custom_call" | custom-call | tf_op jit(solution)/shard_map/pallas_call | solution.py:159
  72.8 2.4 %shard_map.84 = bf16[2048,384]{1,0:T(8,128)(2,1)} custom-call(bf16[384,2048]{1,0:T(8,128)(2,1)S(1)} %copy-done, bf16[384,384]{1,0:T(8,128)(2,1)S(1)} %get-tuple-element.15.hidden_ref), custom_call_target="tpu_custom_call" | custom-call | tf_op jit(solution)/shard_map/pallas_call | solution.py:177
  75.2 4.4 %all-to-all-start.1 = ((bf16[8,256,384]{2,1,0:T(8,128)(2,1)}), bf16[8,256,384]{2,1,0:T(8,128)(2,1)S(1)}, u32[]{:S(2)}, u32[]{:S(2)}) async-start(bf16[8,256,384]{2,1,0:T(8,128)(2,1)} %bitcast.3), calls=%async_computation.1 | async-start | bytes 3145728 | tf_op jit(solution)/shard_map/all_to_all | solution.py:62
  79.6 6.8 %collective-permute-start.8 = (bf16[192,2048]{1,0:T(8,128)(2,1)}, bf16[192,2048]{1,0:T(8,128)(2,1)S(1)}, u32[]{:S(2)}, u32[]{:S(2)}) collective-permute-start(bf16[192,2048]{1,0:T(8,128)(2,1)} %copy-done.3), channel_id=1, source_target_pairs={{0,1},{1,0},{2,3},{3,2},{4,5},{5,4},{6,7},{7,6},{8,9},{9,8},{10,11... | collective-permute-start | bytes 2359304 | tf_op jit(solution)/shard_map/ppermute | solution.py:255
  86.4 2.1 %collective-permute-done.8.right_ref = bf16[192,2048]{1,0:T(8,128)(2,1)S(1)} collective-permute-done((bf16[192,2048]{1,0:T(8,128)(2,1)}, bf16[192,2048]{1,0:T(8,128)(2,1)S(1)}, u32[]{:S(2)}, u32[]{:S(2)}) %collective-permute-start.8) | collective-permute-done | bytes 786464 | tf_op jit(solution)/shard_map/ppermute | solution.py:255
  88.7 4.4 %collective-permute-start.9 = (bf16[96,2048]{1,0:T(8,128)(2,1)S(1)}, bf16[96,2048]{1,0:T(8,128)(2,1)S(1)}, u32[]{:S(2)}, u32[]{:S(2)}) collective-permute-start(bf16[96,2048]{1,0:T(8,128)(2,1)S(1)} %get-tuple-element.13.left_ref), channel_id=1, source_target_pairs={{0,2},{1,7},{2,0},{3,5},{4,6},{5,3},{6,4},{7,1},{8,10},{9,15},{10,... | collective-permute-start | bytes 1179656 | tf_op jit(solution)/shard_map/ppermute | solution.py:251
  93.1 2.1 %collective-permute-start.11 = (bf16[96,2048]{1,0:T(8,128)(2,1)S(1)}, bf16[96,2048]{1,0:T(8,128)(2,1)S(1)}, u32[]{:S(2)}, u32[]{:S(2)}) collective-permute-start(bf16[96,2048]{1,0:T(8,128)(2,1)S(1)} %get-tuple-element.14.left_ref), channel_id=1, source_target_pairs={{0,2},{1,7},{2,0},{3,5},{4,6},{5,3},{6,4},{7,1},{8,10},{9,15},{10,... | collective-permute-start | bytes 1179656 | tf_op jit(solution)/shard_map/ppermute | solution.py:251
  95.2 3.5 %collective-permute-done.9.right_ref = bf16[96,2048]{1,0:T(8,128)(2,1)S(1)} collective-permute-done((bf16[96,2048]{1,0:T(8,128)(2,1)S(1)}, bf16[96,2048]{1,0:T(8,128)(2,1)S(1)}, u32[]{:S(2)}, u32[]{:S(2)}) %collective-permute-start.9) | collective-permute-done | bytes 393248 | tf_op jit(solution)/shard_map/ppermute | solution.py:251
  98.8 1.9 %collective-permute-start.10 = (bf16[96,2048]{1,0:T(8,128)(2,1)S(1)}, bf16[96,2048]{1,0:T(8,128)(2,1)S(1)}, u32[]{:S(2)}, u32[]{:S(2)}) collective-permute-start(bf16[96,2048]{1,0:T(8,128)(2,1)S(1)} %shard_map.80.left1), channel_id=1, source_target_pairs={{0,6},{1,3},{2,4},{3,1},{4,2},{5,7},{6,0},{7,5},{8,14},{9,11},{10,... | collective-permute-start | bytes 1179656 | tf_op jit(solution)/shard_map/ppermute | solution.py:251
  100.7 2.1 %collective-permute-done.11.right_ref = bf16[96,2048]{1,0:T(8,128)(2,1)S(1)} collective-permute-done((bf16[96,2048]{1,0:T(8,128)(2,1)S(1)}, bf16[96,2048]{1,0:T(8,128)(2,1)S(1)}, u32[]{:S(2)}, u32[]{:S(2)}) %collective-permute-start.11) | collective-permute-done | bytes 393248 | tf_op jit(solution)/shard_map/ppermute | solution.py:251
  102.9 2.0 %collective-permute-start.12 = (bf16[96,2048]{1,0:T(8,128)(2,1)S(1)}, bf16[96,2048]{1,0:T(8,128)(2,1)S(1)}, u32[]{:S(2)}, u32[]{:S(2)}) collective-permute-start(bf16[96,2048]{1,0:T(8,128)(2,1)S(1)} %shard_map.81.left2), channel_id=1, source_target_pairs={{0,6},{1,3},{2,4},{3,1},{4,2},{5,7},{6,0},{7,5},{8,14},{9,11},{10,... | collective-permute-start | bytes 1179656 | tf_op jit(solution)/shard_map/ppermute | solution.py:251
  105.0 2.7 %collective-permute-done.10.right1 = bf16[96,2048]{1,0:T(8,128)(2,1)S(1)} collective-permute-done((bf16[96,2048]{1,0:T(8,128)(2,1)S(1)}, bf16[96,2048]{1,0:T(8,128)(2,1)S(1)}, u32[]{:S(2)}, u32[]{:S(2)}) %collective-permute-start.10) | collective-permute-done | bytes 393248 | tf_op jit(solution)/shard_map/ppermute | solution.py:251
  107.6 4.2 %collective-permute-done.12.right2 = bf16[96,2048]{1,0:T(8,128)(2,1)S(1)} collective-permute-done((bf16[96,2048]{1,0:T(8,128)(2,1)S(1)}, bf16[96,2048]{1,0:T(8,128)(2,1)S(1)}, u32[]{:S(2)}, u32[]{:S(2)}) %collective-permute-start.12) | collective-permute-done | bytes 393248 | tf_op jit(solution)/shard_map/ppermute | solution.py:251
  112.6 4.6 %collective-permute-start.13 = (bf16[192,2048]{1,0:T(8,128)(2,1)S(1)}, bf16[192,2048]{1,0:T(8,128)(2,1)S(1)}, u32[]{:S(2)}, u32[]{:S(2)}) collective-permute-start(bf16[192,2048]{1,0:T(8,128)(2,1)S(1)} %shard_map.82.mine_ref), channel_id=1, source_target_pairs={{0,1},{1,0},{2,3},{3,2},{4,5},{5,4},{6,7},{7,6},{8,9},{9,8},{10,11... | collective-permute-start | bytes 2359304 | tf_op jit(solution)/shard_map/ppermute | solution.py:255
  117.2 0.9 shard_map.85
  118.1 6.9 %all-to-all-start.2 = ((bf16[8,32,384]{2,1,0:T(8,128)(2,1)}), bf16[8,32,384]{2,1,0:T(8,128)(2,1)S(1)}, u32[]{:S(2)}, u32[]{:S(2)}) async-start(bf16[8,32,384]{2,1,0:T(8,128)(2,1)} %bitcast.4), calls=%async_computation.2 | async-start | bytes 393216 | tf_op jit(solution)/shard_map/all_to_all | solution.py:62
  125.0 1.2 shard_map.83
  126.2 7.5 %all-to-all-done.2.parts_ref = bf16[8,32,384]{2,1,0:T(8,128)(2,1)S(1)} async-done(((bf16[8,32,384]{2,1,0:T(8,128)(2,1)}), bf16[8,32,384]{2,1,0:T(8,128)(2,1)S(1)}, u32[]{:S(2)}, u32[]{:S(2)}) %all-to-all-start.2) | async-done | bytes 196640 | tf_op jit(solution)/shard_map/all_to_all | solution.py:62
  (24 shorter events, 2.6 us)
Async XLA Ops:
  0.6 57.6 %copy-start.1 = (bf16[384,2048]{1,0:T(8,128)(2,1)S(1)}, bf16[384,2048]{1,0:T(8,128)(2,1)}, u32[]{:S(2)}) copy-start(bf16[384,2048]{1,0:T(8,128)(2,1)} %x_ref.1) | copy-start | bytes 4718596
  0.6 57.6 %copy-start.2 = (f32[2048]{0:T(1024)S(1)}, f32[2048]{0:T(1024)}, u32[]{:S(2)}) copy-start(f32[2048]{0:T(1024)} %param.7) | copy-start | bytes 24580
  25.1 43.0 %copy-start = (bf16[384,2048]{1,0:T(8,128)(2,1)S(1)}, bf16[384,2048]{1,0:T(8,128)(2,1)}, u32[]{:S(2)}) copy-start(bf16[384,2048]{1,0:T(8,128)(2,1)} %cot_ref.3) | copy-start | bytes 4718596
  25.1 16.5 %collective-permute-start.1 = (bf16[256,1152]{1,0:T(8,128)(2,1)S(1)}, bf16[256,1152]{1,0:T(8,128)(2,1)S(1)}, u32[]{:S(2)}, u32[]{:S(2)}) collective-permute-start(bf16[256,1152]{1,0:T(8,128)(2,1)S(1)} %bitcast.7), channel_id=1, source_target_pairs={{0,128},{1,17},{2,130},{3,19},{4,132},{5,21},{6,134},{7,23},{8,136... | collective-permute-start | bytes 1769480 | tf_op jit(solution)/shard_map/ppermute | solution.py:58
  29.4 19.4 %collective-permute-start.5 = (bf16[256,1152]{1,0:T(8,128)(2,1)S(1)}, bf16[256,1152]{1,0:T(8,128)(2,1)S(1)}, u32[]{:S(2)}, u32[]{:S(2)}) collective-permute-start(bf16[256,1152]{1,0:T(8,128)(2,1)S(1)} %bitcast.8), channel_id=1, source_target_pairs={{0,384},{1,49},{2,386},{3,51},{4,388},{5,53},{6,390},{7,55},{8,392... | collective-permute-start | bytes 1769480 | tf_op jit(solution)/shard_map/ppermute | solution.py:58
  33.0 22.1 %collective-permute-start = (bf16[256,1152]{1,0:T(8,128)(2,1)S(1)}, bf16[256,1152]{1,0:T(8,128)(2,1)S(1)}, u32[]{:S(2)}, u32[]{:S(2)}) collective-permute-start(bf16[256,1152]{1,0:T(8,128)(2,1)S(1)} %bitcast.9), channel_id=1, source_target_pairs={{0,64},{1,9},{2,66},{3,11},{4,68},{5,13},{6,70},{7,15},{8,72},{9,1... | collective-permute-start | bytes 1769480 | tf_op jit(solution)/shard_map/ppermute | solution.py:58
  35.8 23.0 %collective-permute-start.4 = (bf16[256,1152]{1,0:T(8,128)(2,1)S(1)}, bf16[256,1152]{1,0:T(8,128)(2,1)S(1)}, u32[]{:S(2)}, u32[]{:S(2)}) collective-permute-start(bf16[256,1152]{1,0:T(8,128)(2,1)S(1)} %bitcast.10), channel_id=1, source_target_pairs={{0,448},{1,57},{2,450},{3,59},{4,452},{5,61},{6,454},{7,63},{8,456... | collective-permute-start | bytes 1769480 | tf_op jit(solution)/shard_map/ppermute | solution.py:58
  41.6 26.4 %collective-permute-start.2 = (bf16[256,1152]{1,0:T(8,128)(2,1)S(1)}, bf16[256,1152]{1,0:T(8,128)(2,1)S(1)}, u32[]{:S(2)}, u32[]{:S(2)}) collective-permute-start(bf16[256,1152]{1,0:T(8,128)(2,1)S(1)} %collective-permute-done.1.p2), channel_id=1, source_target_pairs={{0,64},{1,9},{2,66},{3,11},{4,68},{5,13},{6,70},{7,15},{8,72},{9,1... | collective-permute-start | bytes 1769480 | tf_op jit(solution)/shard_map/ppermute | solution.py:58
  48.8 19.3 %collective-permute-start.6 = (bf16[256,1152]{1,0:T(8,128)(2,1)S(1)}, bf16[256,1152]{1,0:T(8,128)(2,1)S(1)}, u32[]{:S(2)}, u32[]{:S(2)}) collective-permute-start(bf16[256,1152]{1,0:T(8,128)(2,1)S(1)} %collective-permute-done.5.m2), channel_id=1, source_target_pairs={{0,448},{1,57},{2,450},{3,59},{4,452},{5,61},{6,454},{7,63},{8,456... | collective-permute-start | bytes 1769480 | tf_op jit(solution)/shard_map/ppermute | solution.py:58
  50.7 10.7 %collective-permute-start.3 = (bf16[128,1152]{1,0:T(8,128)(2,1)S(1)}, bf16[128,1152]{1,0:T(8,128)(2,1)S(1)}, u32[]{:S(2)}, u32[]{:S(2)}) collective-permute-start(bf16[128,1152]{1,0:T(8,128)(2,1)S(1)} %slice.12), channel_id=1, source_target_pairs={{0,128},{1,17},{2,130},{3,19},{4,132},{5,21},{6,134},{7,23},{8,136... | collective-permute-start | bytes 884744 | tf_op jit(solution)/shard_map/ppermute | solution.py:58
  55.2 12.9 %collective-permute-start.7 = (bf16[128,1152]{1,0:T(8,128)(2,1)S(1)}, bf16[128,1152]{1,0:T(8,128)(2,1)S(1)}, u32[]{:S(2)}, u32[]{:S(2)}) collective-permute-start(bf16[128,1152]{1,0:T(8,128)(2,1)S(1)} %slice.13), channel_id=1, source_target_pairs={{0,384},{1,49},{2,386},{3,51},{4,388},{5,53},{6,390},{7,55},{8,392... | collective-permute-start | bytes 884744 | tf_op jit(solution)/shard_map/ppermute | solution.py:58
  72.8 2.4 %copy-start.3 = (bf16[192,2048]{1,0:T(8,128)(2,1)}, bf16[192,2048]{1,0:T(8,128)(2,1)S(1)}, u32[]{:S(2)}) copy-start(bf16[192,2048]{1,0:T(8,128)(2,1)S(1)} %get-tuple-element.12) | copy-start | bytes 2359300
  75.2 42.0 %all-to-all-start.1 = ((bf16[8,256,384]{2,1,0:T(8,128)(2,1)}), bf16[8,256,384]{2,1,0:T(8,128)(2,1)S(1)}, u32[]{:S(2)}, u32[]{:S(2)}) async-start(bf16[8,256,384]{2,1,0:T(8,128)(2,1)} %bitcast.3), calls=%async_computation.1 | async-start | bytes 3145728 | tf_op jit(solution)/shard_map/all_to_all | solution.py:62
  79.6 8.9 %collective-permute-start.8 = (bf16[192,2048]{1,0:T(8,128)(2,1)}, bf16[192,2048]{1,0:T(8,128)(2,1)S(1)}, u32[]{:S(2)}, u32[]{:S(2)}) collective-permute-start(bf16[192,2048]{1,0:T(8,128)(2,1)} %copy-done.3), channel_id=1, source_target_pairs={{0,1},{1,0},{2,3},{3,2},{4,5},{5,4},{6,7},{7,6},{8,9},{9,8},{10,11... | collective-permute-start | bytes 2359304 | tf_op jit(solution)/shard_map/ppermute | solution.py:255
  88.7 10.0 %collective-permute-start.9 = (bf16[96,2048]{1,0:T(8,128)(2,1)S(1)}, bf16[96,2048]{1,0:T(8,128)(2,1)S(1)}, u32[]{:S(2)}, u32[]{:S(2)}) collective-permute-start(bf16[96,2048]{1,0:T(8,128)(2,1)S(1)} %get-tuple-element.13.left_ref), channel_id=1, source_target_pairs={{0,2},{1,7},{2,0},{3,5},{4,6},{5,3},{6,4},{7,1},{8,10},{9,15},{10,... | collective-permute-start | bytes 1179656 | tf_op jit(solution)/shard_map/ppermute | solution.py:251
  93.1 9.7 %collective-permute-start.11 = (bf16[96,2048]{1,0:T(8,128)(2,1)S(1)}, bf16[96,2048]{1,0:T(8,128)(2,1)S(1)}, u32[]{:S(2)}, u32[]{:S(2)}) collective-permute-start(bf16[96,2048]{1,0:T(8,128)(2,1)S(1)} %get-tuple-element.14.left_ref), channel_id=1, source_target_pairs={{0,2},{1,7},{2,0},{3,5},{4,6},{5,3},{6,4},{7,1},{8,10},{9,15},{10,... | collective-permute-start | bytes 1179656 | tf_op jit(solution)/shard_map/ppermute | solution.py:251
  98.8 8.8 %collective-permute-start.10 = (bf16[96,2048]{1,0:T(8,128)(2,1)S(1)}, bf16[96,2048]{1,0:T(8,128)(2,1)S(1)}, u32[]{:S(2)}, u32[]{:S(2)}) collective-permute-start(bf16[96,2048]{1,0:T(8,128)(2,1)S(1)} %shard_map.80.left1), channel_id=1, source_target_pairs={{0,6},{1,3},{2,4},{3,1},{4,2},{5,7},{6,0},{7,5},{8,14},{9,11},{10,... | collective-permute-start | bytes 1179656 | tf_op jit(solution)/shard_map/ppermute | solution.py:251
  102.9 8.9 %collective-permute-start.12 = (bf16[96,2048]{1,0:T(8,128)(2,1)S(1)}, bf16[96,2048]{1,0:T(8,128)(2,1)S(1)}, u32[]{:S(2)}, u32[]{:S(2)}) collective-permute-start(bf16[96,2048]{1,0:T(8,128)(2,1)S(1)} %shard_map.81.left2), channel_id=1, source_target_pairs={{0,6},{1,3},{2,4},{3,1},{4,2},{5,7},{6,0},{7,5},{8,14},{9,11},{10,... | collective-permute-start | bytes 1179656 | tf_op jit(solution)/shard_map/ppermute | solution.py:251
  112.6 12.4 %collective-permute-start.13 = (bf16[192,2048]{1,0:T(8,128)(2,1)S(1)}, bf16[192,2048]{1,0:T(8,128)(2,1)S(1)}, u32[]{:S(2)}, u32[]{:S(2)}) collective-permute-start(bf16[192,2048]{1,0:T(8,128)(2,1)S(1)} %shard_map.82.mine_ref), channel_id=1, source_target_pairs={{0,1},{1,0},{2,3},{3,2},{4,5},{5,4},{6,7},{7,6},{8,9},{9,8},{10,11... | collective-permute-start | bytes 2359304 | tf_op jit(solution)/shard_map/ppermute | solution.py:255
  118.1 15.6 %all-to-all-start.2 = ((bf16[8,32,384]{2,1,0:T(8,128)(2,1)}), bf16[8,32,384]{2,1,0:T(8,128)(2,1)S(1)}, u32[]{:S(2)}, u32[]{:S(2)}) async-start(bf16[8,32,384]{2,1,0:T(8,128)(2,1)} %bitcast.4), calls=%async_computation.2 | async-start | bytes 393216 | tf_op jit(solution)/shard_map/all_to_all | solution.py:62

commit v4 on v3

--- a/solution.py
+++ b/solution.py
@@ -120,23 +120,19 @@
     send_ref[...] = part_ref[half_rows(1 - c), :]
 
 
-def down_kernel(cot_ref, hidden_ref, down_ref, dt_ref, ordered_ref, sems):
+def turn_kernel(cot_ref, turned_ref):
     c = lax.axis_index("c")
-    dt = dot(cot_ref[...], hidden_ref[...], ((0,), (0,)))
-    dt_ref[...] = (HALF_STEP * dt).astype(jnp.bfloat16)
-    copies = []
-    for q in range(8):
-        for o in range(8):
-            row = jnp.where(c == 0, q * 256 + o * 32, o * 256 + q * 32)
+    for z in range(NZ):
+        block = cot_ref[:, z * 256 : (z + 1) * 256].T
+        for y in range(NY):
+            row = jnp.where(c == 0, z * 256 + y * 32, y * 256 + z * 32)
             rows = pl.ds(pl.multiple_of(row, 32), DROWS)
-            ordered_ref[pl.ds(q * 256 + o * 32, DROWS), :] = dt_ref[rows, :]
-        block = pl.ds(q * 256, 256)
-        copies.append(
-            pltpu.make_async_copy(ordered_ref.at[block, :], down_ref.at[block, :], sems.at[q])
-        )
-        copies[-1].start()
-    for copy in copies:
-        copy.wait()
+            turned_ref[rows, :] = block[y * 32 : (y + 1) * 32, :]
+
+
+def down_kernel(turned_ref, hidden_ref, down_ref):
+    down = HALF_STEP * dot(turned_ref[...], hidden_ref[...], ((1,), (0,)))
+    down_ref[...] = down.astype(jnp.bfloat16)
 
 
 def vmem_specs(count):
@@ -173,19 +169,14 @@
     )(normed, cotangent, *blocks)
 
 
-def down_product(cotangent, hidden):
+def one_call(kernel, out_shape, *operands):
     return pl.pallas_call(
-        down_kernel,
-        out_shape=jax.ShapeDtypeStruct((D, HP), jnp.bfloat16),
-        in_specs=vmem_specs(2),
-        out_specs=pl.BlockSpec(memory_space=pltpu.HBM),
-        scratch_shapes=[
-            pltpu.VMEM((D, HP), jnp.bfloat16),
-            pltpu.VMEM((D, HP), jnp.bfloat16),
-            pltpu.SemaphoreType.DMA((8,)),
-        ],
+        kernel,
+        out_shape=out_shape,
+        in_specs=vmem_specs(len(operands)),
+        out_specs=vmem_specs(1)[0],
         compiler_params=pltpu.CompilerParams(vmem_limit_bytes=DOWN_LIMIT),
-    )(cotangent, hidden)
+    )(*operands)
 
 
 def pair_kernel(left_ref, right_ref, *out_refs):
@@ -237,7 +228,7 @@
     total = parts_ref[0].astype(jnp.float32)
     for k in range(1, 8):
         total = total + parts_ref[k].astype(jnp.float32)
-    out_ref[...] = total.astype(out_ref.dtype)
+    out_ref[...] = total[:, : out_ref.shape[1]].astype(out_ref.dtype)
 
 
 def with_partner(array, first):
@@ -274,14 +265,17 @@
     normed, x_half = small_call(
         normalize_kernel, [jax.ShapeDtypeStruct((TOK, D), jnp.bfloat16), half], inputs, row
     )
+    turned = one_call(turn_kernel, jax.ShapeDtypeStruct((D, TOK), jnp.bfloat16), cotangent)
     keep, send, hidden = compute(normed, cotangent, (b0, p1, p2, p3, p4, m1, m2, m3, m4))
     other = with_core(send)
-    down = down_product(cotangent, hidden)
+    down = one_call(
+        down_kernel, jax.ShapeDtypeStruct((D, HP), jnp.bfloat16), turned, hidden
+    )
     arrived = exchange(down.reshape(8, 256, HP), True)
     (line,) = small_call(sum_kernel, [jax.ShapeDtypeStruct((256, HP), jnp.bfloat16)], arrived)
     arrived = exchange(line.reshape(8, DROWS, HP), False)
-    (total,) = small_call(sum_kernel, [jax.ShapeDtypeStruct((DROWS, HP), jnp.float32)], arrived)
-    grad_down = total[:, :HU].T
+    (total,) = small_call(sum_kernel, [jax.ShapeDtypeStruct((DROWS, HU), jnp.float32)], arrived)
+    grad_down = total.T
 
     piece = jax.ShapeDtypeStruct((HALF // 2, D), jnp.bfloat16)
     chip1, chip2 = small_call(pair_kernel, [piece, piece], keep, other)
@@ -293,7 +287,8 @@
     far2 = with_partner(two2, False)
     (mine,) = small_call(final_kernel, [half], x_half, row, two1, far1, two2, far2)
     away = with_core(mine)
-    return place(mine, away), grad_down
+    whole = place(mine, away)
+    return whole, grad_down
 
 
 def solution(mesh):

time: 135 us -> 135 us (level)
    pallas_call x1 -> x2, Pallas kernels: 2.41 us -> 2.71 us  [one_call(): pl.pallas_call(kernel, out_shape=out_shape, in_specs=vmem_specs(len(opera...]
where the time goes in v4:
time: 135 us
  starting transfers between devices  63.2 us (47%)
  waiting for transfers between devices  34.1 us (25%)
  blocking collectives  23.5 us (17%)
  Pallas kernels  11.9 us (9%)
    ppermute x8, starting transfers between devices, ring(): return lax.ppermute(array, AXES, ring_pairs(step))  29.7 us
    all_to_all x1, blocking collectives, exchange(): lax.all_to_all(array, AXES, 0, 0, axis_index_groups=line_groups(along_rin...  23.5 us
    ppermute x4, waiting for transfers between devices, with_partner(): return lax.ppermute(array, AXES, pairs)  12.5 us
    ppermute x8, waiting for transfers between devices, ring(): return lax.ppermute(array, AXES, ring_pairs(step))  12 us
    ppermute x2, starting transfers between devices, with_core(): return lax.ppermute(array, 'c', [(0, 1), (1, 0)])  11.9 us
    all_to_all x2, starting transfers between devices, exchange(): lax.all_to_all(array, AXES, 0, 0, axis_index_groups=line_groups(along_rin...  11.3 us
    ppermute x4, starting transfers between devices, with_partner(): return lax.ppermute(array, AXES, pairs)  10.4 us
    all_to_all x2, waiting for transfers between devices, exchange(): lax.all_to_all(array, AXES, 0, 0, axis_index_groups=line_groups(along_rin...  7.46 us
  transfers between devices with their start and end apart: 16, of which 10 were waited for; matrix products, arithmetic and copies ran while one was open for 0% of the time, Pallas kernels for 3%

profile of v4, /device:TPU:1, one launch (start us, length us, event | category | flops | bytes accessed | tf_op | source)
XLA Modules:
  0.0 134.6 jit_solution(5575309655757522944)
XLA Ops:
  0.6 0.9 fusion.5
  1.6 23.5 %all_to_all.15 = bf16[8,32,1152]{2,1,0:T(8,128)(2,1)S(1)} all-to-all(bf16[8,32,1152]{2,1,0:T(8,128)(2,1)S(1)} %broadcast_in_dim.2), channel_id=1, replica_groups={{0,8,16,24,32,40,48,56},{64,72,80,88,96,104,112,120},{128,136,144,152,1..., dimensions={0} | all-to-all | bytes 1179648 | tf_op jit(solution)/shard_map/all_to_all | solution.py:62
  25.1 4.2 %collective-permute-start.1 = (bf16[256,1152]{1,0:T(8,128)(2,1)S(1)}, bf16[256,1152]{1,0:T(8,128)(2,1)S(1)}, u32[]{:S(2)}, u32[]{:S(2)}) collective-permute-start(bf16[256,1152]{1,0:T(8,128)(2,1)S(1)} %bitcast.6), channel_id=1, source_target_pairs={{0,128},{1,17},{2,130},{3,19},{4,132},{5,21},{6,134},{7,23},{8,136... | collective-permute-start | bytes 1769480 | tf_op jit(solution)/shard_map/ppermute | solution.py:58
  29.3 3.6 %collective-permute-start.5 = (bf16[256,1152]{1,0:T(8,128)(2,1)S(1)}, bf16[256,1152]{1,0:T(8,128)(2,1)S(1)}, u32[]{:S(2)}, u32[]{:S(2)}) collective-permute-start(bf16[256,1152]{1,0:T(8,128)(2,1)S(1)} %bitcast.7), channel_id=1, source_target_pairs={{0,384},{1,49},{2,386},{3,51},{4,388},{5,53},{6,390},{7,55},{8,392... | collective-permute-start | bytes 1769480 | tf_op jit(solution)/shard_map/ppermute | solution.py:58
  32.9 2.8 %collective-permute-start = (bf16[256,1152]{1,0:T(8,128)(2,1)S(1)}, bf16[256,1152]{1,0:T(8,128)(2,1)S(1)}, u32[]{:S(2)}, u32[]{:S(2)}) collective-permute-start(bf16[256,1152]{1,0:T(8,128)(2,1)S(1)} %bitcast.8), channel_id=1, source_target_pairs={{0,64},{1,9},{2,66},{3,11},{4,68},{5,13},{6,70},{7,15},{8,72},{9,1... | collective-permute-start | bytes 1769480 | tf_op jit(solution)/shard_map/ppermute | solution.py:58
  35.7 3.7 %collective-permute-start.4 = (bf16[256,1152]{1,0:T(8,128)(2,1)S(1)}, bf16[256,1152]{1,0:T(8,128)(2,1)S(1)}, u32[]{:S(2)}, u32[]{:S(2)}) collective-permute-start(bf16[256,1152]{1,0:T(8,128)(2,1)S(1)} %bitcast.9), channel_id=1, source_target_pairs={{0,448},{1,57},{2,450},{3,59},{4,452},{5,61},{6,454},{7,63},{8,456... | collective-permute-start | bytes 1769480 | tf_op jit(solution)/shard_map/ppermute | solution.py:58
  39.4 2.1 %collective-permute-done.1.p2 = bf16[256,1152]{1,0:T(8,128)(2,1)S(1)} collective-permute-done((bf16[256,1152]{1,0:T(8,128)(2,1)S(1)}, bf16[256,1152]{1,0:T(8,128)(2,1)S(1)}, u32[]{:S(2)}, u32[]{:S(2)}) %collective-permute-start.1) | collective-permute-done | bytes 589856 | tf_op jit(solution)/shard_map/ppermute | solution.py:58
  41.5 5.9 %collective-permute-start.2 = (bf16[256,1152]{1,0:T(8,128)(2,1)S(1)}, bf16[256,1152]{1,0:T(8,128)(2,1)S(1)}, u32[]{:S(2)}, u32[]{:S(2)}) collective-permute-start(bf16[256,1152]{1,0:T(8,128)(2,1)S(1)} %collective-permute-done.1.p2), channel_id=1, source_target_pairs={{0,64},{1,9},{2,66},{3,11},{4,68},{5,13},{6,70},{7,15},{8,72},{9,1... | collective-permute-start | bytes 1769480 | tf_op jit(solution)/shard_map/ppermute | solution.py:58
  47.4 1.2 collective-permute-done.5.m2
  48.7 1.9 %collective-permute-start.6 = (bf16[256,1152]{1,0:T(8,128)(2,1)S(1)}, bf16[256,1152]{1,0:T(8,128)(2,1)S(1)}, u32[]{:S(2)}, u32[]{:S(2)}) collective-permute-start(bf16[256,1152]{1,0:T(8,128)(2,1)S(1)} %collective-permute-done.5.m2), channel_id=1, source_target_pairs={{0,448},{1,57},{2,450},{3,59},{4,452},{5,61},{6,454},{7,63},{8,456... | collective-permute-start | bytes 1769480 | tf_op jit(solution)/shard_map/ppermute | solution.py:58
  50.6 4.4 %collective-permute-start.3 = (bf16[128,1152]{1,0:T(8,128)(2,1)S(1)}, bf16[128,1152]{1,0:T(8,128)(2,1)S(1)}, u32[]{:S(2)}, u32[]{:S(2)}) collective-permute-start(bf16[128,1152]{1,0:T(8,128)(2,1)S(1)} %slice.8), channel_id=1, source_target_pairs={{0,128},{1,17},{2,130},{3,19},{4,132},{5,21},{6,134},{7,23},{8,136... | collective-permute-start | bytes 884744 | tf_op jit(solution)/shard_map/ppermute | solution.py:58
  55.0 3.2 %collective-permute-start.7 = (bf16[128,1152]{1,0:T(8,128)(2,1)S(1)}, bf16[128,1152]{1,0:T(8,128)(2,1)S(1)}, u32[]{:S(2)}, u32[]{:S(2)}) collective-permute-start(bf16[128,1152]{1,0:T(8,128)(2,1)S(1)} %slice.9), channel_id=1, source_target_pairs={{0,384},{1,49},{2,386},{3,51},{4,388},{5,53},{6,390},{7,55},{8,392... | collective-permute-start | bytes 884744 | tf_op jit(solution)/shard_map/ppermute | solution.py:58
  59.4 2.0 %collective-permute-done.3.p4 = bf16[128,1152]{1,0:T(8,128)(2,1)S(1)} collective-permute-done((bf16[128,1152]{1,0:T(8,128)(2,1)S(1)}, bf16[128,1152]{1,0:T(8,128)(2,1)S(1)}, u32[]{:S(2)}, u32[]{:S(2)}) %collective-permute-start.3) | collective-permute-done | bytes 294944 | tf_op jit(solution)/shard_map/ppermute | solution.py:58
  61.3 6.7 %collective-permute-done.7.m4 = bf16[128,1152]{1,0:T(8,128)(2,1)S(1)} collective-permute-done((bf16[128,1152]{1,0:T(8,128)(2,1)S(1)}, bf16[128,1152]{1,0:T(8,128)(2,1)S(1)}, u32[]{:S(2)}, u32[]{:S(2)}) %collective-permute-start.7) | collective-permute-done | bytes 294944 | tf_op jit(solution)/shard_map/ppermute | solution.py:58
  68.1 4.7 %shard_map.78 = (bf16[192,2048]{1,0:T(8,128)(2,1)S(1)}, bf16[192,2048]{1,0:T(8,128)(2,1)S(1)}, bf16[384,384]{1,0:T(8,128)(2,1)S(1)}) custom-call(bf16[384,2048]{1,0:T(8,128)(2,1)S(1)} %get-tuple-element.10.norm_ref, bf16[384,2048]{1,0:T(8,128)(2,1)S(1)} %copy-done, bf16[256,1152]{1,0:T(8,128)(2,1)S(1)} %bitcast.10, ...), custom_call_target="tpu_custom_call" | custom-call | tf_op jit(solution)/shard_map/pallas_call | solution.py:155
  72.8 2.3 %shard_map.85 = bf16[2048,384]{1,0:T(8,128)(2,1)} custom-call(bf16[2048,384]{1,0:T(8,128)(2,1)S(1)} %shard_map.84.turned_ref, bf16[384,384]{1,0:T(8,128)(2,1)S(1)} %get-tuple-element.15.hidden_ref), custom_call_target="tpu_custom_call" | custom-call | tf_op jit(solution)/shard_map/pallas_call | solution.py:173
  75.0 4.4 %all-to-all-start.1 = ((bf16[8,256,384]{2,1,0:T(8,128)(2,1)}), bf16[8,256,384]{2,1,0:T(8,128)(2,1)S(1)}, u32[]{:S(2)}, u32[]{:S(2)}) async-start(bf16[8,256,384]{2,1,0:T(8,128)(2,1)} %bitcast.3), calls=%async_computation.1 | async-start | bytes 3145728 | tf_op jit(solution)/shard_map/all_to_all | solution.py:62
  79.4 7.3 %collective-permute-start.8 = (bf16[192,2048]{1,0:T(8,128)(2,1)}, bf16[192,2048]{1,0:T(8,128)(2,1)S(1)}, u32[]{:S(2)}, u32[]{:S(2)}) collective-permute-start(bf16[192,2048]{1,0:T(8,128)(2,1)} %copy-done.3), channel_id=1, source_target_pairs={{0,1},{1,0},{2,3},{3,2},{4,5},{5,4},{6,7},{7,6},{8,9},{9,8},{10,11... | collective-permute-start | bytes 2359304 | tf_op jit(solution)/shard_map/ppermute | solution.py:246
  86.7 2.1 %collective-permute-done.8.right_ref = bf16[192,2048]{1,0:T(8,128)(2,1)S(1)} collective-permute-done((bf16[192,2048]{1,0:T(8,128)(2,1)}, bf16[192,2048]{1,0:T(8,128)(2,1)S(1)}, u32[]{:S(2)}, u32[]{:S(2)}) %collective-permute-start.8) | collective-permute-done | bytes 786464 | tf_op jit(solution)/shard_map/ppermute | solution.py:246
  89.0 4.4 %collective-permute-start.9 = (bf16[96,2048]{1,0:T(8,128)(2,1)S(1)}, bf16[96,2048]{1,0:T(8,128)(2,1)S(1)}, u32[]{:S(2)}, u32[]{:S(2)}) collective-permute-start(bf16[96,2048]{1,0:T(8,128)(2,1)S(1)} %get-tuple-element.13.left_ref), channel_id=1, source_target_pairs={{0,2},{1,7},{2,0},{3,5},{4,6},{5,3},{6,4},{7,1},{8,10},{9,15},{10,... | collective-permute-start | bytes 1179656 | tf_op jit(solution)/shard_map/ppermute | solution.py:242
  93.4 2.1 %collective-permute-start.11 = (bf16[96,2048]{1,0:T(8,128)(2,1)S(1)}, bf16[96,2048]{1,0:T(8,128)(2,1)S(1)}, u32[]{:S(2)}, u32[]{:S(2)}) collective-permute-start(bf16[96,2048]{1,0:T(8,128)(2,1)S(1)} %get-tuple-element.14.left_ref), channel_id=1, source_target_pairs={{0,2},{1,7},{2,0},{3,5},{4,6},{5,3},{6,4},{7,1},{8,10},{9,15},{10,... | collective-permute-start | bytes 1179656 | tf_op jit(solution)/shard_map/ppermute | solution.py:242
  95.5 3.5 %collective-permute-done.9.right_ref = bf16[96,2048]{1,0:T(8,128)(2,1)S(1)} collective-permute-done((bf16[96,2048]{1,0:T(8,128)(2,1)S(1)}, bf16[96,2048]{1,0:T(8,128)(2,1)S(1)}, u32[]{:S(2)}, u32[]{:S(2)}) %collective-permute-start.9) | collective-permute-done | bytes 393248 | tf_op jit(solution)/shard_map/ppermute | solution.py:242
  99.1 1.9 %collective-permute-start.10 = (bf16[96,2048]{1,0:T(8,128)(2,1)S(1)}, bf16[96,2048]{1,0:T(8,128)(2,1)S(1)}, u32[]{:S(2)}, u32[]{:S(2)}) collective-permute-start(bf16[96,2048]{1,0:T(8,128)(2,1)S(1)} %shard_map.80.left1), channel_id=1, source_target_pairs={{0,6},{1,3},{2,4},{3,1},{4,2},{5,7},{6,0},{7,5},{8,14},{9,11},{10,... | collective-permute-start | bytes 1179656 | tf_op jit(solution)/shard_map/ppermute | solution.py:242
  101.0 2.1 %collective-permute-done.11.right_ref = bf16[96,2048]{1,0:T(8,128)(2,1)S(1)} collective-permute-done((bf16[96,2048]{1,0:T(8,128)(2,1)S(1)}, bf16[96,2048]{1,0:T(8,128)(2,1)S(1)}, u32[]{:S(2)}, u32[]{:S(2)}) %collective-permute-start.11) | collective-permute-done | bytes 393248 | tf_op jit(solution)/shard_map/ppermute | solution.py:242
  103.2 2.0 %collective-permute-start.12 = (bf16[96,2048]{1,0:T(8,128)(2,1)S(1)}, bf16[96,2048]{1,0:T(8,128)(2,1)S(1)}, u32[]{:S(2)}, u32[]{:S(2)}) collective-permute-start(bf16[96,2048]{1,0:T(8,128)(2,1)S(1)} %shard_map.81.left2), channel_id=1, source_target_pairs={{0,6},{1,3},{2,4},{3,1},{4,2},{5,7},{6,0},{7,5},{8,14},{9,11},{10,... | collective-permute-start | bytes 1179656 | tf_op jit(solution)/shard_map/ppermute | solution.py:242
  105.2 2.7 %collective-permute-done.10.right1 = bf16[96,2048]{1,0:T(8,128)(2,1)S(1)} collective-permute-done((bf16[96,2048]{1,0:T(8,128)(2,1)S(1)}, bf16[96,2048]{1,0:T(8,128)(2,1)S(1)}, u32[]{:S(2)}, u32[]{:S(2)}) %collective-permute-start.10) | collective-permute-done | bytes 393248 | tf_op jit(solution)/shard_map/ppermute | solution.py:242
  107.9 4.2 %collective-permute-done.12.right2 = bf16[96,2048]{1,0:T(8,128)(2,1)S(1)} collective-permute-done((bf16[96,2048]{1,0:T(8,128)(2,1)S(1)}, bf16[96,2048]{1,0:T(8,128)(2,1)S(1)}, u32[]{:S(2)}, u32[]{:S(2)}) %collective-permute-start.12) | collective-permute-done | bytes 393248 | tf_op jit(solution)/shard_map/ppermute | solution.py:242
  112.9 4.6 %collective-permute-start.13 = (bf16[192,2048]{1,0:T(8,128)(2,1)S(1)}, bf16[192,2048]{1,0:T(8,128)(2,1)S(1)}, u32[]{:S(2)}, u32[]{:S(2)}) collective-permute-start(bf16[192,2048]{1,0:T(8,128)(2,1)S(1)} %shard_map.82.mine_ref), channel_id=1, source_target_pairs={{0,1},{1,0},{2,3},{3,2},{4,5},{5,4},{6,7},{7,6},{8,9},{9,8},{10,11... | collective-permute-start | bytes 2359304 | tf_op jit(solution)/shard_map/ppermute | solution.py:246
  117.5 0.9 shard_map.86
  118.4 6.9 %all-to-all-start.2 = ((bf16[8,32,384]{2,1,0:T(8,128)(2,1)}), bf16[8,32,384]{2,1,0:T(8,128)(2,1)S(1)}, u32[]{:S(2)}, u32[]{:S(2)}) async-start(bf16[8,32,384]{2,1,0:T(8,128)(2,1)} %bitcast.4), calls=%async_computation.2 | async-start | bytes 393216 | tf_op jit(solution)/shard_map/all_to_all | solution.py:62
  125.3 1.2 shard_map.83
  126.5 7.5 %all-to-all-done.2.parts_ref = bf16[8,32,384]{2,1,0:T(8,128)(2,1)S(1)} async-done(((bf16[8,32,384]{2,1,0:T(8,128)(2,1)}), bf16[8,32,384]{2,1,0:T(8,128)(2,1)S(1)}, u32[]{:S(2)}, u32[]{:S(2)}) %all-to-all-start.2) | async-done | bytes 196640 | tf_op jit(solution)/shard_map/all_to_all | solution.py:62
  (24 shorter events, 3.0 us)
Async XLA Ops:
  0.6 57.6 %copy-start = (bf16[384,2048]{1,0:T(8,128)(2,1)S(1)}, bf16[384,2048]{1,0:T(8,128)(2,1)}, u32[]{:S(2)}) copy-start(bf16[384,2048]{1,0:T(8,128)(2,1)} %cot_ref.3) | copy-start | bytes 4718596
  25.1 16.4 %collective-permute-start.1 = (bf16[256,1152]{1,0:T(8,128)(2,1)S(1)}, bf16[256,1152]{1,0:T(8,128)(2,1)S(1)}, u32[]{:S(2)}, u32[]{:S(2)}) collective-permute-start(bf16[256,1152]{1,0:T(8,128)(2,1)S(1)} %bitcast.6), channel_id=1, source_target_pairs={{0,128},{1,17},{2,130},{3,19},{4,132},{5,21},{6,134},{7,23},{8,136... | collective-permute-start | bytes 1769480 | tf_op jit(solution)/shard_map/ppermute | solution.py:58
  29.3 19.4 %collective-permute-start.5 = (bf16[256,1152]{1,0:T(8,128)(2,1)S(1)}, bf16[256,1152]{1,0:T(8,128)(2,1)S(1)}, u32[]{:S(2)}, u32[]{:S(2)}) collective-permute-start(bf16[256,1152]{1,0:T(8,128)(2,1)S(1)} %bitcast.7), channel_id=1, source_target_pairs={{0,384},{1,49},{2,386},{3,51},{4,388},{5,53},{6,390},{7,55},{8,392... | collective-permute-start | bytes 1769480 | tf_op jit(solution)/shard_map/ppermute | solution.py:58
  32.9 22.1 %collective-permute-start = (bf16[256,1152]{1,0:T(8,128)(2,1)S(1)}, bf16[256,1152]{1,0:T(8,128)(2,1)S(1)}, u32[]{:S(2)}, u32[]{:S(2)}) collective-permute-start(bf16[256,1152]{1,0:T(8,128)(2,1)S(1)} %bitcast.8), channel_id=1, source_target_pairs={{0,64},{1,9},{2,66},{3,11},{4,68},{5,13},{6,70},{7,15},{8,72},{9,1... | collective-permute-start | bytes 1769480 | tf_op jit(solution)/shard_map/ppermute | solution.py:58
  35.7 23.7 %collective-permute-start.4 = (bf16[256,1152]{1,0:T(8,128)(2,1)S(1)}, bf16[256,1152]{1,0:T(8,128)(2,1)S(1)}, u32[]{:S(2)}, u32[]{:S(2)}) collective-permute-start(bf16[256,1152]{1,0:T(8,128)(2,1)S(1)} %bitcast.9), channel_id=1, source_target_pairs={{0,448},{1,57},{2,450},{3,59},{4,452},{5,61},{6,454},{7,63},{8,456... | collective-permute-start | bytes 1769480 | tf_op jit(solution)/shard_map/ppermute | solution.py:58
  41.5 26.6 %collective-permute-start.2 = (bf16[256,1152]{1,0:T(8,128)(2,1)S(1)}, bf16[256,1152]{1,0:T(8,128)(2,1)S(1)}, u32[]{:S(2)}, u32[]{:S(2)}) collective-permute-start(bf16[256,1152]{1,0:T(8,128)(2,1)S(1)} %collective-permute-done.1.p2), channel_id=1, source_target_pairs={{0,64},{1,9},{2,66},{3,11},{4,68},{5,13},{6,70},{7,15},{8,72},{9,1... | collective-permute-start | bytes 1769480 | tf_op jit(solution)/shard_map/ppermute | solution.py:58
  48.7 19.4 %collective-permute-start.6 = (bf16[256,1152]{1,0:T(8,128)(2,1)S(1)}, bf16[256,1152]{1,0:T(8,128)(2,1)S(1)}, u32[]{:S(2)}, u32[]{:S(2)}) collective-permute-start(bf16[256,1152]{1,0:T(8,128)(2,1)S(1)} %collective-permute-done.5.m2), channel_id=1, source_target_pairs={{0,448},{1,57},{2,450},{3,59},{4,452},{5,61},{6,454},{7,63},{8,456... | collective-permute-start | bytes 1769480 | tf_op jit(solution)/shard_map/ppermute | solution.py:58
  50.6 10.7 %collective-permute-start.3 = (bf16[128,1152]{1,0:T(8,128)(2,1)S(1)}, bf16[128,1152]{1,0:T(8,128)(2,1)S(1)}, u32[]{:S(2)}, u32[]{:S(2)}) collective-permute-start(bf16[128,1152]{1,0:T(8,128)(2,1)S(1)} %slice.8), channel_id=1, source_target_pairs={{0,128},{1,17},{2,130},{3,19},{4,132},{5,21},{6,134},{7,23},{8,136... | collective-permute-start | bytes 884744 | tf_op jit(solution)/shard_map/ppermute | solution.py:58
  55.0 3.7 %copy-start.1 = (bf16[384,2048]{1,0:T(8,128)(2,1)S(1)}, bf16[384,2048]{1,0:T(8,128)(2,1)}, u32[]{:S(2)}) copy-start(bf16[384,2048]{1,0:T(8,128)(2,1)} %x_ref.1) | copy-start | bytes 4718596
  55.0 3.7 %copy-start.2 = (f32[2048]{0:T(1024)S(1)}, f32[2048]{0:T(1024)}, u32[]{:S(2)}) copy-start(f32[2048]{0:T(1024)} %param.7) | copy-start | bytes 24580
  55.0 13.0 %collective-permute-start.7 = (bf16[128,1152]{1,0:T(8,128)(2,1)S(1)}, bf16[128,1152]{1,0:T(8,128)(2,1)S(1)}, u32[]{:S(2)}, u32[]{:S(2)}) collective-permute-start(bf16[128,1152]{1,0:T(8,128)(2,1)S(1)} %slice.9), channel_id=1, source_target_pairs={{0,384},{1,49},{2,386},{3,51},{4,388},{5,53},{6,390},{7,55},{8,392... | collective-permute-start | bytes 884744 | tf_op jit(solution)/shard_map/ppermute | solution.py:58
  72.8 2.3 %copy-start.3 = (bf16[192,2048]{1,0:T(8,128)(2,1)}, bf16[192,2048]{1,0:T(8,128)(2,1)S(1)}, u32[]{:S(2)}) copy-start(bf16[192,2048]{1,0:T(8,128)(2,1)S(1)} %get-tuple-element.12) | copy-start | bytes 2359300
  75.0 42.5 %all-to-all-start.1 = ((bf16[8,256,384]{2,1,0:T(8,128)(2,1)}), bf16[8,256,384]{2,1,0:T(8,128)(2,1)S(1)}, u32[]{:S(2)}, u32[]{:S(2)}) async-start(bf16[8,256,384]{2,1,0:T(8,128)(2,1)} %bitcast.3), calls=%async_computation.1 | async-start | bytes 3145728 | tf_op jit(solution)/shard_map/all_to_all | solution.py:62
  79.4 9.4 %collective-permute-start.8 = (bf16[192,2048]{1,0:T(8,128)(2,1)}, bf16[192,2048]{1,0:T(8,128)(2,1)S(1)}, u32[]{:S(2)}, u32[]{:S(2)}) collective-permute-start(bf16[192,2048]{1,0:T(8,128)(2,1)} %copy-done.3), channel_id=1, source_target_pairs={{0,1},{1,0},{2,3},{3,2},{4,5},{5,4},{6,7},{7,6},{8,9},{9,8},{10,11... | collective-permute-start | bytes 2359304 | tf_op jit(solution)/shard_map/ppermute | solution.py:246
  89.0 10.0 %collective-permute-start.9 = (bf16[96,2048]{1,0:T(8,128)(2,1)S(1)}, bf16[96,2048]{1,0:T(8,128)(2,1)S(1)}, u32[]{:S(2)}, u32[]{:S(2)}) collective-permute-start(bf16[96,2048]{1,0:T(8,128)(2,1)S(1)} %get-tuple-element.13.left_ref), channel_id=1, source_target_pairs={{0,2},{1,7},{2,0},{3,5},{4,6},{5,3},{6,4},{7,1},{8,10},{9,15},{10,... | collective-permute-start | bytes 1179656 | tf_op jit(solution)/shard_map/ppermute | solution.py:242
  93.4 9.7 %collective-permute-start.11 = (bf16[96,2048]{1,0:T(8,128)(2,1)S(1)}, bf16[96,2048]{1,0:T(8,128)(2,1)S(1)}, u32[]{:S(2)}, u32[]{:S(2)}) collective-permute-start(bf16[96,2048]{1,0:T(8,128)(2,1)S(1)} %get-tuple-element.14.left_ref), channel_id=1, source_target_pairs={{0,2},{1,7},{2,0},{3,5},{4,6},{5,3},{6,4},{7,1},{8,10},{9,15},{10,... | collective-permute-start | bytes 1179656 | tf_op jit(solution)/shard_map/ppermute | solution.py:242
  99.1 8.8 %collective-permute-start.10 = (bf16[96,2048]{1,0:T(8,128)(2,1)S(1)}, bf16[96,2048]{1,0:T(8,128)(2,1)S(1)}, u32[]{:S(2)}, u32[]{:S(2)}) collective-permute-start(bf16[96,2048]{1,0:T(8,128)(2,1)S(1)} %shard_map.80.left1), channel_id=1, source_target_pairs={{0,6},{1,3},{2,4},{3,1},{4,2},{5,7},{6,0},{7,5},{8,14},{9,11},{10,... | collective-permute-start | bytes 1179656 | tf_op jit(solution)/shard_map/ppermute | solution.py:242
  103.2 8.9 %collective-permute-start.12 = (bf16[96,2048]{1,0:T(8,128)(2,1)S(1)}, bf16[96,2048]{1,0:T(8,128)(2,1)S(1)}, u32[]{:S(2)}, u32[]{:S(2)}) collective-permute-start(bf16[96,2048]{1,0:T(8,128)(2,1)S(1)} %shard_map.81.left2), channel_id=1, source_target_pairs={{0,6},{1,3},{2,4},{3,1},{4,2},{5,7},{6,0},{7,5},{8,14},{9,11},{10,... | collective-permute-start | bytes 1179656 | tf_op jit(solution)/shard_map/ppermute | solution.py:242
  112.9 12.4 %collective-permute-start.13 = (bf16[192,2048]{1,0:T(8,128)(2,1)S(1)}, bf16[192,2048]{1,0:T(8,128)(2,1)S(1)}, u32[]{:S(2)}, u32[]{:S(2)}) collective-permute-start(bf16[192,2048]{1,0:T(8,128)(2,1)S(1)} %shard_map.82.mine_ref), channel_id=1, source_target_pairs={{0,1},{1,0},{2,3},{3,2},{4,5},{5,4},{6,7},{7,6},{8,9},{9,8},{10,11... | collective-permute-start | bytes 2359304 | tf_op jit(solution)/shard_map/ppermute | solution.py:246
  118.4 15.6 %all-to-all-start.2 = ((bf16[8,32,384]{2,1,0:T(8,128)(2,1)}), bf16[8,32,384]{2,1,0:T(8,128)(2,1)S(1)}, u32[]{:S(2)}, u32[]{:S(2)}) async-start(bf16[8,32,384]{2,1,0:T(8,128)(2,1)} %bitcast.4), calls=%async_computation.2 | async-start | bytes 393216 | tf_op jit(solution)/shard_map/all_to_all | solution.py:62

commit v5 on v4

--- a/solution.py
+++ b/solution.py
@@ -130,9 +130,19 @@
             turned_ref[rows, :] = block[y * 32 : (y + 1) * 32, :]
 
 
-def down_kernel(turned_ref, hidden_ref, down_ref):
-    down = HALF_STEP * dot(turned_ref[...], hidden_ref[...], ((1,), (0,)))
-    down_ref[...] = down.astype(jnp.bfloat16)
+def down_kernel(turned_ref, hidden_ref, down_ref, staged_ref, sems):
+    hidden = hidden_ref[...]
+    copies = []
+    for q in range(8):
+        block = pl.ds(q * 256, 256)
+        down = HALF_STEP * dot(turned_ref[block, :], hidden, ((1,), (0,)))
+        staged_ref[block, :] = down.astype(jnp.bfloat16)
+        copies.append(
+            pltpu.make_async_copy(staged_ref.at[block, :], down_ref.at[block, :], sems.at[q])
+        )
+        copies[-1].start()
+    for copy in copies:
+        copy.wait()
 
 
 def vmem_specs(count):
@@ -169,14 +179,25 @@
     )(normed, cotangent, *blocks)
 
 
-def one_call(kernel, out_shape, *operands):
-    return pl.pallas_call(
-        kernel,
-        out_shape=out_shape,
-        in_specs=vmem_specs(len(operands)),
+def turn(cotangent):
+    return pl.pallas_call(
+        turn_kernel,
+        out_shape=jax.ShapeDtypeStruct((D, TOK), jnp.bfloat16),
+        in_specs=vmem_specs(1),
         out_specs=vmem_specs(1)[0],
+        compiler_params=pltpu.CompilerParams(vmem_limit_bytes=SMALL_LIMIT),
+    )(cotangent)
+
+
+def down_product(turned, hidden):
+    return pl.pallas_call(
+        down_kernel,
+        out_shape=jax.ShapeDtypeStruct((D, HP), jnp.bfloat16),
+        in_specs=vmem_specs(2),
+        out_specs=pl.BlockSpec(memory_space=pltpu.HBM),
+        scratch_shapes=[pltpu.VMEM((D, HP), jnp.bfloat16), pltpu.SemaphoreType.DMA((8,))],
         compiler_params=pltpu.CompilerParams(vmem_limit_bytes=DOWN_LIMIT),
-    )(*operands)
+    )(turned, hidden)
 
 
 def pair_kernel(left_ref, right_ref, *out_refs):
@@ -265,12 +286,10 @@
     normed, x_half = small_call(
         normalize_kernel, [jax.ShapeDtypeStruct((TOK, D), jnp.bfloat16), half], inputs, row
     )
-    turned = one_call(turn_kernel, jax.ShapeDtypeStruct((D, TOK), jnp.bfloat16), cotangent)
+    turned = turn(cotangent)
     keep, send, hidden = compute(normed, cotangent, (b0, p1, p2, p3, p4, m1, m2, m3, m4))
     other = with_core(send)
-    down = one_call(
-        down_kernel, jax.ShapeDtypeStruct((D, HP), jnp.bfloat16), turned, hidden
-    )
+    down = down_product(turned, hidden)
     arrived = exchange(down.reshape(8, 256, HP), True)
     (line,) = small_call(sum_kernel, [jax.ShapeDtypeStruct((256, HP), jnp.bfloat16)], arrived)
     arrived = exchange(line.reshape(8, DROWS, HP), False)

time: 135 us -> 135 us (level)
  no operation moved by 1% of the time
where the time goes in v5:
time: 135 us; the launch traced here: 134 us
  starting transfers between devices  63.3 us (47%)
  waiting for transfers between devices  34.1 us (25%)
  blocking collectives  23.5 us (17%)
  Pallas kernels  11.5 us (9%)
    ppermute x8, starting transfers between devices, ring(): return lax.ppermute(array, AXES, ring_pairs(step))  29.7 us
    all_to_all x1, blocking collectives, exchange(): lax.all_to_all(array, AXES, 0, 0, axis_index_groups=line_groups(along_rin...  23.5 us
    ppermute x4, waiting for transfers between devices, with_partner(): return lax.ppermute(array, AXES, pairs)  12.5 us
    ppermute x8, waiting for transfers between devices, ring(): return lax.ppermute(array, AXES, ring_pairs(step))  12 us
    ppermute x2, starting transfers between devices, with_core(): return lax.ppermute(array, 'c', [(0, 1), (1, 0)])  11.9 us
    all_to_all x2, starting transfers between devices, exchange(): lax.all_to_all(array, AXES, 0, 0, axis_index_groups=line_groups(along_rin...  11.3 us
    ppermute x4, starting transfers between devices, with_partner(): return lax.ppermute(array, AXES, pairs)  10.4 us
    all_to_all x2, waiting for transfers between devices, exchange(): lax.all_to_all(array, AXES, 0, 0, axis_index_groups=line_groups(along_rin...  7.46 us
  transfers between devices with their start and end apart: 16, of which 10 were waited for; matrix products, arithmetic and copies ran while one was open for 0% of the time, Pallas kernels for 3%

profile of v5, /device:TPU:1, one launch (start us, length us, event | category | flops | bytes accessed | tf_op | source)
XLA Modules:
  0.0 134.2 jit_solution(14724057479935180508)
XLA Ops:
  0.6 0.9 fusion.5
  1.6 23.5 %all_to_all.15 = bf16[8,32,1152]{2,1,0:T(8,128)(2,1)S(1)} all-to-all(bf16[8,32,1152]{2,1,0:T(8,128)(2,1)S(1)} %broadcast_in_dim.2), channel_id=1, replica_groups={{0,8,16,24,32,40,48,56},{64,72,80,88,96,104,112,120},{128,136,144,152,1..., dimensions={0} | all-to-all | bytes 1179648 | tf_op jit(solution)/shard_map/all_to_all | solution.py:62
  25.1 4.2 %collective-permute-start.1 = (bf16[256,1152]{1,0:T(8,128)(2,1)S(1)}, bf16[256,1152]{1,0:T(8,128)(2,1)S(1)}, u32[]{:S(2)}, u32[]{:S(2)}) collective-permute-start(bf16[256,1152]{1,0:T(8,128)(2,1)S(1)} %bitcast.6), channel_id=1, source_target_pairs={{0,128},{1,17},{2,130},{3,19},{4,132},{5,21},{6,134},{7,23},{8,136... | collective-permute-start | bytes 1769480 | tf_op jit(solution)/shard_map/ppermute | solution.py:58
  29.3 3.6 %collective-permute-start.5 = (bf16[256,1152]{1,0:T(8,128)(2,1)S(1)}, bf16[256,1152]{1,0:T(8,128)(2,1)S(1)}, u32[]{:S(2)}, u32[]{:S(2)}) collective-permute-start(bf16[256,1152]{1,0:T(8,128)(2,1)S(1)} %bitcast.7), channel_id=1, source_target_pairs={{0,384},{1,49},{2,386},{3,51},{4,388},{5,53},{6,390},{7,55},{8,392... | collective-permute-start | bytes 1769480 | tf_op jit(solution)/shard_map/ppermute | solution.py:58
  32.9 2.8 %collective-permute-start = (bf16[256,1152]{1,0:T(8,128)(2,1)S(1)}, bf16[256,1152]{1,0:T(8,128)(2,1)S(1)}, u32[]{:S(2)}, u32[]{:S(2)}) collective-permute-start(bf16[256,1152]{1,0:T(8,128)(2,1)S(1)} %bitcast.8), channel_id=1, source_target_pairs={{0,64},{1,9},{2,66},{3,11},{4,68},{5,13},{6,70},{7,15},{8,72},{9,1... | collective-permute-start | bytes 1769480 | tf_op jit(solution)/shard_map/ppermute | solution.py:58
  35.7 3.7 %collective-permute-start.4 = (bf16[256,1152]{1,0:T(8,128)(2,1)S(1)}, bf16[256,1152]{1,0:T(8,128)(2,1)S(1)}, u32[]{:S(2)}, u32[]{:S(2)}) collective-permute-start(bf16[256,1152]{1,0:T(8,128)(2,1)S(1)} %bitcast.9), channel_id=1, source_target_pairs={{0,448},{1,57},{2,450},{3,59},{4,452},{5,61},{6,454},{7,63},{8,456... | collective-permute-start | bytes 1769480 | tf_op jit(solution)/shard_map/ppermute | solution.py:58
  39.4 2.1 %collective-permute-done.1.p2 = bf16[256,1152]{1,0:T(8,128)(2,1)S(1)} collective-permute-done((bf16[256,1152]{1,0:T(8,128)(2,1)S(1)}, bf16[256,1152]{1,0:T(8,128)(2,1)S(1)}, u32[]{:S(2)}, u32[]{:S(2)}) %collective-permute-start.1) | collective-permute-done | bytes 589856 | tf_op jit(solution)/shard_map/ppermute | solution.py:58
  41.5 5.9 %collective-permute-start.2 = (bf16[256,1152]{1,0:T(8,128)(2,1)S(1)}, bf16[256,1152]{1,0:T(8,128)(2,1)S(1)}, u32[]{:S(2)}, u32[]{:S(2)}) collective-permute-start(bf16[256,1152]{1,0:T(8,128)(2,1)S(1)} %collective-permute-done.1.p2), channel_id=1, source_target_pairs={{0,64},{1,9},{2,66},{3,11},{4,68},{5,13},{6,70},{7,15},{8,72},{9,1... | collective-permute-start | bytes 1769480 | tf_op jit(solution)/shard_map/ppermute | solution.py:58
  47.4 1.2 collective-permute-done.5.m2
  48.7 1.9 %collective-permute-start.6 = (bf16[256,1152]{1,0:T(8,128)(2,1)S(1)}, bf16[256,1152]{1,0:T(8,128)(2,1)S(1)}, u32[]{:S(2)}, u32[]{:S(2)}) collective-permute-start(bf16[256,1152]{1,0:T(8,128)(2,1)S(1)} %collective-permute-done.5.m2), channel_id=1, source_target_pairs={{0,448},{1,57},{2,450},{3,59},{4,452},{5,61},{6,454},{7,63},{8,456... | collective-permute-start | bytes 1769480 | tf_op jit(solution)/shard_map/ppermute | solution.py:58
  50.6 4.4 %collective-permute-start.3 = (bf16[128,1152]{1,0:T(8,128)(2,1)S(1)}, bf16[128,1152]{1,0:T(8,128)(2,1)S(1)}, u32[]{:S(2)}, u32[]{:S(2)}) collective-permute-start(bf16[128,1152]{1,0:T(8,128)(2,1)S(1)} %slice.8), channel_id=1, source_target_pairs={{0,128},{1,17},{2,130},{3,19},{4,132},{5,21},{6,134},{7,23},{8,136... | collective-permute-start | bytes 884744 | tf_op jit(solution)/shard_map/ppermute | solution.py:58
  55.0 3.2 %collective-permute-start.7 = (bf16[128,1152]{1,0:T(8,128)(2,1)S(1)}, bf16[128,1152]{1,0:T(8,128)(2,1)S(1)}, u32[]{:S(2)}, u32[]{:S(2)}) collective-permute-start(bf16[128,1152]{1,0:T(8,128)(2,1)S(1)} %slice.9), channel_id=1, source_target_pairs={{0,384},{1,49},{2,386},{3,51},{4,388},{5,53},{6,390},{7,55},{8,392... | collective-permute-start | bytes 884744 | tf_op jit(solution)/shard_map/ppermute | solution.py:58
  59.4 2.0 %collective-permute-done.3.p4 = bf16[128,1152]{1,0:T(8,128)(2,1)S(1)} collective-permute-done((bf16[128,1152]{1,0:T(8,128)(2,1)S(1)}, bf16[128,1152]{1,0:T(8,128)(2,1)S(1)}, u32[]{:S(2)}, u32[]{:S(2)}) %collective-permute-start.3) | collective-permute-done | bytes 294944 | tf_op jit(solution)/shard_map/ppermute | solution.py:58
  61.3 6.7 %collective-permute-done.7.m4 = bf16[128,1152]{1,0:T(8,128)(2,1)S(1)} collective-permute-done((bf16[128,1152]{1,0:T(8,128)(2,1)S(1)}, bf16[128,1152]{1,0:T(8,128)(2,1)S(1)}, u32[]{:S(2)}, u32[]{:S(2)}) %collective-permute-start.7) | collective-permute-done | bytes 294944 | tf_op jit(solution)/shard_map/ppermute | solution.py:58
  68.1 4.7 %shard_map.78 = (bf16[192,2048]{1,0:T(8,128)(2,1)S(1)}, bf16[192,2048]{1,0:T(8,128)(2,1)S(1)}, bf16[384,384]{1,0:T(8,128)(2,1)S(1)}) custom-call(bf16[384,2048]{1,0:T(8,128)(2,1)S(1)} %get-tuple-element.10.norm_ref, bf16[384,2048]{1,0:T(8,128)(2,1)S(1)} %copy-done, bf16[256,1152]{1,0:T(8,128)(2,1)S(1)} %bitcast.10, ...), custom_call_target="tpu_custom_call" | custom-call | tf_op jit(solution)/shard_map/pallas_call | solution.py:165
  72.8 1.9 %shard_map.85 = bf16[2048,384]{1,0:T(8,128)(2,1)} custom-call(bf16[2048,384]{1,0:T(8,128)(2,1)S(1)} %shard_map.84.turned_ref, bf16[384,384]{1,0:T(8,128)(2,1)S(1)} %get-tuple-element.15.hidden_ref), custom_call_target="tpu_custom_call" | custom-call | tf_op jit(solution)/shard_map/pallas_call | solution.py:193
  74.7 4.4 %all-to-all-start.1 = ((bf16[8,256,384]{2,1,0:T(8,128)(2,1)}), bf16[8,256,384]{2,1,0:T(8,128)(2,1)S(1)}, u32[]{:S(2)}, u32[]{:S(2)}) async-start(bf16[8,256,384]{2,1,0:T(8,128)(2,1)} %bitcast.3), calls=%async_computation.1 | async-start | bytes 3145728 | tf_op jit(solution)/shard_map/all_to_all | solution.py:62
  79.0 7.3 %collective-permute-start.8 = (bf16[192,2048]{1,0:T(8,128)(2,1)}, bf16[192,2048]{1,0:T(8,128)(2,1)S(1)}, u32[]{:S(2)}, u32[]{:S(2)}) collective-permute-start(bf16[192,2048]{1,0:T(8,128)(2,1)} %copy-done.3), channel_id=1, source_target_pairs={{0,1},{1,0},{2,3},{3,2},{4,5},{5,4},{6,7},{7,6},{8,9},{9,8},{10,11... | collective-permute-start | bytes 2359304 | tf_op jit(solution)/shard_map/ppermute | solution.py:267
  86.3 2.1 %collective-permute-done.8.right_ref = bf16[192,2048]{1,0:T(8,128)(2,1)S(1)} collective-permute-done((bf16[192,2048]{1,0:T(8,128)(2,1)}, bf16[192,2048]{1,0:T(8,128)(2,1)S(1)}, u32[]{:S(2)}, u32[]{:S(2)}) %collective-permute-start.8) | collective-permute-done | bytes 786464 | tf_op jit(solution)/shard_map/ppermute | solution.py:267
  88.6 4.4 %collective-permute-start.9 = (bf16[96,2048]{1,0:T(8,128)(2,1)S(1)}, bf16[96,2048]{1,0:T(8,128)(2,1)S(1)}, u32[]{:S(2)}, u32[]{:S(2)}) collective-permute-start(bf16[96,2048]{1,0:T(8,128)(2,1)S(1)} %get-tuple-element.13.left_ref), channel_id=1, source_target_pairs={{0,2},{1,7},{2,0},{3,5},{4,6},{5,3},{6,4},{7,1},{8,10},{9,15},{10,... | collective-permute-start | bytes 1179656 | tf_op jit(solution)/shard_map/ppermute | solution.py:263
  93.0 2.1 %collective-permute-start.11 = (bf16[96,2048]{1,0:T(8,128)(2,1)S(1)}, bf16[96,2048]{1,0:T(8,128)(2,1)S(1)}, u32[]{:S(2)}, u32[]{:S(2)}) collective-permute-start(bf16[96,2048]{1,0:T(8,128)(2,1)S(1)} %get-tuple-element.14.left_ref), channel_id=1, source_target_pairs={{0,2},{1,7},{2,0},{3,5},{4,6},{5,3},{6,4},{7,1},{8,10},{9,15},{10,... | collective-permute-start | bytes 1179656 | tf_op jit(solution)/shard_map/ppermute | solution.py:263
  95.1 3.5 %collective-permute-done.9.right_ref = bf16[96,2048]{1,0:T(8,128)(2,1)S(1)} collective-permute-done((bf16[96,2048]{1,0:T(8,128)(2,1)S(1)}, bf16[96,2048]{1,0:T(8,128)(2,1)S(1)}, u32[]{:S(2)}, u32[]{:S(2)}) %collective-permute-start.9) | collective-permute-done | bytes 393248 | tf_op jit(solution)/shard_map/ppermute | solution.py:263
  98.8 1.9 %collective-permute-start.10 = (bf16[96,2048]{1,0:T(8,128)(2,1)S(1)}, bf16[96,2048]{1,0:T(8,128)(2,1)S(1)}, u32[]{:S(2)}, u32[]{:S(2)}) collective-permute-start(bf16[96,2048]{1,0:T(8,128)(2,1)S(1)} %shard_map.80.left1), channel_id=1, source_target_pairs={{0,6},{1,3},{2,4},{3,1},{4,2},{5,7},{6,0},{7,5},{8,14},{9,11},{10,... | collective-permute-start | bytes 1179656 | tf_op jit(solution)/shard_map/ppermute | solution.py:263
  100.7 2.1 %collective-permute-done.11.right_ref = bf16[96,2048]{1,0:T(8,128)(2,1)S(1)} collective-permute-done((bf16[96,2048]{1,0:T(8,128)(2,1)S(1)}, bf16[96,2048]{1,0:T(8,128)(2,1)S(1)}, u32[]{:S(2)}, u32[]{:S(2)}) %collective-permute-start.11) | collective-permute-done | bytes 393248 | tf_op jit(solution)/shard_map/ppermute | solution.py:263
  102.9 2.0 %collective-permute-start.12 = (bf16[96,2048]{1,0:T(8,128)(2,1)S(1)}, bf16[96,2048]{1,0:T(8,128)(2,1)S(1)}, u32[]{:S(2)}, u32[]{:S(2)}) collective-permute-start(bf16[96,2048]{1,0:T(8,128)(2,1)S(1)} %shard_map.81.left2), channel_id=1, source_target_pairs={{0,6},{1,3},{2,4},{3,1},{4,2},{5,7},{6,0},{7,5},{8,14},{9,11},{10,... | collective-permute-start | bytes 1179656 | tf_op jit(solution)/shard_map/ppermute | solution.py:263
  104.9 2.7 %collective-permute-done.10.right1 = bf16[96,2048]{1,0:T(8,128)(2,1)S(1)} collective-permute-done((bf16[96,2048]{1,0:T(8,128)(2,1)S(1)}, bf16[96,2048]{1,0:T(8,128)(2,1)S(1)}, u32[]{:S(2)}, u32[]{:S(2)}) %collective-permute-start.10) | collective-permute-done | bytes 393248 | tf_op jit(solution)/shard_map/ppermute | solution.py:263
  107.6 4.2 %collective-permute-done.12.right2 = bf16[96,2048]{1,0:T(8,128)(2,1)S(1)} collective-permute-done((bf16[96,2048]{1,0:T(8,128)(2,1)S(1)}, bf16[96,2048]{1,0:T(8,128)(2,1)S(1)}, u32[]{:S(2)}, u32[]{:S(2)}) %collective-permute-start.12) | collective-permute-done | bytes 393248 | tf_op jit(solution)/shard_map/ppermute | solution.py:263
  112.6 4.6 %collective-permute-start.13 = (bf16[192,2048]{1,0:T(8,128)(2,1)S(1)}, bf16[192,2048]{1,0:T(8,128)(2,1)S(1)}, u32[]{:S(2)}, u32[]{:S(2)}) collective-permute-start(bf16[192,2048]{1,0:T(8,128)(2,1)S(1)} %shard_map.82.mine_ref), channel_id=1, source_target_pairs={{0,1},{1,0},{2,3},{3,2},{4,5},{5,4},{6,7},{7,6},{8,9},{9,8},{10,11... | collective-permute-start | bytes 2359304 | tf_op jit(solution)/shard_map/ppermute | solution.py:267
  117.1 0.9 shard_map.86
  118.0 6.9 %all-to-all-start.2 = ((bf16[8,32,384]{2,1,0:T(8,128)(2,1)}), bf16[8,32,384]{2,1,0:T(8,128)(2,1)S(1)}, u32[]{:S(2)}, u32[]{:S(2)}) async-start(bf16[8,32,384]{2,1,0:T(8,128)(2,1)} %bitcast.4), calls=%async_computation.2 | async-start | bytes 393216 | tf_op jit(solution)/shard_map/all_to_all | solution.py:62
  125.0 1.2 shard_map.83
  126.1 7.5 %all-to-all-done.2.parts_ref = bf16[8,32,384]{2,1,0:T(8,128)(2,1)S(1)} async-done(((bf16[8,32,384]{2,1,0:T(8,128)(2,1)}), bf16[8,32,384]{2,1,0:T(8,128)(2,1)S(1)}, u32[]{:S(2)}, u32[]{:S(2)}) %all-to-all-start.2) | async-done | bytes 196640 | tf_op jit(solution)/shard_map/all_to_all | solution.py:62
  (24 shorter events, 3.0 us)
Async XLA Ops:
  0.6 57.6 %copy-start = (bf16[384,2048]{1,0:T(8,128)(2,1)S(1)}, bf16[384,2048]{1,0:T(8,128)(2,1)}, u32[]{:S(2)}) copy-start(bf16[384,2048]{1,0:T(8,128)(2,1)} %cot_ref.3) | copy-start | bytes 4718596
  25.1 16.4 %collective-permute-start.1 = (bf16[256,1152]{1,0:T(8,128)(2,1)S(1)}, bf16[256,1152]{1,0:T(8,128)(2,1)S(1)}, u32[]{:S(2)}, u32[]{:S(2)}) collective-permute-start(bf16[256,1152]{1,0:T(8,128)(2,1)S(1)} %bitcast.6), channel_id=1, source_target_pairs={{0,128},{1,17},{2,130},{3,19},{4,132},{5,21},{6,134},{7,23},{8,136... | collective-permute-start | bytes 1769480 | tf_op jit(solution)/shard_map/ppermute | solution.py:58
  29.3 19.4 %collective-permute-start.5 = (bf16[256,1152]{1,0:T(8,128)(2,1)S(1)}, bf16[256,1152]{1,0:T(8,128)(2,1)S(1)}, u32[]{:S(2)}, u32[]{:S(2)}) collective-permute-start(bf16[256,1152]{1,0:T(8,128)(2,1)S(1)} %bitcast.7), channel_id=1, source_target_pairs={{0,384},{1,49},{2,386},{3,51},{4,388},{5,53},{6,390},{7,55},{8,392... | collective-permute-start | bytes 1769480 | tf_op jit(solution)/shard_map/ppermute | solution.py:58
  32.9 22.1 %collective-permute-start = (bf16[256,1152]{1,0:T(8,128)(2,1)S(1)}, bf16[256,1152]{1,0:T(8,128)(2,1)S(1)}, u32[]{:S(2)}, u32[]{:S(2)}) collective-permute-start(bf16[256,1152]{1,0:T(8,128)(2,1)S(1)} %bitcast.8), channel_id=1, source_target_pairs={{0,64},{1,9},{2,66},{3,11},{4,68},{5,13},{6,70},{7,15},{8,72},{9,1... | collective-permute-start | bytes 1769480 | tf_op jit(solution)/shard_map/ppermute | solution.py:58
  35.7 23.7 %collective-permute-start.4 = (bf16[256,1152]{1,0:T(8,128)(2,1)S(1)}, bf16[256,1152]{1,0:T(8,128)(2,1)S(1)}, u32[]{:S(2)}, u32[]{:S(2)}) collective-permute-start(bf16[256,1152]{1,0:T(8,128)(2,1)S(1)} %bitcast.9), channel_id=1, source_target_pairs={{0,448},{1,57},{2,450},{3,59},{4,452},{5,61},{6,454},{7,63},{8,456... | collective-permute-start | bytes 1769480 | tf_op jit(solution)/shard_map/ppermute | solution.py:58
  41.5 26.6 %collective-permute-start.2 = (bf16[256,1152]{1,0:T(8,128)(2,1)S(1)}, bf16[256,1152]{1,0:T(8,128)(2,1)S(1)}, u32[]{:S(2)}, u32[]{:S(2)}) collective-permute-start(bf16[256,1152]{1,0:T(8,128)(2,1)S(1)} %collective-permute-done.1.p2), channel_id=1, source_target_pairs={{0,64},{1,9},{2,66},{3,11},{4,68},{5,13},{6,70},{7,15},{8,72},{9,1... | collective-permute-start | bytes 1769480 | tf_op jit(solution)/shard_map/ppermute | solution.py:58
  48.7 19.4 %collective-permute-start.6 = (bf16[256,1152]{1,0:T(8,128)(2,1)S(1)}, bf16[256,1152]{1,0:T(8,128)(2,1)S(1)}, u32[]{:S(2)}, u32[]{:S(2)}) collective-permute-start(bf16[256,1152]{1,0:T(8,128)(2,1)S(1)} %collective-permute-done.5.m2), channel_id=1, source_target_pairs={{0,448},{1,57},{2,450},{3,59},{4,452},{5,61},{6,454},{7,63},{8,456... | collective-permute-start | bytes 1769480 | tf_op jit(solution)/shard_map/ppermute | solution.py:58
  50.6 10.7 %collective-permute-start.3 = (bf16[128,1152]{1,0:T(8,128)(2,1)S(1)}, bf16[128,1152]{1,0:T(8,128)(2,1)S(1)}, u32[]{:S(2)}, u32[]{:S(2)}) collective-permute-start(bf16[128,1152]{1,0:T(8,128)(2,1)S(1)} %slice.8), channel_id=1, source_target_pairs={{0,128},{1,17},{2,130},{3,19},{4,132},{5,21},{6,134},{7,23},{8,136... | collective-permute-start | bytes 884744 | tf_op jit(solution)/shard_map/ppermute | solution.py:58
  55.0 3.7 %copy-start.1 = (bf16[384,2048]{1,0:T(8,128)(2,1)S(1)}, bf16[384,2048]{1,0:T(8,128)(2,1)}, u32[]{:S(2)}) copy-start(bf16[384,2048]{1,0:T(8,128)(2,1)} %x_ref.1) | copy-start | bytes 4718596
  55.0 3.7 %copy-start.2 = (f32[2048]{0:T(1024)S(1)}, f32[2048]{0:T(1024)}, u32[]{:S(2)}) copy-start(f32[2048]{0:T(1024)} %param.7) | copy-start | bytes 24580
  55.0 13.0 %collective-permute-start.7 = (bf16[128,1152]{1,0:T(8,128)(2,1)S(1)}, bf16[128,1152]{1,0:T(8,128)(2,1)S(1)}, u32[]{:S(2)}, u32[]{:S(2)}) collective-permute-start(bf16[128,1152]{1,0:T(8,128)(2,1)S(1)} %slice.9), channel_id=1, source_target_pairs={{0,384},{1,49},{2,386},{3,51},{4,388},{5,53},{6,390},{7,55},{8,392... | collective-permute-start | bytes 884744 | tf_op jit(solution)/shard_map/ppermute | solution.py:58
  72.8 1.9 %copy-start.3 = (bf16[192,2048]{1,0:T(8,128)(2,1)}, bf16[192,2048]{1,0:T(8,128)(2,1)S(1)}, u32[]{:S(2)}) copy-start(bf16[192,2048]{1,0:T(8,128)(2,1)S(1)} %get-tuple-element.12) | copy-start | bytes 2359300
  74.7 42.5 %all-to-all-start.1 = ((bf16[8,256,384]{2,1,0:T(8,128)(2,1)}), bf16[8,256,384]{2,1,0:T(8,128)(2,1)S(1)}, u32[]{:S(2)}, u32[]{:S(2)}) async-start(bf16[8,256,384]{2,1,0:T(8,128)(2,1)} %bitcast.3), calls=%async_computation.1 | async-start | bytes 3145728 | tf_op jit(solution)/shard_map/all_to_all | solution.py:62
  79.0 9.4 %collective-permute-start.8 = (bf16[192,2048]{1,0:T(8,128)(2,1)}, bf16[192,2048]{1,0:T(8,128)(2,1)S(1)}, u32[]{:S(2)}, u32[]{:S(2)}) collective-permute-start(bf16[192,2048]{1,0:T(8,128)(2,1)} %copy-done.3), channel_id=1, source_target_pairs={{0,1},{1,0},{2,3},{3,2},{4,5},{5,4},{6,7},{7,6},{8,9},{9,8},{10,11... | collective-permute-start | bytes 2359304 | tf_op jit(solution)/shard_map/ppermute | solution.py:267
  88.6 10.0 %collective-permute-start.9 = (bf16[96,2048]{1,0:T(8,128)(2,1)S(1)}, bf16[96,2048]{1,0:T(8,128)(2,1)S(1)}, u32[]{:S(2)}, u32[]{:S(2)}) collective-permute-start(bf16[96,2048]{1,0:T(8,128)(2,1)S(1)} %get-tuple-element.13.left_ref), channel_id=1, source_target_pairs={{0,2},{1,7},{2,0},{3,5},{4,6},{5,3},{6,4},{7,1},{8,10},{9,15},{10,... | collective-permute-start | bytes 1179656 | tf_op jit(solution)/shard_map/ppermute | solution.py:263
  93.0 9.7 %collective-permute-start.11 = (bf16[96,2048]{1,0:T(8,128)(2,1)S(1)}, bf16[96,2048]{1,0:T(8,128)(2,1)S(1)}, u32[]{:S(2)}, u32[]{:S(2)}) collective-permute-start(bf16[96,2048]{1,0:T(8,128)(2,1)S(1)} %get-tuple-element.14.left_ref), channel_id=1, source_target_pairs={{0,2},{1,7},{2,0},{3,5},{4,6},{5,3},{6,4},{7,1},{8,10},{9,15},{10,... | collective-permute-start | bytes 1179656 | tf_op jit(solution)/shard_map/ppermute | solution.py:263
  98.8 8.8 %collective-permute-start.10 = (bf16[96,2048]{1,0:T(8,128)(2,1)S(1)}, bf16[96,2048]{1,0:T(8,128)(2,1)S(1)}, u32[]{:S(2)}, u32[]{:S(2)}) collective-permute-start(bf16[96,2048]{1,0:T(8,128)(2,1)S(1)} %shard_map.80.left1), channel_id=1, source_target_pairs={{0,6},{1,3},{2,4},{3,1},{4,2},{5,7},{6,0},{7,5},{8,14},{9,11},{10,... | collective-permute-start | bytes 1179656 | tf_op jit(solution)/shard_map/ppermute | solution.py:263
  102.9 8.9 %collective-permute-start.12 = (bf16[96,2048]{1,0:T(8,128)(2,1)S(1)}, bf16[96,2048]{1,0:T(8,128)(2,1)S(1)}, u32[]{:S(2)}, u32[]{:S(2)}) collective-permute-start(bf16[96,2048]{1,0:T(8,128)(2,1)S(1)} %shard_map.81.left2), channel_id=1, source_target_pairs={{0,6},{1,3},{2,4},{3,1},{4,2},{5,7},{6,0},{7,5},{8,14},{9,11},{10,... | collective-permute-start | bytes 1179656 | tf_op jit(solution)/shard_map/ppermute | solution.py:263
  112.6 12.4 %collective-permute-start.13 = (bf16[192,2048]{1,0:T(8,128)(2,1)S(1)}, bf16[192,2048]{1,0:T(8,128)(2,1)S(1)}, u32[]{:S(2)}, u32[]{:S(2)}) collective-permute-start(bf16[192,2048]{1,0:T(8,128)(2,1)S(1)} %shard_map.82.mine_ref), channel_id=1, source_target_pairs={{0,1},{1,0},{2,3},{3,2},{4,5},{5,4},{6,7},{7,6},{8,9},{9,8},{10,11... | collective-permute-start | bytes 2359304 | tf_op jit(solution)/shard_map/ppermute | solution.py:267
  118.0 15.6 %all-to-all-start.2 = ((bf16[8,32,384]{2,1,0:T(8,128)(2,1)}), bf16[8,32,384]{2,1,0:T(8,128)(2,1)S(1)}, u32[]{:S(2)}, u32[]{:S(2)}) async-start(bf16[8,32,384]{2,1,0:T(8,128)(2,1)} %bitcast.4), calls=%async_computation.2 | async-start | bytes 393216 | tf_op jit(solution)/shard_map/all_to_all | solution.py:62
